TPU v7x, 32 devices: a whole 2x2x4 slice. The times are simulated.
32 devices in a mesh: sp: 8 (over z, y), tp: 4 (over x, core).
Axes of the slice: x: 2, y: 2, z: 4, core: 2. Of those that a mesh axis runs over, the one named last changes fastest.
Arguments:
- skip_trunk_vector: bfloat16 [4096, 2048], P('sp', 'tp'), may hold values from -16 to 16
- valve_preactivation: bfloat16 [4096, 2048], P('sp', 'tp'), may hold values from -6 to 6
- projected_heads_payload: bfloat16 [4096, 2048], P('sp', 'tp'), may hold values from -6 to 6
- cluster_ingests: bfloat16 [4096, 1024], P('sp', 'tp'), may hold values from -6 to 6
- cluster_observers: bfloat16 [4096, 1024], P('sp', 'tp'), may hold values from -6 to 6
- pre_softplus_increments: float32 [2, 4096, 32], P(None, 'sp', 'tp'), may hold values from -6 to 6
- attenuation_ln_rate: float32 [2, 32], P(None, 'tp'), may hold values from -13 to -3
- additional_attenuation: float32 [2, 4096, 32], P(None, 'sp', 'tp'), may hold values from -3 to 0
- payload_conv_weights: float32 [7, 2048], P(None, 'tp'), may hold values from -2 to 2
- ingest_conv_weights: float32 [7, 1024], P(None, 'tp'), may hold values from -2 to 2
- observer_conv_weights: float32 [7, 1024], P(None, 'tp'), may hold values from -2 to 2
- valved_cluster_factor: float32 [2048], P('tp'), may hold values from 0.1 to 1.9
- closing_map_matrix: bfloat16 [2048, 2048], P('tp'), may hold values from -0.125 to 0.125
- dense_standardize_factor: float32 [2048], replicated, may hold values from 0.1 to 1.9
- dense_valve_map: bfloat16 [2048, 5120], P('sp', 'tp'), may hold values from -0.125 to 0.125
- dense_payload_map: bfloat16 [2048, 5120], P('sp', 'tp'), may hold values from -0.125 to 0.125
- valve_series_smoother: float32 [3, 5120], P(None, 'tp'), may hold values from -3.5 to 3.5
- payload_series_smoother: float32 [3, 5120], P(None, 'tp'), may hold values from -3.5 to 3.5
- dense_contract_map: bfloat16 [5120, 2048], P('tp', 'sp'), may hold values from -0.078125 to 0.078125
Outputs:
- updated: bfloat16 [4096, 2048], P('sp', 'tp')
All inputs are finite; a program needn't handle non-finite values.
Results may differ from a plain program's by a relative error of at most 0.019.
Values may be sent and summed in bfloat16 or wider, within the bound.
No kernel may reach another device: no remote copies, remote signals or barrier semaphores. Data moves between devices by JAX's collectives and lax.ppermute only.
A program may use at most 64 MiB of HBM per device.

v0:
```python
import functools

import jax
import jax.numpy as jnp
import numpy as np
from jax import lax
from jax.experimental import pallas as pl
from jax.experimental.pallas import tpu as pltpu
from jax.sharding import PartitionSpec as P


STATE = 128
EPSILON = 1e-06
TAIL = 16


def ring_cycle(mesh):
    line = mesh.devices[:, 0].ravel()
    count = len(line)
    if not all(hasattr(d, "coords") for d in line):
        return list(range(count))
    spots = {(d.coords[2], d.coords[1]): i for i, d in enumerate(line)}
    deep = sorted({z for z, _ in spots})
    wide = sorted({y for _, y in spots})
    if len(spots) != count or len(deep) % 2 or len(wide) < 2:
        return list(range(count))
    path = []
    for at, z in enumerate(deep):
        row = wide[1:] if at % 2 == 0 else wide[:0:-1]
        path += [(z, y) for y in row]
    path += [(z, wide[0]) for z in reversed(deep)]
    return [spots[spot] for spot in path]


def bit_reverse(value, bits):
    return int(format(value, f"0{bits}b")[::-1], 2) if bits else 0


class Butterfly:
    def __init__(self, count):
        self.count = count
        self.bits = count.bit_length() - 1
        self.scatter_mask = [bit_reverse(count - 1 - p, self.bits) for p in range(count)]
        self.gather_mask = [bit_reverse(p, self.bits) for p in range(count)]

    def swap(self, array, bit):
        return lax.ppermute(array, "tp", [(i, i ^ (1 << bit)) for i in range(self.count)])

    def reduce_scatter(self, send, keep):
        for bit in range(self.bits):
            received = self.swap(send.astype(jnp.bfloat16), bit)
            held = keep.astype(jnp.float32) + received.astype(jnp.float32)
            half = held.shape[1] // 2
            send, keep = held[:, :half], held[:, half:]
        return held

    def gather(self, own):
        pieces = [own]
        for bit in reversed(range(self.bits)):
            held = pieces[0] if len(pieces) == 1 else jnp.concatenate(pieces, axis=1)
            pieces.append(self.swap(held, bit))
        return pieces


def softplus(v):
    return jnp.maximum(v, 0.0) + jnp.log1p(jnp.exp(-jnp.abs(v)))


def three(v, axis):
    high = v.astype(jnp.bfloat16)
    rest = v - high.astype(jnp.float32)
    mid = rest.astype(jnp.bfloat16)
    low = (rest - mid.astype(jnp.float32)).astype(jnp.bfloat16)
    return jnp.concatenate([high, mid, low], axis=axis)


def spread(v, width):
    heads = v.shape[1]
    high = v.astype(jnp.bfloat16)
    low = (v - high.astype(jnp.float32)).astype(jnp.bfloat16)
    row = lax.broadcasted_iota(jnp.int32, (2 * heads, heads * width), 0)
    column = lax.broadcasted_iota(jnp.int32, (2 * heads, heads * width), 1) // width
    pick = ((row == column) | (row - heads == column)).astype(jnp.float32).astype(jnp.bfloat16)
    return jnp.dot(
        jnp.concatenate([high, low], axis=1), pick, preferred_element_type=jnp.float32
    )


def decay_kernel(pre_ref, add_ref, rate_ref, rows_ref, cols_ref, scale_ref, last_ref):
    _, heads, length = pre_ref.shape
    width = scale_ref.shape[2] // heads
    at0 = lax.broadcasted_iota(jnp.int32, (length, length), 0)
    at1 = lax.broadcasted_iota(jnp.int32, (length, length), 1)
    steps, runs = [], []
    for way in range(2):
        reach = (at0 <= at1) if way == 0 else (at0 >= at1)
        reach = reach.astype(jnp.float32).astype(jnp.bfloat16)
        step = softplus(pre_ref[way])
        log = add_ref[way] - step * jnp.exp(rate_ref[:, way : way + 1])
        sums = jnp.dot(three(log, 0), reach, preferred_element_type=jnp.float32)
        run = sums[:heads] + sums[heads : 2 * heads] + sums[2 * heads :]
        rows_ref[way] = jnp.log(step) - run
        steps.append(step)
        runs.append(run)
    rows_ref[2] = jnp.log(steps[0] + steps[1])
    rest = jnp.zeros((128 - 4 * heads, length), jnp.float32)
    turned = jnp.concatenate([*runs, *steps, rest], axis=0).T
    for way in range(2):
        down = turned[:, way * heads : (way + 1) * heads]
        step = turned[:, (2 + way) * heads : (3 + way) * heads]
        end = down[length - 1 : length] if way == 0 else down[0:1]
        cols_ref[way] = down
        scale_ref[way] = spread(jnp.exp(end - down) * step, width)
        last_ref[way] = spread(jnp.broadcast_to(jnp.exp(end), (8, heads)), width)


def message(state, decay):
    high = decay.astype(jnp.bfloat16).astype(jnp.float32)
    low = decay - high
    row = lax.broadcasted_iota(jnp.int32, (TAIL, state.shape[1]), 0)
    tail = jnp.where(row == 0, high, jnp.where(row == 1, low, 0.0))
    return jnp.concatenate([state, tail], axis=0).astype(jnp.bfloat16)


def state_kernel(values_ref, inputs_ref, scale_ref, last_ref, window_ref, decay_ref, send_f_ref, send_b_ref):
    groups = inputs_ref.shape[1] // STATE
    wide = values_ref.shape[1] // groups
    values = values_ref[...].astype(jnp.float32)
    for way, send_ref in enumerate((send_f_ref, send_b_ref)):
        scaled = (values * scale_ref[way]).astype(jnp.bfloat16)
        state = jnp.concatenate(
            [
                lax.dot_general(
                    inputs_ref[:, g * STATE : (g + 1) * STATE],
                    scaled[:, g * wide : (g + 1) * wide],
                    (((0,), (0,)), ((), ())),
                    preferred_element_type=jnp.float32,
                )
                for g in range(groups)
            ],
            axis=1,
        )
        window_ref[way] = state
        decay_ref[way] = last_ref[way]
        send_ref[...] = message(state, last_ref[way, 0:1])


def link_kernel(first, final, *refs):
    got_refs, window_ref, decay_ref = refs[:2], refs[2], refs[3]
    before_ref, before_decay_ref = (None, None) if first else refs[4:6]
    outs = refs[4:] if first else refs[6:]
    for way in range(2):
        got = got_refs[way][:STATE].astype(jnp.float32)
        got_decay = got_refs[way][STATE : STATE + 1].astype(jnp.float32) + got_refs[way][
            STATE + 1 : STATE + 2
        ].astype(jnp.float32)
        before, before_decay = got, got_decay
        if not first:
            before = got * before_decay_ref[way, 0:1] + before_ref[way]
            before_decay = got_decay * before_decay_ref[way, 0:1]
        if final:
            outs[0][way] = before.astype(jnp.bfloat16)
            continue
        decay = decay_ref[way, 0:1]
        state = got * decay + window_ref[way]
        decay = decay * got_decay
        outs[0][way] = before
        outs[1][way] = jnp.broadcast_to(before_decay, outs[1].shape[1:])
        outs[2][way] = state
        outs[3][way] = jnp.broadcast_to(decay, outs[3].shape[1:])
        outs[4 + way][...] = message(state, decay)


def within_kernel(values_ref, inputs_ref, readout_ref, rows_ref, cols_ref, out_ref):
    heads = rows_ref.shape[1]
    length = values_ref.shape[0]
    width = values_ref.shape[1] // heads
    tile = min(256, length)
    groups = inputs_ref.shape[1] // STATE
    per_group = heads // groups
    pack = max(1, 128 // width)
    lane = lax.broadcasted_iota(jnp.int32, (length, pack * width), 1) // width
    at0 = lax.broadcasted_iota(jnp.int32, (tile, tile), 0)
    at1 = lax.broadcasted_iota(jnp.int32, (tile, tile), 1)
    for g in range(groups):
        for i in range(length // tile):
            here = slice(i * tile, (i + 1) * tile)
            scores = lax.dot_general(
                readout_ref[here, g * STATE : (g + 1) * STATE],
                inputs_ref[:, g * STATE : (g + 1) * STATE],
                (((1,), (1,)), ((), ())),
                preferred_element_type=jnp.float32,
            )
            for first in range(0, per_group, pack):
                total = None
                channels = slice((g * per_group + first) * width, (g * per_group + first + pack) * width)
                packed = values_ref[:, channels]
                for sub in range(pack):
                    h = g * per_group + first + sub
                    own = jnp.where(lane == sub, packed, jnp.zeros_like(packed))
                    down_f = cols_ref[0, here, h : h + 1]
                    down_b = cols_ref[1, here, h : h + 1]
                    pieces = []
                    for j in range(length // tile):
                        there = slice(j * tile, (j + 1) * tile)
                        if i > j:
                            gap = down_f + rows_ref[0, h : h + 1, there]
                        elif i < j:
                            gap = down_b + rows_ref[1, h : h + 1, there]
                        else:
                            gap = jnp.where(
                                at0 > at1,
                                down_f + rows_ref[0, h : h + 1, there],
                                jnp.where(
                                    at0 < at1,
                                    down_b + rows_ref[1, h : h + 1, there],
                                    rows_ref[2, h : h + 1, there],
                                ),
                            )
                        pieces.append((scores[:, there] * jnp.exp(gap)).astype(jnp.bfloat16))
                    weights = jnp.concatenate(pieces, axis=1)
                    term = jnp.dot(weights, own, preferred_element_type=jnp.float32)
                    total = term if total is None else total + term
                out_ref[here, channels] = total


def close_kernel(sizes, info_ref, within_ref, readout_ref, cols_ref, states_ref, valve_ref, factor_ref, map_ref, send_ref, keep_ref):
    groups = readout_ref.shape[1] // STATE
    wide = within_ref.shape[1] // groups
    heads = cols_ref.shape[2]
    width = within_ref.shape[1] // heads
    lift_f = spread(jnp.exp(cols_ref[0]), width)
    lift_b = spread(jnp.exp(cols_ref[1]), width)
    blended = []
    for g in range(groups):
        at = slice(g * wide, (g + 1) * wide)
        readout = readout_ref[:, g * STATE : (g + 1) * STATE]
        carried_f = jnp.dot(readout, states_ref[0, :, at], preferred_element_type=jnp.float32)
        carried_b = jnp.dot(readout, states_ref[1, :, at], preferred_element_type=jnp.float32)
        mixed = within_ref[:, at] + carried_f * lift_f[:, at] + carried_b * lift_b[:, at]
        valve = valve_ref[:, at].astype(jnp.float32)
        gated = mixed * (valve / (1.0 + jnp.exp(-valve)))
        square = jnp.mean(gated * gated, axis=1, keepdims=True)
        scaled = gated * lax.rsqrt(square + EPSILON)
        blended.append((scaled * factor_ref[:, at]).astype(jnp.bfloat16))
    rows = jnp.concatenate(blended, axis=1)
    sp_count, count = sizes
    block = map_ref.shape[1] // count
    for p in range(count):
        columns = pl.ds(pl.multiple_of(info_ref[2 * sp_count + p] * block, block), block)
        term = jnp.dot(rows, map_ref[:, columns], preferred_element_type=jnp.float32).astype(jnp.bfloat16)
        target, at = (send_ref, p) if p < count // 2 else (keep_ref, p - count // 2)
        target[:, at * block : (at + 1) * block] = term


def up_kernel(sizes, plan, counts, *refs):
    n_pieces, n_arrays = counts
    sp_count, tp_count = sizes
    info_ref, gain_ref = refs[:2]
    pieces = refs[2 : 2 + n_pieces]
    arrays = refs[2 + n_pieces : 2 + n_pieces + n_arrays]
    outs = refs[2 + n_pieces + n_arrays : 4 + n_pieces + n_arrays]
    rows_scr, gain_scr = refs[4 + n_pieces + n_arrays :]
    length, full = pieces[0].shape[0], gain_ref.shape[1]
    chunk, block = full // sp_count, full // tp_count
    for p in range(tp_count):
        at = pl.multiple_of(info_ref[2 * sp_count + tp_count + p] * block, block)
        gain_scr[:, p * block : (p + 1) * block] = gain_ref[:, pl.ds(at, block)]

    band = 64

    def norm(r, carry):
        rows = pl.ds(pl.multiple_of(r * band, band), band)
        parts = [piece[rows, :].astype(jnp.float32) for piece in pieces]
        square = sum(jnp.sum(part * part, axis=1, keepdims=True) for part in parts) / full
        factor = lax.rsqrt(square + EPSILON)
        start = 0
        for part in parts:
            for first in range(0, part.shape[1], chunk):
                at = start + first
                rows_scr[at // chunk, rows, :] = (
                    part[:, first : first + chunk] * factor * gain_scr[:, at : at + chunk]
                ).astype(jnp.bfloat16)
            start += part.shape[1]
        return carry

    lax.fori_loop(0, length // band, norm, 0)
    columns = outs[0].shape[1]
    tile = 256 if columns % 256 == 0 else columns
    for which in range(2):
        for j in range(columns // tile):
            at = slice(j * tile, (j + 1) * tile)
            total = None
            for array, first, source in plan[which]:
                term = jnp.dot(
                    rows_scr[info_ref[source] // chunk],
                    arrays[array][first : first + chunk, at],
                    preferred_element_type=jnp.float32,
                )
                total = term if total is None else total + term
            outs[which][:, at] = total.astype(jnp.bfloat16)


def down_kernel(sizes, plan, n_arrays, *refs):
    info_ref, hidden_ref = refs[:2]
    arrays = refs[2 : 2 + n_arrays]
    send_ref, keep_ref = refs[2 + n_arrays :]
    half = send_ref.shape[1]
    for source, parts in enumerate(plan):
        term = None
        for array, row in parts:
            depth, chunk = arrays[array].shape
            part = jnp.dot(
                hidden_ref[:, row : row + depth], arrays[array][...], preferred_element_type=jnp.float32
            )
            term = part if term is None else term + part
        term = term.astype(jnp.bfloat16)
        if len(plan) == 1:
            send_ref[...] = term[:, :half]
            keep_ref[...] = term[:, half:]
            continue
        at = info_ref[sizes[0] + source]

        @pl.when(at < half)
        def _():
            send_ref[:, pl.ds(pl.multiple_of(at, chunk), chunk)] = term

        @pl.when(at >= half)
        def _():
            keep_ref[:, pl.ds(pl.multiple_of(at - half, chunk), chunk)] = term


def conv_rows(padded, kernel, length):
    summed = padded[0:length] * kernel[0]
    for offset in range(1, kernel.shape[0]):
        summed = summed + padded[offset : offset + length] * kernel[offset]
    return summed


def edges(last, first):
    count = lax.axis_size("sp")
    forward = [(i, i + 1) for i in range(count - 1)]
    backward = [(b, a) for a, b in forward]
    low = lax.ppermute(last, "sp", forward)
    high = lax.ppermute(first, "sp", backward)
    return low, high


def call(kernel, outs, *args, scalars=0, scratch=()):
    spaces = [pltpu.SMEM] * scalars + [pltpu.VMEM] * (len(args) - scalars)
    return pl.pallas_call(
        kernel,
        out_shape=[jax.ShapeDtypeStruct(shape, kind) for shape, kind in outs],
        in_specs=[pl.BlockSpec(memory_space=space) for space in spaces],
        scratch_shapes=list(scratch),
        compiler_params=pltpu.CompilerParams(vmem_limit_bytes=32 * 1024 * 1024),
    )(*args)


def solution(mesh):
    cycle = ring_cycle(mesh)
    sp_count = mesh.shape["sp"]
    tp_count = mesh.shape["tp"]
    place = {s: i for i, s in enumerate(cycle)}
    right = [(cycle[i], cycle[(i + 1) % sp_count]) for i in range(sp_count)]
    left = [(b, a) for a, b in right]
    tp = Butterfly(tp_count)
    scatter_place = np.argsort(np.array(tp.scatter_mask))
    gather_place = np.argsort(np.array(tp.gather_mask))

    def table(chunk, own_cols):
        lines = []
        for s in range(sp_count):
            for t in range(tp_count):
                up, down = [], []
                for steps in range(sp_count):
                    block, rest = divmod(cycle[(place[s] - steps) % sp_count] * chunk, own_cols)
                    up.append(gather_place[block ^ t] * own_cols + rest)
                    down.append(scatter_place[block ^ t] * own_cols + rest)
                lines.append(up + down + [t ^ m for m in tp.scatter_mask] + [t ^ m for m in tp.gather_mask])
        return np.array(lines, np.int32)

    def send_on(array, pairs):
        return lax.ppermute(array, "sp", pairs)

    def ring(join, half):
        out = []
        going, coming = join, join
        for step in range(1, (sp_count - 1) // 2 + 1):
            going = send_on(going, right)
            coming = send_on(coming, left)
            out += [(step, going, None), (-step, coming, None)]
        if sp_count % 2 == 0:
            far = sp_count // 2
            out.append((far, send_on(going[:half], right), 0))
            out.append((far, send_on(coming[half:], left), 1))
        return out

    def shards(
        skip_trunk_vector,
        valve_preactivation,
        projected_heads_payload,
        cluster_ingests,
        cluster_observers,
        pre_softplus_increments,
        attenuation_ln_rate,
        additional_attenuation,
        payload_conv_weights,
        ingest_conv_weights,
        observer_conv_weights,
        valved_cluster_factor,
        closing_map_matrix,
        dense_standardize_factor,
        dense_valve_map,
        dense_payload_map,
        valve_series_smoother,
        payload_series_smoother,
        dense_contract_map,
    ):
        length = skip_trunk_vector.shape[0]
        heads = pre_softplus_increments.shape[2]
        channels = projected_heads_payload.shape[1]
        in_cols = cluster_ingests.shape[1]
        own_cols = skip_trunk_vector.shape[1]
        me = lax.axis_index("tp")

        margin = payload_conv_weights.shape[0] // 2
        streams = (projected_heads_payload, cluster_ingests, cluster_observers)
        low, high = edges(
            jnp.concatenate([a[length - margin :] for a in streams], axis=1),
            jnp.concatenate([a[:margin] for a in streams], axis=1),
        )

        full = own_cols * tp_count
        hidden_cols = dense_valve_map.shape[1]
        chunk = dense_valve_map.shape[0]
        middle_row = hidden_cols // 2
        up_ring = [(0, dense_valve_map, 0), (0, dense_payload_map, 1)]
        up_ring += ring(jnp.concatenate([dense_valve_map, dense_payload_map], axis=0), chunk)
        down_ring = [(0, dense_contract_map, None)] + ring(dense_contract_map, middle_row)

        info = jnp.asarray(table(chunk, own_cols))[lax.axis_index("sp") * tp_count + me]

        rows, cols, scale, last = call(
            decay_kernel,
            [
                ((3, heads, length), jnp.float32),
                ((2, length, heads), jnp.float32),
                ((2, length, channels), jnp.float32),
                ((2, 8, channels), jnp.float32),
            ],
            jnp.transpose(pre_softplus_increments, (0, 2, 1)),
            jnp.transpose(additional_attenuation, (0, 2, 1)),
            attenuation_ln_rate.T,
        )

        def mixed(array, low, high, kernel):
            padded = jnp.concatenate([low, array, high], axis=0).astype(jnp.float32)
            return jax.nn.silu(conv_rows(padded, kernel, length)).astype(jnp.bfloat16)

        ends = (channels, channels + in_cols)
        lows, highs = jnp.split(low, ends, axis=1), jnp.split(high, ends, axis=1)
        values = mixed(projected_heads_payload, lows[0], highs[0], payload_conv_weights)
        inputs = mixed(cluster_ingests, lows[1], highs[1], ingest_conv_weights)
        readout = mixed(cluster_observers, lows[2], highs[2], observer_conv_weights)
        wide_state = ((2, STATE, channels), jnp.float32)
        wide_decay = ((2, 8, channels), jnp.float32)
        sent = ((STATE + TAIL, channels), jnp.bfloat16)
        window, decay, send_f, send_b = call(
            state_kernel, [wide_state, wide_decay, sent, sent], values, inputs, scale, last
        )
        (within,) = call(
            within_kernel, [((length, channels), jnp.float32)], values, inputs, readout, rows, cols
        )

        before, offset = (), 1
        while offset < sp_count:
            forward = [(i, i + offset) for i in range(sp_count - offset)]
            got_f = lax.ppermute(send_f, "sp", forward)
            got_b = lax.ppermute(send_b, "sp", [(b, a) for a, b in forward])
            final = 2 * offset >= sp_count
            outs = [((2, STATE, channels), jnp.bfloat16)]
            if not final:
                outs = [wide_state, wide_decay, wide_state, wide_decay, sent, sent]
            result = call(
                functools.partial(link_kernel, offset == 1, final), outs, got_f, got_b, window, decay, *before
            )
            if final:
                states = result[0]
            else:
                before, (window, decay, send_f, send_b) = tuple(result[:2]), result[2:]
            offset *= 2

        half_full = full // 2
        send, keep = call(
            functools.partial(close_kernel, (sp_count, tp_count)),
            [((length, half_full), jnp.bfloat16)] * 2,
            info,
            within,
            readout,
            cols,
            states,
            valve_preactivation,
            valved_cluster_factor[None, :],
            closing_map_matrix,
            scalars=1,
        )
        projected = tp.reduce_scatter(send, keep)
        middle = (skip_trunk_vector.astype(jnp.float32) + projected).astype(jnp.bfloat16)
        pieces = tp.gather(middle)

        arrays, plan = [], ([], [])
        for steps, array, part in up_ring:
            for which in (0, 1) if part is None else (part,):
                plan[which].append((len(arrays), which * chunk if part is None else 0, steps % sp_count))
            arrays.append(array)
        gate_rows, value_rows = call(
            functools.partial(up_kernel, (sp_count, tp_count), plan, (len(pieces), len(arrays))),
            [((length, hidden_cols), jnp.bfloat16)] * 2,
            info,
            dense_standardize_factor[None, :],
            *pieces,
            *arrays,
            scalars=1,
            scratch=[pltpu.VMEM((sp_count, length, chunk), jnp.bfloat16), pltpu.VMEM((1, full), jnp.float32)],
        )
        margin = valve_series_smoother.shape[0] // 2
        low, high = edges(
            jnp.concatenate([gate_rows[length - margin :], value_rows[length - margin :]], axis=1),
            jnp.concatenate([gate_rows[:margin], value_rows[:margin]], axis=1),
        )

        def smooth(array, low, high, kernel):
            return conv_rows(jnp.concatenate([low, array, high], axis=0).astype(jnp.float32), kernel, length)

        gate = smooth(gate_rows, low[:, :hidden_cols], high[:, :hidden_cols], valve_series_smoother)
        value = smooth(value_rows, low[:, hidden_cols:], high[:, hidden_cols:], payload_series_smoother)
        hidden = (jax.nn.silu(gate) * value).astype(jnp.bfloat16)

        arrays = []
        if chunk % 128 == 0:
            plan = [[] for _ in range(sp_count)]
            for steps, array, part in down_ring:
                plan[steps % sp_count].append((len(arrays), middle_row if part == 1 else 0))
                arrays.append(array)
        else:
            whole = jnp.zeros((hidden_cols, full), jnp.bfloat16)
            for steps, array, part in down_ring:
                corner = (middle_row if part == 1 else 0, info[sp_count + steps % sp_count])
                whole = lax.dynamic_update_slice(whole, array, corner)
            arrays, plan = [whole], [[(0, 0)]]
        send, keep = call(
            functools.partial(down_kernel, (sp_count, tp_count), plan, len(arrays)),
            [((length, half_full), jnp.bfloat16)] * 2,
            info,
            hidden,
            *arrays,
            scalars=1,
        )
        down_sum = tp.reduce_scatter(send, keep)
        return (middle.astype(jnp.float32) + down_sum).astype(jnp.bfloat16)

    return jax.shard_map(
        shards,
        mesh=mesh,
        in_specs=(
            P("sp", "tp"),
            P("sp", "tp"),
            P("sp", "tp"),
            P("sp", "tp"),
            P("sp", "tp"),
            P(None, "sp", "tp"),
            P(None, "tp"),
            P(None, "sp", "tp"),
            P(None, "tp"),
            P(None, "tp"),
            P(None, "tp"),
            P("tp"),
            P("tp", None),
            P(),
            P("sp", "tp"),
            P("sp", "tp"),
            P(None, "tp"),
            P(None, "tp"),
            P("tp", "sp"),
        ),
        out_specs=P("sp", "tp"),
        check_vma=False,
    )
```

profile of v0, /device:TPU:0, one launch (start us, length us, event | category | flops | bytes accessed | tf_op | source)
XLA Modules:
  0.0 241.2 jit_solution(13045485682832768177)
XLA Ops:
  0.0 2.1 constant_dynamic-update-slice_fusion.1
  2.1 2.0 constant_dynamic-update-slice_fusion
  4.1 3.0 %collective-permute-start.12 = (bf16[512,1280]{1,0:T(8,128)(2,1)}, bf16[512,1280]{1,0:T(8,128)(2,1)S(1)}, u32[]{:S(2)}, u32[]{:S(2)}) collective-permute-start(bf16[512,1280]{1,0:T(8,128)(2,1)} %constant_dynamic-update-slice_fusion), channel_id=1, source_target_pairs={{4,12},{12,20},{20,28},{28,24},{24,16},{16,8},{8,0},{0,4},{5,13},{... | collective-permute-start | bytes 3932168 | tf_op jit(solution)/shard_map/ppermute | solution.py:384
  7.2 0.7 fusion.31
  7.9 3.9 %collective-permute-start = (bf16[3,1024]{1,0:T(4,128)(2,1)S(1)}, bf16[3,1024]{1,0:T(4,128)(2,1)S(1)}, u32[]{:S(2)}, u32[]{:S(2)}) collective-permute-start(bf16[3,1024]{1,0:T(4,128)(2,1)S(1)} %pad_maximum_fusion.3), channel_id=1, source_target_pairs={{0,4},{4,8},{8,12},{12,16},{16,20},{20,24},{24,28},{1,5},{5,9},{9,... | collective-permute-start | bytes 18440 | tf_op jit(solution)/shard_map/ppermute | solution.py:344
  11.8 1.3 collective-permute-start.1
  13.1 0.6 fusion.39
  13.7 0.8 copy.21
  14.5 1.2 shard_map.190
  15.7 20.1 %collective-permute-done = bf16[3,1024]{1,0:T(4,128)(2,1)S(1)} collective-permute-done((bf16[3,1024]{1,0:T(4,128)(2,1)S(1)}, bf16[3,1024]{1,0:T(4,128)(2,1)S(1)}, u32[]{:S(2)}, u32[]{:S(2)}) %collective-permute-start) | collective-permute-done | bytes 6176 | tf_op jit(solution)/shard_map/ppermute | solution.py:344
  35.7 2.0 collective-permute-done.1
  38.0 0.5 multiply_convert_fusion.2.inputs_ref
  38.5 1.1 multiply_convert_fusion.values_ref
  39.6 0.5 shard_map.192
  40.1 2.4 collective-permute-start.2
  42.5 1.3 collective-permute-start.3
  43.8 1.3 collective-permute-done.2.refs_0_
  45.1 4.7 %collective-permute-done.3.refs_1_ = bf16[144,512]{1,0:T(8,128)(2,1)S(1)} collective-permute-done((bf16[144,512]{1,0:T(8,128)(2,1)S(1)}, bf16[144,512]{1,0:T(8,128)(2,1)S(1)}, u32[]{:S(2)}, u32[]{:S(2)}) %collective-permute-start.3) | collective-permute-done | bytes 147488 | tf_op jit(solution)/shard_map/ppermute | solution.py:480
  49.9 4.4 %collective-permute-start.4 = (bf16[144,512]{1,0:T(8,128)(2,1)S(1)}, bf16[144,512]{1,0:T(8,128)(2,1)S(1)}, u32[]{:S(2)}, u32[]{:S(2)}) collective-permute-start(bf16[144,512]{1,0:T(8,128)(2,1)S(1)} %get-tuple-element.39), channel_id=1, source_target_pairs={{0,8},{4,12},{8,16},{12,20},{16,24},{20,28},{1,9},{5,13},{9,17},{1... | collective-permute-start | bytes 442376 | tf_op jit(solution)/shard_map/ppermute | solution.py:479
  54.3 1.3 collective-permute-start.5
  55.6 0.7 dynamic-slice_bitcast_fusion.info_ref.refs_0_
  56.4 0.6 collective-permute-done.4.refs_0_
  56.9 4.4 %collective-permute-done.5.refs_1_ = bf16[144,512]{1,0:T(8,128)(2,1)S(1)} collective-permute-done((bf16[144,512]{1,0:T(8,128)(2,1)S(1)}, bf16[144,512]{1,0:T(8,128)(2,1)S(1)}, u32[]{:S(2)}, u32[]{:S(2)}) %collective-permute-start.5) | collective-permute-done | bytes 147488 | tf_op jit(solution)/shard_map/ppermute | solution.py:480
  61.5 4.0 %collective-permute-start.6 = (bf16[144,512]{1,0:T(8,128)(2,1)S(1)}, bf16[144,512]{1,0:T(8,128)(2,1)S(1)}, u32[]{:S(2)}, u32[]{:S(2)}) collective-permute-start(bf16[144,512]{1,0:T(8,128)(2,1)S(1)} %get-tuple-element.45), channel_id=1, source_target_pairs={{0,16},{4,20},{8,24},{12,28},{1,17},{5,21},{9,25},{13,29},{2,18},{... | collective-permute-start | bytes 442376 | tf_op jit(solution)/shard_map/ppermute | solution.py:479
  65.5 1.3 collective-permute-start.7
  66.8 0.5 multiply_convert_fusion.1.readout_ref
  67.4 2.9 %shard_map.191.within_ref = f32[512,512]{1,0:T(8,128)S(1)} custom-call(bf16[512,512]{1,0:T(8,128)(2,1)S(1)} %multiply_convert_fusion.values_ref, bf16[512,256]{1,0:T(8,128)(2,1)S(1)} %multiply_convert_fusion.2.inputs_ref, bf16[512,256]{1,0:T(8,128)(2,1)S(1)} %multiply_convert_fusion.1.readout_ref, f32[3,8,512]{2,1,0:T(8,128)S(1)} %get-tuple-element.31.rows_ref, ...), custom_call_target="tpu_custom_call" | custom-call | tf_op jit(solution)/shard_map/pallas_call | solution.py:351
  70.3 3.7 %collective-permute-done.7.refs_1_ = bf16[144,512]{1,0:T(8,128)(2,1)S(1)} collective-permute-done((bf16[144,512]{1,0:T(8,128)(2,1)S(1)}, bf16[144,512]{1,0:T(8,128)(2,1)S(1)}, u32[]{:S(2)}, u32[]{:S(2)}) %collective-permute-start.7) | collective-permute-done | bytes 147488 | tf_op jit(solution)/shard_map/ppermute | solution.py:480
  74.1 2.7 %shard_map.196 = (bf16[512,1024]{1,0:T(8,128)(2,1)S(1)}, bf16[512,1024]{1,0:T(8,128)(2,1)S(1)}) custom-call(s32[24]{0:T(128)S(1)} %dynamic-slice_bitcast_fusion.info_ref.refs_0_, f32[512,512]{1,0:T(8,128)S(1)} %shard_map.191.within_ref, bf16[512,256]{1,0:T(8,128)(2,1)S(1)} %multiply_convert_fusion.1.readout_ref, ...), custom_call_target="tpu_custom_call" | custom-call | tf_op jit(solution)/shard_map/pallas_call | solution.py:351
  77.0 1.4 collective-permute-start.14
  78.4 0.7 collective-permute-start.15
  79.1 0.6 collective-permute-done.8
  79.6 0.4 convert_add_fusion.1
  80.1 1.6 collective-permute-start.9
  81.7 1.3 collective-permute-start.22
  83.0 0.7 collective-permute-start.23
  83.7 25.0 %collective-permute-done.14.refs_9_ = bf16[512,1280]{1,0:T(8,128)(2,1)S(1)} collective-permute-done((bf16[512,1280]{1,0:T(8,128)(2,1)S(1)}, bf16[512,1280]{1,0:T(8,128)(2,1)S(1)}, u32[]{:S(2)}, u32[]{:S(2)}) %collective-permute-start.14) | collective-permute-done | bytes 1310752 | tf_op jit(solution)/shard_map/ppermute | solution.py:384
  108.7 1.3 collective-permute-start.16
  110.0 0.7 collective-permute-start.17
  111.0 1.6 collective-permute-start.10
  112.5 10.2 %collective-permute-done.22.refs_3_ = bf16[1280,256]{1,0:T(8,128)(2,1)S(1)} collective-permute-done((bf16[1280,256]{1,0:T(8,128)(2,1)S(1)}, bf16[1280,256]{1,0:T(8,128)(2,1)S(1)}, u32[]{:S(2)}, u32[]{:S(2)}) %collective-permute-start.22) | collective-permute-done | bytes 655392 | tf_op jit(solution)/shard_map/ppermute | solution.py:384
  122.7 1.3 collective-permute-start.24
  124.0 0.7 collective-permute-start.25
  125.0 39.3 %collective-permute-done.24.refs_5_ = bf16[1280,256]{1,0:T(8,128)(2,1)S(1)} collective-permute-done((bf16[1280,256]{1,0:T(8,128)(2,1)S(1)}, bf16[1280,256]{1,0:T(8,128)(2,1)S(1)}, u32[]{:S(2)}, u32[]{:S(2)}) %collective-permute-start.24) | collective-permute-done | bytes 655392 | tf_op jit(solution)/shard_map/ppermute | solution.py:384
  164.3 1.3 collective-permute-start.26
  165.7 0.7 collective-permute-start.27
  166.4 1.4 collective-permute-start.18
  167.8 0.8 collective-permute-start.19
  168.7 13.2 %collective-permute-done.26.refs_7_ = bf16[1280,256]{1,0:T(8,128)(2,1)S(1)} collective-permute-done((bf16[1280,256]{1,0:T(8,128)(2,1)S(1)}, bf16[1280,256]{1,0:T(8,128)(2,1)S(1)}, u32[]{:S(2)}, u32[]{:S(2)}) %collective-permute-start.26) | collective-permute-done | bytes 655392 | tf_op jit(solution)/shard_map/ppermute | solution.py:384
  182.0 1.4 collective-permute-start.28
  183.4 0.8 collective-permute-start.29
  184.1 11.9 %collective-permute-done.18.refs_13_ = bf16[256,1280]{1,0:T(8,128)(2,1)S(1)} collective-permute-done((bf16[256,1280]{1,0:T(8,128)(2,1)S(1)}, bf16[256,1280]{1,0:T(8,128)(2,1)S(1)}, u32[]{:S(2)}, u32[]{:S(2)}) %collective-permute-start.18) | collective-permute-done | bytes 655392 | tf_op jit(solution)/shard_map/ppermute | solution.py:384
  196.0 1.3 collective-permute-done.19.refs_14_
  197.3 7.5 %shard_map.197 = (bf16[512,1280]{1,0:T(8,128)(2,1)S(1)}, bf16[512,1280]{1,0:T(8,128)(2,1)S(1)}) custom-call(s32[24]{0:T(128)S(1)} %dynamic-slice_bitcast_fusion.info_ref.refs_0_, f32[1,2048]{1,0:T(1,128)S(1)} %bitcast.31, bf16[512,512]{1,0:T(8,128)(2,1)S(1)} %fusion.9.refs_2_, bf16[512,512]{1,0:T(8,128)(2,1)S(1)} %collective-permute-done.10.refs_3_, ...), custom_call_target="tpu_custom_call" | custom-call | tf_op jit(solution)/shard_map/pallas_call | solution.py:351
  204.9 2.2 collective-permute-start.20
  207.1 1.3 collective-permute-start.21
  208.4 4.2 %collective-permute-done.21 = bf16[1,2560]{1,0:T(2,128)(2,1)S(1)} collective-permute-done((bf16[1,2560]{1,0:T(2,128)(2,1)S(1)}, bf16[1,2560]{1,0:T(2,128)(2,1)S(1)}, u32[]{:S(2)}, u32[]{:S(2)}) %collective-permute-start.21) | collective-permute-done | bytes 5152 | tf_op jit(solution)/shard_map/ppermute | solution.py:345
  213.2 2.1 fusion.2.refs_1_
  215.4 7.5 %shard_map.198 = (bf16[512,1024]{1,0:T(8,128)(2,1)S(1)}, bf16[512,1024]{1,0:T(8,128)(2,1)S(1)}) custom-call(s32[24]{0:T(128)S(1)} %dynamic-slice_bitcast_fusion.info_ref.refs_0_, bf16[512,1280]{1,0:T(8,128)(2,1)S(1)} %fusion.2.refs_1_, bf16[1280,256]{1,0:T(8,128)(2,1)S(1)} %copy-done.3, bf16[1280,256]{1,0:T(8,128)(2,1)S(1)} %collective-permute-done.22.refs_3_, ...), custom_call_target="tpu_custom_call" | custom-call | tf_op jit(solution)/shard_map/pallas_call | solution.py:351
  223.0 2.6 %collective-permute-done.30 = bf16[512,1024]{1,0:T(8,128)(2,1)S(1)} collective-permute-done((bf16[512,1024]{1,0:T(8,128)(2,1)S(1)}, bf16[512,1024]{1,0:T(8,128)(2,1)S(1)}, u32[]{:S(2)}, u32[]{:S(2)}) %collective-permute-start.30) | collective-permute-done | bytes 1048608 | tf_op jit(solution)/shard_map/ppermute | solution.py:47
  225.6 0.4 convert_add_fusion
  226.1 1.6 collective-permute-start.31
  227.6 12.5 %collective-permute-done.31 = bf16[512,512]{1,0:T(8,128)(2,1)S(1)} collective-permute-done((bf16[512,512]{1,0:T(8,128)(2,1)S(1)}, bf16[512,512]{1,0:T(8,128)(2,1)S(1)}, u32[]{:S(2)}, u32[]{:S(2)}) %collective-permute-start.31) | collective-permute-done | bytes 524320 | tf_op jit(solution)/shard_map/ppermute | solution.py:47
  240.1 1.0 fusion.7
  (93 shorter events, 2.5 us)
Async XLA Ops:
  0.0 7.1 %copy-start.9 = (bf16[512,512]{1,0:T(8,128)(2,1)S(1)}, bf16[512,512]{1,0:T(8,128)(2,1)}, u32[]{:S(2)}) copy-start(bf16[512,512]{1,0:T(8,128)(2,1)} %param.22) | copy-start | bytes 1572868
  0.0 7.1 %copy-start.11 = (bf16[512,256]{1,0:T(8,128)(2,1)S(1)}, bf16[512,256]{1,0:T(8,128)(2,1)}, u32[]{:S(2)}) copy-start(bf16[512,256]{1,0:T(8,128)(2,1)} %param.23) | copy-start | bytes 786436
  0.0 13.1 %copy-start.13 = (f32[7,512]{1,0:T(8,128)S(1)}, f32[7,512]{1,0:T(8,128)}, u32[]{:S(2)}) copy-start(f32[7,512]{1,0:T(8,128)} %param.28) | copy-start | bytes 43012
  0.0 13.1 %copy-start.16 = (f32[7,256]{1,0:T(8,128)S(1)}, f32[7,256]{1,0:T(8,128)}, u32[]{:S(2)}) copy-start(f32[7,256]{1,0:T(8,128)} %param.29) | copy-start | bytes 21508
  0.0 14.5 %copy-start.5 = (f32[2,512,8]{1,2,0:T(8,128)S(1)}, f32[2,512,8]{1,2,0:T(8,128)}, u32[]{:S(2)}) copy-start(f32[2,512,8]{1,2,0:T(8,128)} %param.25) | copy-start | bytes 98308
  0.0 14.5 %copy-start.6 = (f32[2,512,8]{1,2,0:T(8,128)S(1)}, f32[2,512,8]{1,2,0:T(8,128)}, u32[]{:S(2)}) copy-start(f32[2,512,8]{1,2,0:T(8,128)} %param.27) | copy-start | bytes 98308
  4.1 72.9 %collective-permute-start.12 = (bf16[512,1280]{1,0:T(8,128)(2,1)}, bf16[512,1280]{1,0:T(8,128)(2,1)S(1)}, u32[]{:S(2)}, u32[]{:S(2)}) collective-permute-start(bf16[512,1280]{1,0:T(8,128)(2,1)} %constant_dynamic-update-slice_fusion), channel_id=1, source_target_pairs={{4,12},{12,20},{20,28},{28,24},{24,16},{16,8},{8,0},{0,4},{5,13},{... | collective-permute-start | bytes 3932168 | tf_op jit(solution)/shard_map/ppermute | solution.py:384
  7.1 71.3 %collective-permute-start.13 = (bf16[512,1280]{1,0:T(8,128)(2,1)}, bf16[512,1280]{1,0:T(8,128)(2,1)S(1)}, u32[]{:S(2)}, u32[]{:S(2)}) collective-permute-start(bf16[512,1280]{1,0:T(8,128)(2,1)} %constant_dynamic-update-slice_fusion), channel_id=1, source_target_pairs={{12,4},{20,12},{28,20},{24,28},{16,24},{8,16},{0,8},{4,0},{13,5},{... | collective-permute-start | bytes 3932168 | tf_op jit(solution)/shard_map/ppermute | solution.py:384
  7.9 27.8 %collective-permute-start = (bf16[3,1024]{1,0:T(4,128)(2,1)S(1)}, bf16[3,1024]{1,0:T(4,128)(2,1)S(1)}, u32[]{:S(2)}, u32[]{:S(2)}) collective-permute-start(bf16[3,1024]{1,0:T(4,128)(2,1)S(1)} %pad_maximum_fusion.3), channel_id=1, source_target_pairs={{0,4},{4,8},{8,12},{12,16},{16,20},{20,24},{24,28},{1,5},{5,9},{9,... | collective-permute-start | bytes 18440 | tf_op jit(solution)/shard_map/ppermute | solution.py:344
  11.8 25.9 %collective-permute-start.1 = (bf16[3,1024]{1,0:T(4,128)(2,1)S(1)}, bf16[3,1024]{1,0:T(4,128)(2,1)S(1)}, u32[]{:S(2)}, u32[]{:S(2)}) collective-permute-start(bf16[3,1024]{1,0:T(4,128)(2,1)S(1)} %pad_maximum_fusion.4), channel_id=1, source_target_pairs={{4,0},{8,4},{12,8},{16,12},{20,16},{24,20},{28,24},{5,1},{9,5},{13... | collective-permute-start | bytes 18440 | tf_op jit(solution)/shard_map/ppermute | solution.py:345
  14.5 23.5 %copy-start.18 = (f32[1,256]{1,0:T(1,128)S(1)}, f32[1,256]{1,0:T(1,128)}, u32[]{:S(2)}) copy-start(f32[1,256]{1,0:T(1,128)} %get-tuple-element.99) | copy-start | bytes 3076
  14.5 23.5 %copy-start.19 = (f32[1,256]{1,0:T(1,128)S(1)}, f32[1,256]{1,0:T(1,128)}, u32[]{:S(2)}) copy-start(f32[1,256]{1,0:T(1,128)} %get-tuple-element.100) | copy-start | bytes 3076
  14.5 23.5 %copy-start.20 = (f32[1,256]{1,0:T(1,128)S(1)}, f32[1,256]{1,0:T(1,128)}, u32[]{:S(2)}) copy-start(f32[1,256]{1,0:T(1,128)} %get-tuple-element.101) | copy-start | bytes 3076
  39.6 4.2 %copy-start.17 = (f32[7,256]{1,0:T(8,128)S(1)}, f32[7,256]{1,0:T(8,128)}, u32[]{:S(2)}) copy-start(f32[7,256]{1,0:T(8,128)} %param.30) | copy-start | bytes 21508
  39.6 16.7 %copy-start.12 = (bf16[512,256]{1,0:T(8,128)(2,1)S(1)}, bf16[512,256]{1,0:T(8,128)(2,1)}, u32[]{:S(2)}) copy-start(bf16[512,256]{1,0:T(8,128)(2,1)} %param.24) | copy-start | bytes 786436
  40.1 5.0 %collective-permute-start.2 = (bf16[144,512]{1,0:T(8,128)(2,1)S(1)}, bf16[144,512]{1,0:T(8,128)(2,1)S(1)}, u32[]{:S(2)}, u32[]{:S(2)}) collective-permute-start(bf16[144,512]{1,0:T(8,128)(2,1)S(1)} %get-tuple-element.35), channel_id=1, source_target_pairs={{0,4},{4,8},{8,12},{12,16},{16,20},{20,24},{24,28},{1,5},{5,9},{9,... | collective-permute-start | bytes 442376 | tf_op jit(solution)/shard_map/ppermute | solution.py:479
  42.5 7.3 %collective-permute-start.3 = (bf16[144,512]{1,0:T(8,128)(2,1)S(1)}, bf16[144,512]{1,0:T(8,128)(2,1)S(1)}, u32[]{:S(2)}, u32[]{:S(2)}) collective-permute-start(bf16[144,512]{1,0:T(8,128)(2,1)S(1)} %get-tuple-element.36), channel_id=1, source_target_pairs={{4,0},{8,4},{12,8},{16,12},{20,16},{24,20},{28,24},{5,1},{9,5},{13... | collective-permute-start | bytes 442376 | tf_op jit(solution)/shard_map/ppermute | solution.py:480
  49.9 7.0 %collective-permute-start.4 = (bf16[144,512]{1,0:T(8,128)(2,1)S(1)}, bf16[144,512]{1,0:T(8,128)(2,1)S(1)}, u32[]{:S(2)}, u32[]{:S(2)}) collective-permute-start(bf16[144,512]{1,0:T(8,128)(2,1)S(1)} %get-tuple-element.39), channel_id=1, source_target_pairs={{0,8},{4,12},{8,16},{12,20},{16,24},{20,28},{1,9},{5,13},{9,17},{1... | collective-permute-start | bytes 442376 | tf_op jit(solution)/shard_map/ppermute | solution.py:479
  54.3 7.0 %collective-permute-start.5 = (bf16[144,512]{1,0:T(8,128)(2,1)S(1)}, bf16[144,512]{1,0:T(8,128)(2,1)S(1)}, u32[]{:S(2)}, u32[]{:S(2)}) collective-permute-start(bf16[144,512]{1,0:T(8,128)(2,1)S(1)} %get-tuple-element.40), channel_id=1, source_target_pairs={{8,0},{12,4},{16,8},{20,12},{24,16},{28,20},{9,1},{13,5},{17,9},{2... | collective-permute-start | bytes 442376 | tf_op jit(solution)/shard_map/ppermute | solution.py:480
  61.5 8.8 %collective-permute-start.6 = (bf16[144,512]{1,0:T(8,128)(2,1)S(1)}, bf16[144,512]{1,0:T(8,128)(2,1)S(1)}, u32[]{:S(2)}, u32[]{:S(2)}) collective-permute-start(bf16[144,512]{1,0:T(8,128)(2,1)S(1)} %get-tuple-element.45), channel_id=1, source_target_pairs={{0,16},{4,20},{8,24},{12,28},{1,17},{5,21},{9,25},{13,29},{2,18},{... | collective-permute-start | bytes 442376 | tf_op jit(solution)/shard_map/ppermute | solution.py:479
  65.5 8.5 %collective-permute-start.7 = (bf16[144,512]{1,0:T(8,128)(2,1)S(1)}, bf16[144,512]{1,0:T(8,128)(2,1)S(1)}, u32[]{:S(2)}, u32[]{:S(2)}) collective-permute-start(bf16[144,512]{1,0:T(8,128)(2,1)S(1)} %get-tuple-element.46), channel_id=1, source_target_pairs={{16,0},{20,4},{24,8},{28,12},{17,1},{21,5},{25,9},{29,13},{18,2},{... | collective-permute-start | bytes 442376 | tf_op jit(solution)/shard_map/ppermute | solution.py:480
  67.4 6.8 %copy-start.2 = (bf16[512,2048]{1,0:T(8,128)(2,1)S(1)}, bf16[512,2048]{1,0:T(8,128)(2,1)}, u32[]{:S(2)}) copy-start(bf16[512,2048]{1,0:T(8,128)(2,1)} %map_ref.1) | copy-start | bytes 6291460
  67.4 6.7 %copy-start.4 = (bf16[512,512]{1,0:T(8,128)(2,1)S(1)}, bf16[512,512]{1,0:T(8,128)(2,1)}, u32[]{:S(2)}) copy-start(bf16[512,512]{1,0:T(8,128)(2,1)} %valve_ref.1) | copy-start | bytes 1572868
  67.4 6.7 %copy-start.8 = (f32[512]{0:T(512)S(1)}, f32[512]{0:T(512)}, u32[]{:S(2)}) copy-start(f32[512]{0:T(512)} %param.31) | copy-start | bytes 6148
  76.9 2.7 %collective-permute-start.8 = (bf16[512,1024]{1,0:T(8,128)(2,1)S(1)}, bf16[512,1024]{1,0:T(8,128)(2,1)S(1)}, u32[]{:S(2)}, u32[]{:S(2)}) collective-permute-start(bf16[512,1024]{1,0:T(8,128)(2,1)S(1)} %get-tuple-element.52), channel_id=1, source_target_pairs={{0,1},{1,0},{2,3},{3,2},{4,5},{5,4},{6,7},{7,6},{8,9},{9,8},{10,11... | collective-permute-start | bytes 3145736 | tf_op jit(solution)/shard_map/ppermute | solution.py:47
  77.0 31.7 %collective-permute-start.14 = (bf16[512,1280]{1,0:T(8,128)(2,1)S(1)}, bf16[512,1280]{1,0:T(8,128)(2,1)S(1)}, u32[]{:S(2)}, u32[]{:S(2)}) collective-permute-start(bf16[512,1280]{1,0:T(8,128)(2,1)S(1)} %collective-permute-done.12.refs_7_), channel_id=1, source_target_pairs={{4,12},{12,20},{20,28},{28,24},{24,16},{16,8},{8,0},{0,4},{5,13},{... | collective-permute-start | bytes 3932168 | tf_op jit(solution)/shard_map/ppermute | solution.py:384
  78.4 31.7 %collective-permute-start.15 = (bf16[512,1280]{1,0:T(8,128)(2,1)S(1)}, bf16[512,1280]{1,0:T(8,128)(2,1)S(1)}, u32[]{:S(2)}, u32[]{:S(2)}) collective-permute-start(bf16[512,1280]{1,0:T(8,128)(2,1)S(1)} %collective-permute-done.13.refs_8_), channel_id=1, source_target_pairs={{12,4},{20,12},{28,20},{24,28},{16,24},{8,16},{0,8},{4,0},{13,5},{... | collective-permute-start | bytes 3932168 | tf_op jit(solution)/shard_map/ppermute | solution.py:384
  79.6 2.0 copy-start.3
  79.6 31.1 %copy-start.10 = (bf16[512,512]{1,0:T(8,128)(2,1)S(1)}, bf16[512,512]{1,0:T(8,128)(2,1)}, u32[]{:S(2)}) copy-start(bf16[512,512]{1,0:T(8,128)(2,1)} %param.20) | copy-start | bytes 1572868
  80.1 30.6 %collective-permute-start.9 = (bf16[512,512]{1,0:T(8,128)(2,1)S(1)}, bf16[512,512]{1,0:T(8,128)(2,1)S(1)}, u32[]{:S(2)}, u32[]{:S(2)}) collective-permute-start(bf16[512,512]{1,0:T(8,128)(2,1)S(1)} %slice.531), channel_id=1, source_target_pairs={{0,2},{1,3},{2,0},{3,1},{4,6},{5,7},{6,4},{7,5},{8,10},{9,11},{10,... | collective-permute-start | bytes 1572872 | tf_op jit(solution)/shard_map/ppermute | solution.py:47
  81.7 41.1 %collective-permute-start.22 = (bf16[1280,256]{1,0:T(8,128)(2,1)S(1)}, bf16[1280,256]{1,0:T(8,128)(2,1)S(1)}, u32[]{:S(2)}, u32[]{:S(2)}) collective-permute-start(bf16[1280,256]{1,0:T(8,128)(2,1)S(1)} %copy-done.3), channel_id=1, source_target_pairs={{4,12},{12,20},{20,28},{28,24},{24,16},{16,8},{8,0},{0,4},{5,13},{... | collective-permute-start | bytes 1966088 | tf_op jit(solution)/shard_map/ppermute | solution.py:384
  83.0 41.1 %collective-permute-start.23 = (bf16[1280,256]{1,0:T(8,128)(2,1)S(1)}, bf16[1280,256]{1,0:T(8,128)(2,1)S(1)}, u32[]{:S(2)}, u32[]{:S(2)}) collective-permute-start(bf16[1280,256]{1,0:T(8,128)(2,1)S(1)} %copy-done.3), channel_id=1, source_target_pairs={{12,4},{20,12},{28,20},{24,28},{16,24},{8,16},{0,8},{4,0},{13,5},{... | collective-permute-start | bytes 1966088 | tf_op jit(solution)/shard_map/ppermute | solution.py:384
  108.7 57.7 %collective-permute-start.16 = (bf16[512,1280]{1,0:T(8,128)(2,1)S(1)}, bf16[512,1280]{1,0:T(8,128)(2,1)S(1)}, u32[]{:S(2)}, u32[]{:S(2)}) collective-permute-start(bf16[512,1280]{1,0:T(8,128)(2,1)S(1)} %collective-permute-done.14.refs_9_), channel_id=1, source_target_pairs={{4,12},{12,20},{20,28},{28,24},{24,16},{16,8},{8,0},{0,4},{5,13},{... | collective-permute-start | bytes 3932168 | tf_op jit(solution)/shard_map/ppermute | solution.py:384
  110.0 57.8 %collective-permute-start.17 = (bf16[512,1280]{1,0:T(8,128)(2,1)S(1)}, bf16[512,1280]{1,0:T(8,128)(2,1)S(1)}, u32[]{:S(2)}, u32[]{:S(2)}) collective-permute-start(bf16[512,1280]{1,0:T(8,128)(2,1)S(1)} %collective-permute-done.15.refs_10_), channel_id=1, source_target_pairs={{12,4},{20,12},{28,20},{24,28},{16,24},{8,16},{0,8},{4,0},{13,5},{... | collective-permute-start | bytes 3932168 | tf_op jit(solution)/shard_map/ppermute | solution.py:384
  111.0 57.6 %copy-start.14 = (f32[3,1280]{1,0:T(4,128)S(1)}, f32[3,1280]{1,0:T(4,128)}, u32[]{:S(2)}) copy-start(f32[3,1280]{1,0:T(4,128)} %param.37) | copy-start | bytes 46084
  111.0 57.6 %copy-start.15 = (f32[3,1280]{1,0:T(4,128)S(1)}, f32[3,1280]{1,0:T(4,128)}, u32[]{:S(2)}) copy-start(f32[3,1280]{1,0:T(4,128)} %param.36) | copy-start | bytes 46084
  111.0 13.8 %collective-permute-start.10 = (bf16[512,512]{1,0:T(8,128)(2,1)S(1)}, bf16[512,512]{1,0:T(8,128)(2,1)S(1)}, u32[]{:S(2)}, u32[]{:S(2)}) collective-permute-start(bf16[512,512]{1,0:T(8,128)(2,1)S(1)} %fusion.9.refs_2_), channel_id=1, source_target_pairs={{0,2},{1,3},{2,0},{3,1},{4,6},{5,7},{6,4},{7,5},{8,10},{9,11},{10,... | collective-permute-start | bytes 1572872 | tf_op jit(solution)/shard_map/ppermute | solution.py:47
  122.7 41.6 %collective-permute-start.24 = (bf16[1280,256]{1,0:T(8,128)(2,1)S(1)}, bf16[1280,256]{1,0:T(8,128)(2,1)S(1)}, u32[]{:S(2)}, u32[]{:S(2)}) collective-permute-start(bf16[1280,256]{1,0:T(8,128)(2,1)S(1)} %collective-permute-done.22.refs_3_), channel_id=1, source_target_pairs={{4,12},{12,20},{20,28},{28,24},{24,16},{16,8},{8,0},{0,4},{5,13},{... | collective-permute-start | bytes 1966088 | tf_op jit(solution)/shard_map/ppermute | solution.py:384
  124.0 41.6 %collective-permute-start.25 = (bf16[1280,256]{1,0:T(8,128)(2,1)S(1)}, bf16[1280,256]{1,0:T(8,128)(2,1)S(1)}, u32[]{:S(2)}, u32[]{:S(2)}) collective-permute-start(bf16[1280,256]{1,0:T(8,128)(2,1)S(1)} %collective-permute-done.23.refs_4_), channel_id=1, source_target_pairs={{12,4},{20,12},{28,20},{24,28},{16,24},{8,16},{0,8},{4,0},{13,5},{... | collective-permute-start | bytes 1966088 | tf_op jit(solution)/shard_map/ppermute | solution.py:384
  124.9 72.4 %copy-start = (bf16[256,1280]{1,0:T(8,128)(2,1)S(1)}, bf16[256,1280]{1,0:T(8,128)(2,1)}, u32[]{:S(2)}) copy-start(bf16[256,1280]{1,0:T(8,128)(2,1)} %refs_5_.1) | copy-start | bytes 1966084
  124.9 72.4 %copy-start.1 = (bf16[256,1280]{1,0:T(8,128)(2,1)S(1)}, bf16[256,1280]{1,0:T(8,128)(2,1)}, u32[]{:S(2)}) copy-start(bf16[256,1280]{1,0:T(8,128)(2,1)} %refs_6_.1) | copy-start | bytes 1966084
  124.9 72.4 %copy-start.7 = (f32[2048]{0:T(1024)S(1)}, f32[2048]{0:T(1024)}, u32[]{:S(2)}) copy-start(f32[2048]{0:T(1024)} %param.33) | copy-start | bytes 24580
  124.9 59.2 %collective-permute-start.11 = (bf16[512,1024]{1,0:T(8,128)(2,1)S(1)}, bf16[512,1024]{1,0:T(8,128)(2,1)S(1)}, u32[]{:S(2)}, u32[]{:S(2)}) collective-permute-start(bf16[512,1024]{1,0:T(8,128)(2,1)S(1)} %pad_maximum_fusion), channel_id=1, source_target_pairs={{0,1},{1,0},{2,3},{3,2},{4,5},{5,4},{6,7},{7,6},{8,9},{9,8},{10,11... | collective-permute-start | bytes 3145736 | tf_op jit(solution)/shard_map/ppermute | solution.py:47
  164.3 17.6 %collective-permute-start.26 = (bf16[1280,256]{1,0:T(8,128)(2,1)S(1)}, bf16[1280,256]{1,0:T(8,128)(2,1)S(1)}, u32[]{:S(2)}, u32[]{:S(2)}) collective-permute-start(bf16[1280,256]{1,0:T(8,128)(2,1)S(1)} %collective-permute-done.24.refs_5_), channel_id=1, source_target_pairs={{4,12},{12,20},{20,28},{28,24},{24,16},{16,8},{8,0},{0,4},{5,13},{... | collective-permute-start | bytes 1966088 | tf_op jit(solution)/shard_map/ppermute | solution.py:384
  165.7 17.7 %collective-permute-start.27 = (bf16[1280,256]{1,0:T(8,128)(2,1)S(1)}, bf16[1280,256]{1,0:T(8,128)(2,1)S(1)}, u32[]{:S(2)}, u32[]{:S(2)}) collective-permute-start(bf16[1280,256]{1,0:T(8,128)(2,1)S(1)} %collective-permute-done.25.refs_6_), channel_id=1, source_target_pairs={{12,4},{20,12},{28,20},{24,28},{16,24},{8,16},{0,8},{4,0},{13,5},{... | collective-permute-start | bytes 1966088 | tf_op jit(solution)/shard_map/ppermute | solution.py:384
  166.4 29.6 %collective-permute-start.18 = (bf16[256,1280]{1,0:T(8,128)(2,1)S(1)}, bf16[256,1280]{1,0:T(8,128)(2,1)S(1)}, u32[]{:S(2)}, u32[]{:S(2)}) collective-permute-start(bf16[256,1280]{1,0:T(8,128)(2,1)S(1)} %slice.329), channel_id=1, source_target_pairs={{4,12},{12,20},{20,28},{28,24},{24,16},{16,8},{8,0},{0,4},{5,13},{... | collective-permute-start | bytes 1966088 | tf_op jit(solution)/shard_map/ppermute | solution.py:384
  167.8 29.5 %collective-permute-start.19 = (bf16[256,1280]{1,0:T(8,128)(2,1)S(1)}, bf16[256,1280]{1,0:T(8,128)(2,1)S(1)}, u32[]{:S(2)}, u32[]{:S(2)}) collective-permute-start(bf16[256,1280]{1,0:T(8,128)(2,1)S(1)} %slice.330), channel_id=1, source_target_pairs={{12,4},{20,12},{28,20},{24,28},{16,24},{8,16},{0,8},{4,0},{13,5},{... | collective-permute-start | bytes 1966088 | tf_op jit(solution)/shard_map/ppermute | solution.py:384
  182.0 33.4 %collective-permute-start.28 = (bf16[640,256]{1,0:T(8,128)(2,1)S(1)}, bf16[640,256]{1,0:T(8,128)(2,1)S(1)}, u32[]{:S(2)}, u32[]{:S(2)}) collective-permute-start(bf16[640,256]{1,0:T(8,128)(2,1)S(1)} %slice.341), channel_id=1, source_target_pairs={{4,12},{12,20},{20,28},{28,24},{24,16},{16,8},{8,0},{0,4},{5,13},{... | collective-permute-start | bytes 983048 | tf_op jit(solution)/shard_map/ppermute | solution.py:384
  183.4 32.0 %collective-permute-start.29 = (bf16[640,256]{1,0:T(8,128)(2,1)S(1)}, bf16[640,256]{1,0:T(8,128)(2,1)S(1)}, u32[]{:S(2)}, u32[]{:S(2)}) collective-permute-start(bf16[640,256]{1,0:T(8,128)(2,1)S(1)} %slice.342), channel_id=1, source_target_pairs={{12,4},{20,12},{28,20},{24,28},{16,24},{8,16},{0,8},{4,0},{13,5},{... | collective-permute-start | bytes 983048 | tf_op jit(solution)/shard_map/ppermute | solution.py:384
  204.9 3.6 %collective-permute-start.20 = (bf16[1,2560]{1,0:T(2,128)(2,1)S(1)}, bf16[1,2560]{1,0:T(2,128)(2,1)S(1)}, u32[]{:S(2)}, u32[]{:S(2)}) collective-permute-start(bf16[1,2560]{1,0:T(2,128)(2,1)S(1)} %pad_maximum_fusion.1), channel_id=1, source_target_pairs={{0,4},{4,8},{8,12},{12,16},{16,20},{20,24},{24,28},{1,5},{5,9},{9,... | collective-permute-start | bytes 15368 | tf_op jit(solution)/shard_map/ppermute | solution.py:344
  207.1 5.6 %collective-permute-start.21 = (bf16[1,2560]{1,0:T(2,128)(2,1)S(1)}, bf16[1,2560]{1,0:T(2,128)(2,1)S(1)}, u32[]{:S(2)}, u32[]{:S(2)}) collective-permute-start(bf16[1,2560]{1,0:T(2,128)(2,1)S(1)} %pad_maximum_fusion.2), channel_id=1, source_target_pairs={{4,0},{8,4},{12,8},{16,12},{20,16},{24,20},{28,24},{5,1},{9,5},{13... | collective-permute-start | bytes 15368 | tf_op jit(solution)/shard_map/ppermute | solution.py:345
  222.9 2.7 %collective-permute-start.30 = (bf16[512,1024]{1,0:T(8,128)(2,1)S(1)}, bf16[512,1024]{1,0:T(8,128)(2,1)S(1)}, u32[]{:S(2)}, u32[]{:S(2)}) collective-permute-start(bf16[512,1024]{1,0:T(8,128)(2,1)S(1)} %get-tuple-element.56), channel_id=1, source_target_pairs={{0,1},{1,0},{2,3},{3,2},{4,5},{5,4},{6,7},{7,6},{8,9},{9,8},{10,11... | collective-permute-start | bytes 3145736 | tf_op jit(solution)/shard_map/ppermute | solution.py:47
  226.1 14.0 %collective-permute-start.31 = (bf16[512,512]{1,0:T(8,128)(2,1)S(1)}, bf16[512,512]{1,0:T(8,128)(2,1)S(1)}, u32[]{:S(2)}, u32[]{:S(2)}) collective-permute-start(bf16[512,512]{1,0:T(8,128)(2,1)S(1)} %slice.530), channel_id=1, source_target_pairs={{0,2},{1,3},{2,0},{3,1},{4,6},{5,7},{6,4},{7,5},{8,10},{9,11},{10,... | collective-permute-start | bytes 1572872 | tf_op jit(solution)/shard_map/ppermute | solution.py:47
where the time goes:
time: 242 us; the launch traced here: 241 us
  waiting for transfers between devices  158 us (65%)
  starting transfers between devices  45.7 us (19%)
  Pallas kernels  22.6 us (9%)
  local copies, waits for them, and re-layouts  7.37 us (3%)
  other arithmetic  7.29 us (3%)
    ppermute x16, waiting for transfers between devices, send_on(): return lax.ppermute(array, 'sp', pairs)  101 us
    pallas_call x9, Pallas kernels, call(): pl.pallas_call(kernel, out_shape=[jax.ShapeDtypeStruct(shape, kind) for s...  22.6 us
    ppermute x2, waiting for transfers between devices, edges(): low = lax.ppermute(last, 'sp', forward)  20.1 us
    ppermute x16, starting transfers between devices, send_on(): return lax.ppermute(array, 'sp', pairs)  17.5 us
    ppermute x6, waiting for transfers between devices, swap(): lax.ppermute(array, 'tp', [(i, i ^ 1 << bit) for i in range(self.count)])  15.7 us
    ppermute x3, waiting for transfers between devices, shards(): got_b = lax.ppermute(send_b, 'sp', [(b, a) for a, b in forward])  12.8 us
    ppermute x3, starting transfers between devices, shards(): got_f = lax.ppermute(send_f, 'sp', forward)  10.8 us
    ppermute x2, waiting for transfers between devices, edges(): high = lax.ppermute(first, 'sp', backward)  6.18 us
  transfers between devices with their start and end apart: 32, of which 17 were waited for; matrix products, arithmetic and copies ran while one was open for 4% of the time, Pallas kernels for 6%

commit v1 on v0

--- a/solution.py
+++ b/solution.py
@@ -12,6 +12,7 @@
 STATE = 128
 EPSILON = 1e-06
 TAIL = 16
+LIMIT = 16
 
 
 def ring_cycle(mesh):
@@ -122,7 +123,7 @@
     return jnp.concatenate([state, tail], axis=0).astype(jnp.bfloat16)
 
 
-def state_kernel(values_ref, inputs_ref, scale_ref, last_ref, window_ref, decay_ref, send_f_ref, send_b_ref):
+def state_kernel(values_ref, inputs_ref, scale_ref, last_ref, window_ref, send_f_ref, send_b_ref):
     groups = inputs_ref.shape[1] // STATE
     wide = values_ref.shape[1] // groups
     values = values_ref[...].astype(jnp.float32)
@@ -140,15 +141,15 @@
             ],
             axis=1,
         )
-        window_ref[way] = state
-        decay_ref[way] = last_ref[way]
+        window_ref[way, :STATE] = state
+        window_ref[way, STATE:] = last_ref[way]
         send_ref[...] = message(state, last_ref[way, 0:1])
 
 
 def link_kernel(first, final, *refs):
-    got_refs, window_ref, decay_ref = refs[:2], refs[2], refs[3]
-    before_ref, before_decay_ref = (None, None) if first else refs[4:6]
-    outs = refs[4:] if first else refs[6:]
+    got_refs, refs = refs[:2], list(refs[2:])
+    before_ref = None if first else refs.pop(0)
+    window_ref = None if final else refs.pop(0)
     for way in range(2):
         got = got_refs[way][:STATE].astype(jnp.float32)
         got_decay = got_refs[way][STATE : STATE + 1].astype(jnp.float32) + got_refs[way][
@@ -156,19 +157,19 @@
         ].astype(jnp.float32)
         before, before_decay = got, got_decay
         if not first:
-            before = got * before_decay_ref[way, 0:1] + before_ref[way]
-            before_decay = got_decay * before_decay_ref[way, 0:1]
+            held_decay = before_ref[way, STATE : STATE + 1]
+            before = got * held_decay + before_ref[way, :STATE]
+            before_decay = got_decay * held_decay
         if final:
-            outs[0][way] = before.astype(jnp.bfloat16)
+            refs[0][way] = before.astype(jnp.bfloat16)
             continue
-        decay = decay_ref[way, 0:1]
-        state = got * decay + window_ref[way]
+        decay = window_ref[way, STATE : STATE + 1]
+        state = got * decay + window_ref[way, :STATE]
         decay = decay * got_decay
-        outs[0][way] = before
-        outs[1][way] = jnp.broadcast_to(before_decay, outs[1].shape[1:])
-        outs[2][way] = state
-        outs[3][way] = jnp.broadcast_to(decay, outs[3].shape[1:])
-        outs[4 + way][...] = message(state, decay)
+        for ref, value, factor in ((refs[0], before, before_decay), (refs[1], state, decay)):
+            ref[way, :STATE] = value
+            ref[way, STATE:] = jnp.broadcast_to(factor, (8, factor.shape[1]))
+        refs[2 + way][...] = message(state, decay)
 
 
 def within_kernel(values_ref, inputs_ref, readout_ref, rows_ref, cols_ref, out_ref):
@@ -291,43 +292,57 @@
         for j in range(columns // tile):
             at = slice(j * tile, (j + 1) * tile)
             total = None
-            for array, first, source in plan[which]:
+            for n, source in enumerate(plan[which]):
                 term = jnp.dot(
                     rows_scr[info_ref[source] // chunk],
-                    arrays[array][first : first + chunk, at],
+                    arrays[which * len(plan[0]) + n][:, at],
                     preferred_element_type=jnp.float32,
                 )
                 total = term if total is None else total + term
             outs[which][:, at] = total.astype(jnp.bfloat16)
 
 
-def down_kernel(sizes, plan, n_arrays, *refs):
+def down_kernel(sizes, plan, blank, n_arrays, *refs):
     info_ref, hidden_ref = refs[:2]
     arrays = refs[2 : 2 + n_arrays]
-    send_ref, keep_ref = refs[2 + n_arrays :]
-    half = send_ref.shape[1]
-    for source, parts in enumerate(plan):
-        term = None
-        for array, row in parts:
-            depth, chunk = arrays[array].shape
-            part = jnp.dot(
-                hidden_ref[:, row : row + depth], arrays[array][...], preferred_element_type=jnp.float32
-            )
-            term = part if term is None else term + part
-        term = term.astype(jnp.bfloat16)
-        if len(plan) == 1:
-            send_ref[...] = term[:, :half]
-            keep_ref[...] = term[:, half:]
-            continue
+    held = refs[2 + n_arrays : -2]
+    outs = refs[-2:]
+    half = outs[0].shape[1]
+    for held_ref, out_ref in zip(held, outs):
+        out_ref[...] = held_ref[...]
+
+    def put(source, term):
         at = info_ref[sizes[0] + source]
-
-        @pl.when(at < half)
-        def _():
-            send_ref[:, pl.ds(pl.multiple_of(at, chunk), chunk)] = term
-
-        @pl.when(at >= half)
-        def _():
-            keep_ref[:, pl.ds(pl.multiple_of(at - half, chunk), chunk)] = term
+        for side in range(2):
+
+            @pl.when((at >= half) if side else (at < half))
+            def _():
+                columns = pl.ds(pl.multiple_of(at - side * half, term.shape[1]), term.shape[1])
+                outs[side][:, columns] = term
+
+    for source, parts in plan:
+        term = down_term(hidden_ref, [(arrays[array], row) for array, row in parts])
+        if term.shape[1] == 2 * half:
+            outs[0][...] = term[:, :half]
+            outs[1][...] = term[:, half:]
+        else:
+            put(source, term)
+    if blank is not None:
+        put(blank, jnp.zeros_like(term))
+
+
+def down_term(hidden_ref, parts):
+    term = None
+    for array, row in parts:
+        part = jnp.dot(
+            hidden_ref[:, row : row + array.shape[0]], array[...], preferred_element_type=jnp.float32
+        )
+        term = part if term is None else term + part
+    return term.astype(jnp.bfloat16)
+
+
+def far_kernel(hidden_ref, top_ref, bottom_ref, out_ref):
+    out_ref[...] = down_term(hidden_ref, [(top_ref, 0), (bottom_ref, top_ref.shape[0])])
 
 
 def conv_rows(padded, kernel, length):
@@ -353,7 +368,7 @@
         out_shape=[jax.ShapeDtypeStruct(shape, kind) for shape, kind in outs],
         in_specs=[pl.BlockSpec(memory_space=space) for space in spaces],
         scratch_shapes=list(scratch),
-        compiler_params=pltpu.CompilerParams(vmem_limit_bytes=32 * 1024 * 1024),
+        compiler_params=pltpu.CompilerParams(vmem_limit_bytes=LIMIT * 1024 * 1024),
     )(*args)
 
 
@@ -383,17 +398,23 @@
     def send_on(array, pairs):
         return lax.ppermute(array, "sp", pairs)
 
-    def ring(join, half):
+    def ring(own, far_ways):
         out = []
-        going, coming = join, join
+        going, coming = own, own
         for step in range(1, (sp_count - 1) // 2 + 1):
             going = send_on(going, right)
             coming = send_on(coming, left)
-            out += [(step, going, None), (-step, coming, None)]
+            out += [(step, going, 0), (-step, coming, 0)]
         if sp_count % 2 == 0:
             far = sp_count // 2
-            out.append((far, send_on(going[:half], right), 0))
-            out.append((far, send_on(coming[half:], left), 1))
+            half = own.shape[0] // 2
+            if far_ways == "f":
+                out.append((far, send_on(going, right), 0))
+            elif far_ways == "b":
+                out.append((far, send_on(coming, left), 0))
+            else:
+                out.append((far, send_on(going[:half], right), 0))
+                out.append((far, send_on(coming[half:], left), half))
         return out
 
     def shards(
@@ -434,11 +455,8 @@
         full = own_cols * tp_count
         hidden_cols = dense_valve_map.shape[1]
         chunk = dense_valve_map.shape[0]
-        middle_row = hidden_cols // 2
-        up_ring = [(0, dense_valve_map, 0), (0, dense_payload_map, 1)]
-        up_ring += ring(jnp.concatenate([dense_valve_map, dense_payload_map], axis=0), chunk)
-        down_ring = [(0, dense_contract_map, None)] + ring(dense_contract_map, middle_row)
-
+        up_rings = [[(0, own, 0)] + ring(own, way) for own, way in ((dense_valve_map, "f"), (dense_payload_map, "b"))]
+        down_ring = [(0, dense_contract_map, 0)] + ring(dense_contract_map, "fb")
         info = jnp.asarray(table(chunk, own_cols))[lax.axis_index("sp") * tp_count + me]
 
         rows, cols, scale, last = call(
@@ -463,11 +481,10 @@
         values = mixed(projected_heads_payload, lows[0], highs[0], payload_conv_weights)
         inputs = mixed(cluster_ingests, lows[1], highs[1], ingest_conv_weights)
         readout = mixed(cluster_observers, lows[2], highs[2], observer_conv_weights)
-        wide_state = ((2, STATE, channels), jnp.float32)
-        wide_decay = ((2, 8, channels), jnp.float32)
+        wide_state = ((2, STATE + 8, channels), jnp.float32)
         sent = ((STATE + TAIL, channels), jnp.bfloat16)
-        window, decay, send_f, send_b = call(
-            state_kernel, [wide_state, wide_decay, sent, sent], values, inputs, scale, last
+        window, send_f, send_b = call(
+            state_kernel, [wide_state, sent, sent], values, inputs, scale, last
         )
         (within,) = call(
             within_kernel, [((length, channels), jnp.float32)], values, inputs, readout, rows, cols
@@ -481,14 +498,19 @@
             final = 2 * offset >= sp_count
             outs = [((2, STATE, channels), jnp.bfloat16)]
             if not final:
-                outs = [wide_state, wide_decay, wide_state, wide_decay, sent, sent]
+                outs = [wide_state, wide_state, sent, sent]
             result = call(
-                functools.partial(link_kernel, offset == 1, final), outs, got_f, got_b, window, decay, *before
+                functools.partial(link_kernel, offset == 1, final),
+                outs,
+                got_f,
+                got_b,
+                *before,
+                *(() if final else (window,)),
             )
             if final:
                 states = result[0]
             else:
-                before, (window, decay, send_f, send_b) = tuple(result[:2]), result[2:]
+                before, (window, send_f, send_b) = (result[0],), result[1:]
             offset *= 2
 
         half_full = full // 2
@@ -509,11 +531,8 @@
         middle = (skip_trunk_vector.astype(jnp.float32) + projected).astype(jnp.bfloat16)
         pieces = tp.gather(middle)
 
-        arrays, plan = [], ([], [])
-        for steps, array, part in up_ring:
-            for which in (0, 1) if part is None else (part,):
-                plan[which].append((len(arrays), which * chunk if part is None else 0, steps % sp_count))
-            arrays.append(array)
+        arrays = [array for entries in up_rings for _, array, _ in entries]
+        plan = [[steps % sp_count for steps, _, _ in entries] for entries in up_rings]
         gate_rows, value_rows = call(
             functools.partial(up_kernel, (sp_count, tp_count), plan, (len(pieces), len(arrays))),
             [((length, hidden_cols), jnp.bfloat16)] * 2,
@@ -537,28 +556,48 @@
         value = smooth(value_rows, low[:, hidden_cols:], high[:, hidden_cols:], payload_series_smoother)
         hidden = (jax.nn.silu(gate) * value).astype(jnp.bfloat16)
 
-        arrays = []
-        if chunk % 128 == 0:
-            plan = [[] for _ in range(sp_count)]
-            for steps, array, part in down_ring:
-                plan[steps % sp_count].append((len(arrays), middle_row if part == 1 else 0))
-                arrays.append(array)
-        else:
+        def down(plan, blank, arrays, held=()):
+            return call(
+                functools.partial(down_kernel, (sp_count, tp_count), plan, blank, len(arrays)),
+                [((length, half_full), jnp.bfloat16)] * 2,
+                info,
+                hidden,
+                *arrays,
+                *held,
+                scalars=1,
+            )
+
+        if chunk % 128:
             whole = jnp.zeros((hidden_cols, full), jnp.bfloat16)
-            for steps, array, part in down_ring:
-                corner = (middle_row if part == 1 else 0, info[sp_count + steps % sp_count])
-                whole = lax.dynamic_update_slice(whole, array, corner)
-            arrays, plan = [whole], [[(0, 0)]]
-        send, keep = call(
-            functools.partial(down_kernel, (sp_count, tp_count), plan, len(arrays)),
-            [((length, half_full), jnp.bfloat16)] * 2,
-            info,
-            hidden,
-            *arrays,
-            scalars=1,
-        )
+            for steps, array, first in down_ring:
+                whole = lax.dynamic_update_slice(whole, array, (first, info[sp_count + steps % sp_count]))
+            send, keep = down([(0, [(0, 0)])], None, [whole])
+            down_sum = tp.reduce_scatter(send, keep)
+            return (middle.astype(jnp.float32) + down_sum).astype(jnp.bfloat16)
+
+        far = sp_count // 2
+        near_chunks = [(steps % sp_count, array) for steps, array, _ in down_ring if abs(steps) < far]
+        early, late = near_chunks[:-2], near_chunks[-2:]
+        held = down([(slot, [(n, 0)]) for n, (slot, _) in enumerate(early)], None, [a for _, a in early])
+        send, keep = down([(slot, [(n, 0)]) for n, (slot, _) in enumerate(late)], far, [a for _, a in late], held)
         down_sum = tp.reduce_scatter(send, keep)
-        return (middle.astype(jnp.float32) + down_sum).astype(jnp.bfloat16)
+        (part,) = call(
+            far_kernel, [((length, chunk), jnp.bfloat16)], hidden, *(a for _, a, _ in down_ring[-2:])
+        )
+        for bit in range(tp.bits):
+            pairs = []
+            for s in range(sp_count):
+                owner = cycle[(place[s] - far) % sp_count] * chunk // own_cols
+                for t in range(tp_count):
+                    apart = t ^ owner
+                    if apart >> bit & 1 and apart % (1 << bit) == 0:
+                        pairs.append((s * tp_count + t, s * tp_count + (t ^ (1 << bit))))
+            received = lax.ppermute(part.astype(jnp.bfloat16), ("sp", "tp"), pairs)
+            part = part.astype(jnp.float32) + received.astype(jnp.float32)
+        at = info[sp_count + far] - (tp_count - 1) * own_cols
+        spots = range(0, own_cols, chunk)
+        placed = jnp.concatenate([jnp.where(at == spot, part, 0.0) for spot in spots], axis=1)
+        return (middle.astype(jnp.float32) + down_sum + placed).astype(jnp.bfloat16)
 
     return jax.shard_map(
         shards,

time: 242 us -> 251 us (1.037); the launches traced: 241 us -> 247 us
  starting transfers between devices: 45.7 us -> 56.8 us
  waiting for transfers between devices: 158 us -> 149 us
    ppermute x2, waiting for transfers between devices: 20.1 us -> 0.71 us  [edges(): low = lax.ppermute(last, 'sp', forward)]
    ppermute x16 -> x22, waiting for transfers between devices: 101 us -> 116 us  [send_on(): return lax.ppermute(array, 'sp', pairs)]
    ppermute x16 -> x22, starting transfers between devices: 17.5 us -> 23 us  [send_on(): return lax.ppermute(array, 'sp', pairs)]
    ppermute x6, waiting for transfers between devices: 15.7 us -> 10.9 us  [swap(): lax.ppermute(array, 'tp', [(i, i ^ 1 << bit) for i in range(self.count)])]
    ppermute x3, starting transfers between devices: 10.8 us -> 13.8 us  [shards(): got_f = lax.ppermute(send_f, 'sp', forward)]
    pallas_call x9 -> x11, Pallas kernels: 22.6 us -> 23.2 us  [call(): pl.pallas_call(kernel, out_shape=[jax.ShapeDtypeStruct(shape, kind) for s...]
  transfers between devices with their start and end apart: 32 -> 40, of which waited for: 17 -> 25; matrix products, arithmetic and copies ran while one was open for 4% -> 4% of each run, Pallas kernels for 6% -> 7%
where the time goes in v1:
time: 251 us; the launch traced here: 247 us
  waiting for transfers between devices  149 us (59%)
  starting transfers between devices  56.8 us (23%)
  Pallas kernels  23.2 us (9%)
  other arithmetic  9.58 us (4%)
  local copies, waits for them, and re-layouts  7.39 us (3%)
    ppermute x22, waiting for transfers between devices, send_on(): return lax.ppermute(array, 'sp', pairs)  116 us
    pallas_call x11, Pallas kernels, call(): pl.pallas_call(kernel, out_shape=[jax.ShapeDtypeStruct(shape, kind) for s...  23.2 us
    ppermute x22, starting transfers between devices, send_on(): return lax.ppermute(array, 'sp', pairs)  23 us
    ppermute x3, starting transfers between devices, shards(): got_f = lax.ppermute(send_f, 'sp', forward)  13.8 us
    ppermute x3, waiting for transfers between devices, shards(): got_b = lax.ppermute(send_b, 'sp', [(b, a) for a, b in forward])  13.6 us
    ppermute x6, waiting for transfers between devices, swap(): lax.ppermute(array, 'tp', [(i, i ^ 1 << bit) for i in range(self.count)])  10.9 us
    ppermute x2, starting transfers between devices, edges(): low = lax.ppermute(last, 'sp', forward)  6.76 us
  transfers between devices with their start and end apart: 40, of which 25 were waited for; matrix products, arithmetic and copies ran while one was open for 4% of the time, Pallas kernels for 7%

profile of v1, /device:TPU:0, one launch (start us, length us, event | category | flops | bytes accessed | tf_op | source)
XLA Modules:
  0.0 247.4 jit_solution(2258794618667737249)
XLA Ops:
  0.0 0.7 fusion.35
  0.7 0.7 fusion.36
  1.5 4.9 %collective-permute-start = (bf16[3,1024]{1,0:T(4,128)(2,1)S(1)}, bf16[3,1024]{1,0:T(4,128)(2,1)S(1)}, u32[]{:S(2)}, u32[]{:S(2)}) collective-permute-start(bf16[3,1024]{1,0:T(4,128)(2,1)S(1)} %pad_maximum_fusion.3), channel_id=1, source_target_pairs={{0,4},{4,8},{8,12},{12,16},{16,20},{20,24},{24,28},{1,5},{5,9},{9,... | collective-permute-start | bytes 18440 | tf_op jit(solution)/shard_map/ppermute | solution.py:359
  6.4 1.3 collective-permute-start.1
  7.7 1.0 fusion.38
  8.7 1.0 fusion.44
  9.7 0.8 copy.21
  10.4 0.8 copy-done.5
  11.2 0.8 copy-done.6
  11.9 1.2 shard_map.190
  13.1 1.0 maximum_convert_fusion.3
  14.2 1.2 maximum_convert_fusion.2
  15.9 1.1 multiply_convert_fusion.values_ref
  17.4 4.6 %collective-permute-start.2 = (bf16[144,512]{1,0:T(8,128)(2,1)S(1)}, bf16[144,512]{1,0:T(8,128)(2,1)S(1)}, u32[]{:S(2)}, u32[]{:S(2)}) collective-permute-start(bf16[144,512]{1,0:T(8,128)(2,1)S(1)} %get-tuple-element.31), channel_id=1, source_target_pairs={{0,4},{4,8},{8,12},{12,16},{16,20},{20,24},{24,28},{1,5},{5,9},{9,... | collective-permute-start | bytes 442376 | tf_op jit(solution)/shard_map/ppermute | solution.py:496
  22.0 1.3 collective-permute-start.3
  23.3 1.3 collective-permute-done.2.refs_0_
  24.6 4.8 %collective-permute-done.3.refs_1_ = bf16[144,512]{1,0:T(8,128)(2,1)S(1)} collective-permute-done((bf16[144,512]{1,0:T(8,128)(2,1)S(1)}, bf16[144,512]{1,0:T(8,128)(2,1)S(1)}, u32[]{:S(2)}, u32[]{:S(2)}) %collective-permute-start.3) | collective-permute-done | bytes 147488 | tf_op jit(solution)/shard_map/ppermute | solution.py:497
  29.6 4.6 %collective-permute-start.4 = (bf16[144,512]{1,0:T(8,128)(2,1)S(1)}, bf16[144,512]{1,0:T(8,128)(2,1)S(1)}, u32[]{:S(2)}, u32[]{:S(2)}) collective-permute-start(bf16[144,512]{1,0:T(8,128)(2,1)S(1)} %get-tuple-element.34), channel_id=1, source_target_pairs={{0,8},{4,12},{8,16},{12,20},{16,24},{20,28},{1,9},{5,13},{9,17},{1... | collective-permute-start | bytes 442376 | tf_op jit(solution)/shard_map/ppermute | solution.py:496
  34.2 1.3 collective-permute-start.5
  36.2 0.8 collective-permute-done.4.refs_0_
  37.1 4.1 %collective-permute-done.5.refs_1_ = bf16[144,512]{1,0:T(8,128)(2,1)S(1)} collective-permute-done((bf16[144,512]{1,0:T(8,128)(2,1)S(1)}, bf16[144,512]{1,0:T(8,128)(2,1)S(1)}, u32[]{:S(2)}, u32[]{:S(2)}) %collective-permute-start.5) | collective-permute-done | bytes 147488 | tf_op jit(solution)/shard_map/ppermute | solution.py:497
  41.2 0.9 shard_map.194
  42.1 4.6 %collective-permute-start.6 = (bf16[144,512]{1,0:T(8,128)(2,1)S(1)}, bf16[144,512]{1,0:T(8,128)(2,1)S(1)}, u32[]{:S(2)}, u32[]{:S(2)}) collective-permute-start(bf16[144,512]{1,0:T(8,128)(2,1)S(1)} %get-tuple-element.38), channel_id=1, source_target_pairs={{0,16},{4,20},{8,24},{12,28},{1,17},{5,21},{9,25},{13,29},{2,18},{... | collective-permute-start | bytes 442376 | tf_op jit(solution)/shard_map/ppermute | solution.py:496
  46.8 1.3 collective-permute-start.7
  48.7 2.7 %shard_map.191.within_ref = f32[512,512]{1,0:T(8,128)S(1)} custom-call(bf16[512,512]{1,0:T(8,128)(2,1)S(1)} %multiply_convert_fusion.values_ref, bf16[512,256]{1,0:T(8,128)(2,1)S(1)} %multiply_convert_fusion.2.inputs_ref, bf16[512,256]{1,0:T(8,128)(2,1)S(1)} %multiply_convert_fusion.1.readout_ref, f32[3,8,512]{2,1,0:T(8,128)S(1)} %get-tuple-element.27.rows_ref, ...), custom_call_target="tpu_custom_call" | custom-call | tf_op jit(solution)/shard_map/pallas_call | solution.py:366
  51.4 4.6 %collective-permute-done.7.refs_1_ = bf16[144,512]{1,0:T(8,128)(2,1)S(1)} collective-permute-done((bf16[144,512]{1,0:T(8,128)(2,1)S(1)}, bf16[144,512]{1,0:T(8,128)(2,1)S(1)}, u32[]{:S(2)}, u32[]{:S(2)}) %collective-permute-start.7) | collective-permute-done | bytes 147488 | tf_op jit(solution)/shard_map/ppermute | solution.py:497
  56.1 2.8 %shard_map.196 = (bf16[512,1024]{1,0:T(8,128)(2,1)S(1)}, bf16[512,1024]{1,0:T(8,128)(2,1)S(1)}) custom-call(s32[24]{0:T(128)S(1)} %get-tuple-element.68.info_ref.refs_0_, f32[512,512]{1,0:T(8,128)S(1)} %shard_map.191.within_ref, bf16[512,256]{1,0:T(8,128)(2,1)S(1)} %multiply_convert_fusion.1.readout_ref, f32[2,512,8]{2,1,0:T(8,128)S(1)} %get-tuple-element.28.cols_ref, ...), custom_call_target="tpu_custom_call" | custom-call | tf_op jit(solution)/shard_map/pallas_call | solution.py:366
  59.1 2.0 collective-permute-start.20
  61.1 2.0 collective-permute-start.19
  63.6 1.5 collective-permute-start.9
  65.2 11.5 %collective-permute-done.12.refs_6_ = bf16[256,1280]{1,0:T(8,128)(2,1)S(1)} collective-permute-done((bf16[256,1280]{1,0:T(8,128)(2,1)S(1)}, bf16[256,1280]{1,0:T(8,128)(2,1)S(1)}, u32[]{:S(2)}, u32[]{:S(2)}) %collective-permute-start.12) | collective-permute-done | bytes 655392 | tf_op jit(solution)/shard_map/ppermute | solution.py:399
  76.7 2.0 collective-permute-start.31
  78.7 12.1 %collective-permute-done.13.refs_7_ = bf16[256,1280]{1,0:T(8,128)(2,1)S(1)} collective-permute-done((bf16[256,1280]{1,0:T(8,128)(2,1)S(1)}, bf16[256,1280]{1,0:T(8,128)(2,1)S(1)}, u32[]{:S(2)}, u32[]{:S(2)}) %collective-permute-start.13) | collective-permute-done | bytes 655392 | tf_op jit(solution)/shard_map/ppermute | solution.py:399
  90.8 2.0 collective-permute-start.22
  92.8 2.0 collective-permute-start.15
  95.0 9.8 %collective-permute-done.28.refs_3_ = bf16[1280,256]{1,0:T(8,128)(2,1)S(1)} collective-permute-done((bf16[1280,256]{1,0:T(8,128)(2,1)S(1)}, bf16[1280,256]{1,0:T(8,128)(2,1)S(1)}, u32[]{:S(2)}, u32[]{:S(2)}) %collective-permute-start.28) | collective-permute-done | bytes 655392 | tf_op jit(solution)/shard_map/ppermute | solution.py:399
  104.7 1.5 collective-permute-start.10
  106.2 12.6 %collective-permute-done.14.refs_8_ = bf16[256,1280]{1,0:T(8,128)(2,1)S(1)} collective-permute-done((bf16[256,1280]{1,0:T(8,128)(2,1)S(1)}, bf16[256,1280]{1,0:T(8,128)(2,1)S(1)}, u32[]{:S(2)}, u32[]{:S(2)}) %collective-permute-start.14) | collective-permute-done | bytes 655392 | tf_op jit(solution)/shard_map/ppermute | solution.py:399
  118.9 2.0 collective-permute-start.32
  120.8 12.1 %collective-permute-done.15.refs_9_ = bf16[256,1280]{1,0:T(8,128)(2,1)S(1)} collective-permute-done((bf16[256,1280]{1,0:T(8,128)(2,1)S(1)}, bf16[256,1280]{1,0:T(8,128)(2,1)S(1)}, u32[]{:S(2)}, u32[]{:S(2)}) %collective-permute-start.15) | collective-permute-done | bytes 655392 | tf_op jit(solution)/shard_map/ppermute | solution.py:399
  132.9 2.0 collective-permute-start.24
  135.2 11.7 %collective-permute-done.29.refs_5_ = bf16[1280,256]{1,0:T(8,128)(2,1)S(1)} collective-permute-done((bf16[1280,256]{1,0:T(8,128)(2,1)S(1)}, bf16[1280,256]{1,0:T(8,128)(2,1)S(1)}, u32[]{:S(2)}, u32[]{:S(2)}) %collective-permute-start.29) | collective-permute-done | bytes 655392 | tf_op jit(solution)/shard_map/ppermute | solution.py:399
  146.9 2.0 collective-permute-start.23
  148.9 12.0 %collective-permute-done.16.refs_10_ = bf16[256,1280]{1,0:T(8,128)(2,1)S(1)} collective-permute-done((bf16[256,1280]{1,0:T(8,128)(2,1)S(1)}, bf16[256,1280]{1,0:T(8,128)(2,1)S(1)}, u32[]{:S(2)}, u32[]{:S(2)}) %collective-permute-start.16) | collective-permute-done | bytes 655392 | tf_op jit(solution)/shard_map/ppermute | solution.py:399
  161.0 2.0 collective-permute-start.25
  163.0 12.0 %collective-permute-done.17.refs_11_ = bf16[256,1280]{1,0:T(8,128)(2,1)S(1)} collective-permute-done((bf16[256,1280]{1,0:T(8,128)(2,1)S(1)}, bf16[256,1280]{1,0:T(8,128)(2,1)S(1)}, u32[]{:S(2)}, u32[]{:S(2)}) %collective-permute-start.17) | collective-permute-done | bytes 655392 | tf_op jit(solution)/shard_map/ppermute | solution.py:399
  175.0 2.0 collective-permute-start.33
  177.1 11.9 %collective-permute-done.18.refs_12_ = bf16[256,1280]{1,0:T(8,128)(2,1)S(1)} collective-permute-done((bf16[256,1280]{1,0:T(8,128)(2,1)S(1)}, bf16[256,1280]{1,0:T(8,128)(2,1)S(1)}, u32[]{:S(2)}, u32[]{:S(2)}) %collective-permute-start.18) | collective-permute-done | bytes 655392 | tf_op jit(solution)/shard_map/ppermute | solution.py:399
  189.1 7.5 %shard_map.197 = (bf16[512,1280]{1,0:T(8,128)(2,1)S(1)}, bf16[512,1280]{1,0:T(8,128)(2,1)S(1)}) custom-call(s32[24]{0:T(128)S(1)} %get-tuple-element.68.info_ref.refs_0_, f32[1,2048]{1,0:T(1,128)S(1)} %bitcast.33, bf16[512,512]{1,0:T(8,128)(2,1)S(1)} %fusion.10.refs_2_, bf16[512,512]{1,0:T(8,128)(2,1)S(1)} %collective-permute-done.10.refs_3_, ...), custom_call_target="tpu_custom_call" | custom-call | tf_op jit(solution)/shard_map/pallas_call | solution.py:366
  196.6 1.9 collective-permute-start.26
  198.5 1.3 collective-permute-start.27
  199.8 0.7 collective-permute-done.26
  200.6 5.0 %collective-permute-done.27 = bf16[1,2560]{1,0:T(2,128)(2,1)S(1)} collective-permute-done((bf16[1,2560]{1,0:T(2,128)(2,1)S(1)}, bf16[1,2560]{1,0:T(2,128)(2,1)S(1)}, u32[]{:S(2)}, u32[]{:S(2)}) %collective-permute-start.27) | collective-permute-done | bytes 5152 | tf_op jit(solution)/shard_map/ppermute | solution.py:360
  206.1 2.2 fusion.2.refs_1_.hidden_ref
  208.3 4.6 %shard_map.198 = (bf16[512,1024]{1,0:T(8,128)(2,1)S(1)}, bf16[512,1024]{1,0:T(8,128)(2,1)S(1)}) custom-call(s32[24]{0:T(128)S(1)} %get-tuple-element.68.info_ref.refs_0_, bf16[512,1280]{1,0:T(8,128)(2,1)S(1)} %fusion.2.refs_1_.hidden_ref, bf16[1280,256]{1,0:T(8,128)(2,1)S(1)} %copy-done.3, bf16[1280,256]{1,0:T(8,128)(2,1)S(1)} %collective-permute-done.28.refs_3_, ...), custom_call_target="tpu_custom_call" | custom-call | tf_op jit(solution)/shard_map/pallas_call | solution.py:366
  212.9 2.4 shard_map.199
  215.4 3.0 %collective-permute-start.36 = (bf16[640,256]{1,0:T(8,128)(2,1)S(1)}, bf16[640,256]{1,0:T(8,128)(2,1)S(1)}, u32[]{:S(2)}, u32[]{:S(2)}) collective-permute-start(bf16[640,256]{1,0:T(8,128)(2,1)S(1)} %slice.338), channel_id=1, source_target_pairs={{4,12},{12,20},{20,28},{28,24},{24,16},{16,8},{8,0},{0,4},{5,13},{... | collective-permute-start | bytes 983048 | tf_op jit(solution)/shard_map/ppermute | solution.py:399
  218.5 7.5 %collective-permute-done.36.top_ref = bf16[640,256]{1,0:T(8,128)(2,1)S(1)} collective-permute-done((bf16[640,256]{1,0:T(8,128)(2,1)S(1)}, bf16[640,256]{1,0:T(8,128)(2,1)S(1)}, u32[]{:S(2)}, u32[]{:S(2)}) %collective-permute-start.36) | collective-permute-done | bytes 327712 | tf_op jit(solution)/shard_map/ppermute | solution.py:399
  226.0 2.3 collective-permute-done.37.bottom_ref
  228.9 1.3 collective-permute-start.38
  230.2 1.1 collective-permute-done.38
  232.5 1.5 collective-permute-start.35
  235.5 10.9 %collective-permute-done.35 = bf16[512,512]{1,0:T(8,128)(2,1)S(1)} collective-permute-done((bf16[512,512]{1,0:T(8,128)(2,1)S(1)}, bf16[512,512]{1,0:T(8,128)(2,1)S(1)}, u32[]{:S(2)}, u32[]{:S(2)}) %collective-permute-start.35) | collective-permute-done | bytes 524320 | tf_op jit(solution)/shard_map/ppermute | solution.py:48
  246.3 1.1 fusion.8
  (96 shorter events, 7.3 us)
Async XLA Ops:
  1.5 11.6 %collective-permute-start = (bf16[3,1024]{1,0:T(4,128)(2,1)S(1)}, bf16[3,1024]{1,0:T(4,128)(2,1)S(1)}, u32[]{:S(2)}, u32[]{:S(2)}) collective-permute-start(bf16[3,1024]{1,0:T(4,128)(2,1)S(1)} %pad_maximum_fusion.3), channel_id=1, source_target_pairs={{0,4},{4,8},{8,12},{12,16},{16,20},{20,24},{24,28},{1,5},{5,9},{9,... | collective-permute-start | bytes 18440 | tf_op jit(solution)/shard_map/ppermute | solution.py:359
  6.4 6.7 %collective-permute-start.1 = (bf16[3,1024]{1,0:T(4,128)(2,1)S(1)}, bf16[3,1024]{1,0:T(4,128)(2,1)S(1)}, u32[]{:S(2)}, u32[]{:S(2)}) collective-permute-start(bf16[3,1024]{1,0:T(4,128)(2,1)S(1)} %pad_maximum_fusion.4), channel_id=1, source_target_pairs={{4,0},{8,4},{12,8},{16,12},{20,16},{24,20},{28,24},{5,1},{9,5},{13... | collective-permute-start | bytes 18440 | tf_op jit(solution)/shard_map/ppermute | solution.py:360
  10.4 0.8 copy-start.5
  11.2 0.8 copy-start.6
  17.0 6.3 %copy-start.13 = (f32[7,256]{1,0:T(8,128)S(1)}, f32[7,256]{1,0:T(8,128)}, u32[]{:S(2)}) copy-start(f32[7,256]{1,0:T(8,128)} %param.30) | copy-start | bytes 21508
  17.0 19.2 %copy-start.10 = (bf16[512,256]{1,0:T(8,128)(2,1)S(1)}, bf16[512,256]{1,0:T(8,128)(2,1)}, u32[]{:S(2)}) copy-start(bf16[512,256]{1,0:T(8,128)(2,1)} %param.24) | copy-start | bytes 786436
  17.4 7.2 %collective-permute-start.2 = (bf16[144,512]{1,0:T(8,128)(2,1)S(1)}, bf16[144,512]{1,0:T(8,128)(2,1)S(1)}, u32[]{:S(2)}, u32[]{:S(2)}) collective-permute-start(bf16[144,512]{1,0:T(8,128)(2,1)S(1)} %get-tuple-element.31), channel_id=1, source_target_pairs={{0,4},{4,8},{8,12},{12,16},{16,20},{20,24},{24,28},{1,5},{5,9},{9,... | collective-permute-start | bytes 442376 | tf_op jit(solution)/shard_map/ppermute | solution.py:496
  22.0 7.4 %collective-permute-start.3 = (bf16[144,512]{1,0:T(8,128)(2,1)S(1)}, bf16[144,512]{1,0:T(8,128)(2,1)S(1)}, u32[]{:S(2)}, u32[]{:S(2)}) collective-permute-start(bf16[144,512]{1,0:T(8,128)(2,1)S(1)} %get-tuple-element.32), channel_id=1, source_target_pairs={{4,0},{8,4},{12,8},{16,12},{20,16},{24,20},{28,24},{5,1},{9,5},{13... | collective-permute-start | bytes 442376 | tf_op jit(solution)/shard_map/ppermute | solution.py:497
  29.6 7.5 %collective-permute-start.4 = (bf16[144,512]{1,0:T(8,128)(2,1)S(1)}, bf16[144,512]{1,0:T(8,128)(2,1)S(1)}, u32[]{:S(2)}, u32[]{:S(2)}) collective-permute-start(bf16[144,512]{1,0:T(8,128)(2,1)S(1)} %get-tuple-element.34), channel_id=1, source_target_pairs={{0,8},{4,12},{8,16},{12,20},{16,24},{20,28},{1,9},{5,13},{9,17},{1... | collective-permute-start | bytes 442376 | tf_op jit(solution)/shard_map/ppermute | solution.py:496
  34.2 7.0 %collective-permute-start.5 = (bf16[144,512]{1,0:T(8,128)(2,1)S(1)}, bf16[144,512]{1,0:T(8,128)(2,1)S(1)}, u32[]{:S(2)}, u32[]{:S(2)}) collective-permute-start(bf16[144,512]{1,0:T(8,128)(2,1)S(1)} %get-tuple-element.35), channel_id=1, source_target_pairs={{8,0},{12,4},{16,8},{20,12},{24,16},{28,20},{9,1},{13,5},{17,9},{2... | collective-permute-start | bytes 442376 | tf_op jit(solution)/shard_map/ppermute | solution.py:497
  42.1 9.2 %collective-permute-start.6 = (bf16[144,512]{1,0:T(8,128)(2,1)S(1)}, bf16[144,512]{1,0:T(8,128)(2,1)S(1)}, u32[]{:S(2)}, u32[]{:S(2)}) collective-permute-start(bf16[144,512]{1,0:T(8,128)(2,1)S(1)} %get-tuple-element.38), channel_id=1, source_target_pairs={{0,16},{4,20},{8,24},{12,28},{1,17},{5,21},{9,25},{13,29},{2,18},{... | collective-permute-start | bytes 442376 | tf_op jit(solution)/shard_map/ppermute | solution.py:496
  46.8 9.2 %collective-permute-start.7 = (bf16[144,512]{1,0:T(8,128)(2,1)S(1)}, bf16[144,512]{1,0:T(8,128)(2,1)S(1)}, u32[]{:S(2)}, u32[]{:S(2)}) collective-permute-start(bf16[144,512]{1,0:T(8,128)(2,1)S(1)} %get-tuple-element.39), channel_id=1, source_target_pairs={{16,0},{20,4},{24,8},{28,12},{17,1},{21,5},{25,9},{29,13},{18,2},{... | collective-permute-start | bytes 442376 | tf_op jit(solution)/shard_map/ppermute | solution.py:497
  48.6 7.5 %copy-start = (bf16[512,2048]{1,0:T(8,128)(2,1)S(1)}, bf16[512,2048]{1,0:T(8,128)(2,1)}, u32[]{:S(2)}) copy-start(bf16[512,2048]{1,0:T(8,128)(2,1)} %map_ref.1) | copy-start | bytes 6291460
  48.7 7.5 %copy-start.4 = (bf16[512,512]{1,0:T(8,128)(2,1)S(1)}, bf16[512,512]{1,0:T(8,128)(2,1)}, u32[]{:S(2)}) copy-start(bf16[512,512]{1,0:T(8,128)(2,1)} %valve_ref.1) | copy-start | bytes 1572868
  48.7 7.5 %copy-start.8 = (f32[512]{0:T(512)S(1)}, f32[512]{0:T(512)}, u32[]{:S(2)}) copy-start(f32[512]{0:T(512)} %param.31) | copy-start | bytes 6148
  56.1 2.9 %copy-start.1 = (bf16[256,1280]{1,0:T(8,128)(2,1)S(1)}, bf16[256,1280]{1,0:T(8,128)(2,1)}, u32[]{:S(2)}) copy-start(bf16[256,1280]{1,0:T(8,128)(2,1)} %refs_5_.1) | copy-start | bytes 1966084
  56.1 3.0 %copy-start.2 = (bf16[256,1280]{1,0:T(8,128)(2,1)S(1)}, bf16[256,1280]{1,0:T(8,128)(2,1)}, u32[]{:S(2)}) copy-start(bf16[256,1280]{1,0:T(8,128)(2,1)} %refs_13_.1) | copy-start | bytes 1966084
  58.9 4.2 %collective-permute-start.8 = (bf16[512,1024]{1,0:T(8,128)(2,1)S(1)}, bf16[512,1024]{1,0:T(8,128)(2,1)S(1)}, u32[]{:S(2)}, u32[]{:S(2)}) collective-permute-start(bf16[512,1024]{1,0:T(8,128)(2,1)S(1)} %get-tuple-element.42), channel_id=1, source_target_pairs={{0,1},{1,0},{2,3},{3,2},{4,5},{5,4},{6,7},{7,6},{8,9},{9,8},{10,11... | collective-permute-start | bytes 3145736 | tf_op jit(solution)/shard_map/ppermute | solution.py:48
  59.0 17.7 %collective-permute-start.12 = (bf16[256,1280]{1,0:T(8,128)(2,1)S(1)}, bf16[256,1280]{1,0:T(8,128)(2,1)S(1)}, u32[]{:S(2)}, u32[]{:S(2)}) collective-permute-start(bf16[256,1280]{1,0:T(8,128)(2,1)S(1)} %copy-done.1), channel_id=1, source_target_pairs={{4,12},{12,20},{20,28},{28,24},{24,16},{16,8},{8,0},{0,4},{5,13},{... | collective-permute-start | bytes 1966088 | tf_op jit(solution)/shard_map/ppermute | solution.py:399
  59.1 17.7 %collective-permute-start.20 = (bf16[256,1280]{1,0:T(8,128)(2,1)S(1)}, bf16[256,1280]{1,0:T(8,128)(2,1)S(1)}, u32[]{:S(2)}, u32[]{:S(2)}) collective-permute-start(bf16[256,1280]{1,0:T(8,128)(2,1)S(1)} %copy-done.2), channel_id=1, source_target_pairs={{12,4},{20,12},{28,20},{24,28},{16,24},{8,16},{0,8},{4,0},{13,5},{... | collective-permute-start | bytes 1966088 | tf_op jit(solution)/shard_map/ppermute | solution.py:399
  61.1 29.7 %collective-permute-start.13 = (bf16[256,1280]{1,0:T(8,128)(2,1)S(1)}, bf16[256,1280]{1,0:T(8,128)(2,1)S(1)}, u32[]{:S(2)}, u32[]{:S(2)}) collective-permute-start(bf16[256,1280]{1,0:T(8,128)(2,1)S(1)} %copy-done.1), channel_id=1, source_target_pairs={{12,4},{20,12},{28,20},{24,28},{16,24},{8,16},{0,8},{4,0},{13,5},{... | collective-permute-start | bytes 1966088 | tf_op jit(solution)/shard_map/ppermute | solution.py:399
  61.1 29.7 %collective-permute-start.19 = (bf16[256,1280]{1,0:T(8,128)(2,1)S(1)}, bf16[256,1280]{1,0:T(8,128)(2,1)S(1)}, u32[]{:S(2)}, u32[]{:S(2)}) collective-permute-start(bf16[256,1280]{1,0:T(8,128)(2,1)S(1)} %copy-done.2), channel_id=1, source_target_pairs={{4,12},{12,20},{20,28},{28,24},{24,16},{16,8},{8,0},{0,4},{5,13},{... | collective-permute-start | bytes 1966088 | tf_op jit(solution)/shard_map/ppermute | solution.py:399
  63.1 13.6 %copy-start.3 = (bf16[1280,256]{1,0:T(8,128)(2,1)S(1)}, bf16[1280,256]{1,0:T(8,128)(2,1)}, u32[]{:S(2)}) copy-start(bf16[1280,256]{1,0:T(8,128)(2,1)} %refs_2_.1) | copy-start | bytes 1966084
  63.1 31.7 %copy-start.9 = (bf16[512,512]{1,0:T(8,128)(2,1)S(1)}, bf16[512,512]{1,0:T(8,128)(2,1)}, u32[]{:S(2)}) copy-start(bf16[512,512]{1,0:T(8,128)(2,1)} %param.20) | copy-start | bytes 1572868
  63.6 99.4 %copy-start.11 = (f32[3,1280]{1,0:T(4,128)S(1)}, f32[3,1280]{1,0:T(4,128)}, u32[]{:S(2)}) copy-start(f32[3,1280]{1,0:T(4,128)} %param.37) | copy-start | bytes 46084
  63.6 99.4 %copy-start.12 = (f32[3,1280]{1,0:T(4,128)S(1)}, f32[3,1280]{1,0:T(4,128)}, u32[]{:S(2)}) copy-start(f32[3,1280]{1,0:T(4,128)} %param.36) | copy-start | bytes 46084
  63.6 125.5 %copy-start.7 = (f32[2048]{0:T(1024)S(1)}, f32[2048]{0:T(1024)}, u32[]{:S(2)}) copy-start(f32[2048]{0:T(1024)} %param.33) | copy-start | bytes 24580
  63.6 29.2 %collective-permute-start.9 = (bf16[512,512]{1,0:T(8,128)(2,1)S(1)}, bf16[512,512]{1,0:T(8,128)(2,1)S(1)}, u32[]{:S(2)}, u32[]{:S(2)}) collective-permute-start(bf16[512,512]{1,0:T(8,128)(2,1)S(1)} %slice.528), channel_id=1, source_target_pairs={{0,2},{1,3},{2,0},{3,1},{4,6},{5,7},{6,4},{7,5},{8,10},{9,11},{10,... | collective-permute-start | bytes 1572872 | tf_op jit(solution)/shard_map/ppermute | solution.py:48
  76.7 28.1 %collective-permute-start.28 = (bf16[1280,256]{1,0:T(8,128)(2,1)S(1)}, bf16[1280,256]{1,0:T(8,128)(2,1)S(1)}, u32[]{:S(2)}, u32[]{:S(2)}) collective-permute-start(bf16[1280,256]{1,0:T(8,128)(2,1)S(1)} %copy-done.3), channel_id=1, source_target_pairs={{4,12},{12,20},{20,28},{28,24},{24,16},{16,8},{8,0},{0,4},{5,13},{... | collective-permute-start | bytes 1966088 | tf_op jit(solution)/shard_map/ppermute | solution.py:399
  76.7 29.5 %collective-permute-start.31 = (bf16[1280,256]{1,0:T(8,128)(2,1)S(1)}, bf16[1280,256]{1,0:T(8,128)(2,1)S(1)}, u32[]{:S(2)}, u32[]{:S(2)}) collective-permute-start(bf16[1280,256]{1,0:T(8,128)(2,1)S(1)} %copy-done.3), channel_id=1, source_target_pairs={{12,4},{20,12},{28,20},{24,28},{16,24},{8,16},{0,8},{4,0},{13,5},{... | collective-permute-start | bytes 1966088 | tf_op jit(solution)/shard_map/ppermute | solution.py:399
  90.8 28.0 %collective-permute-start.14 = (bf16[256,1280]{1,0:T(8,128)(2,1)S(1)}, bf16[256,1280]{1,0:T(8,128)(2,1)S(1)}, u32[]{:S(2)}, u32[]{:S(2)}) collective-permute-start(bf16[256,1280]{1,0:T(8,128)(2,1)S(1)} %collective-permute-done.12.refs_6_), channel_id=1, source_target_pairs={{4,12},{12,20},{20,28},{28,24},{24,16},{16,8},{8,0},{0,4},{5,13},{... | collective-permute-start | bytes 1966088 | tf_op jit(solution)/shard_map/ppermute | solution.py:399
  90.8 28.1 %collective-permute-start.22 = (bf16[256,1280]{1,0:T(8,128)(2,1)S(1)}, bf16[256,1280]{1,0:T(8,128)(2,1)S(1)}, u32[]{:S(2)}, u32[]{:S(2)}) collective-permute-start(bf16[256,1280]{1,0:T(8,128)(2,1)S(1)} %collective-permute-done.20.refs_15_), channel_id=1, source_target_pairs={{12,4},{20,12},{28,20},{24,28},{16,24},{8,16},{0,8},{4,0},{13,5},{... | collective-permute-start | bytes 1966088 | tf_op jit(solution)/shard_map/ppermute | solution.py:399
  92.8 40.1 %collective-permute-start.15 = (bf16[256,1280]{1,0:T(8,128)(2,1)S(1)}, bf16[256,1280]{1,0:T(8,128)(2,1)S(1)}, u32[]{:S(2)}, u32[]{:S(2)}) collective-permute-start(bf16[256,1280]{1,0:T(8,128)(2,1)S(1)} %collective-permute-done.13.refs_7_), channel_id=1, source_target_pairs={{12,4},{20,12},{28,20},{24,28},{16,24},{8,16},{0,8},{4,0},{13,5},{... | collective-permute-start | bytes 1966088 | tf_op jit(solution)/shard_map/ppermute | solution.py:399
  104.7 28.2 %collective-permute-start.10 = (bf16[512,512]{1,0:T(8,128)(2,1)S(1)}, bf16[512,512]{1,0:T(8,128)(2,1)S(1)}, u32[]{:S(2)}, u32[]{:S(2)}) collective-permute-start(bf16[512,512]{1,0:T(8,128)(2,1)S(1)} %fusion.10.refs_2_), channel_id=1, source_target_pairs={{0,2},{1,3},{2,0},{3,1},{4,6},{5,7},{6,4},{7,5},{8,10},{9,11},{10,... | collective-permute-start | bytes 1572872 | tf_op jit(solution)/shard_map/ppermute | solution.py:48
  106.2 28.9 %collective-permute-start.21 = (bf16[256,1280]{1,0:T(8,128)(2,1)S(1)}, bf16[256,1280]{1,0:T(8,128)(2,1)S(1)}, u32[]{:S(2)}, u32[]{:S(2)}) collective-permute-start(bf16[256,1280]{1,0:T(8,128)(2,1)S(1)} %collective-permute-done.19.refs_14_), channel_id=1, source_target_pairs={{4,12},{12,20},{20,28},{28,24},{24,16},{16,8},{8,0},{0,4},{5,13},{... | collective-permute-start | bytes 1966088 | tf_op jit(solution)/shard_map/ppermute | solution.py:399
  118.8 28.1 %collective-permute-start.29 = (bf16[1280,256]{1,0:T(8,128)(2,1)S(1)}, bf16[1280,256]{1,0:T(8,128)(2,1)S(1)}, u32[]{:S(2)}, u32[]{:S(2)}) collective-permute-start(bf16[1280,256]{1,0:T(8,128)(2,1)S(1)} %collective-permute-done.28.refs_3_), channel_id=1, source_target_pairs={{4,12},{12,20},{20,28},{28,24},{24,16},{16,8},{8,0},{0,4},{5,13},{... | collective-permute-start | bytes 1966088 | tf_op jit(solution)/shard_map/ppermute | solution.py:399
  118.9 28.1 %collective-permute-start.32 = (bf16[1280,256]{1,0:T(8,128)(2,1)S(1)}, bf16[1280,256]{1,0:T(8,128)(2,1)S(1)}, u32[]{:S(2)}, u32[]{:S(2)}) collective-permute-start(bf16[1280,256]{1,0:T(8,128)(2,1)S(1)} %collective-permute-done.31.refs_4_), channel_id=1, source_target_pairs={{12,4},{20,12},{28,20},{24,28},{16,24},{8,16},{0,8},{4,0},{13,5},{... | collective-permute-start | bytes 1966088 | tf_op jit(solution)/shard_map/ppermute | solution.py:399
  132.9 28.0 %collective-permute-start.16 = (bf16[256,1280]{1,0:T(8,128)(2,1)S(1)}, bf16[256,1280]{1,0:T(8,128)(2,1)S(1)}, u32[]{:S(2)}, u32[]{:S(2)}) collective-permute-start(bf16[256,1280]{1,0:T(8,128)(2,1)S(1)} %collective-permute-done.14.refs_8_), channel_id=1, source_target_pairs={{4,12},{12,20},{20,28},{28,24},{24,16},{16,8},{8,0},{0,4},{5,13},{... | collective-permute-start | bytes 1966088 | tf_op jit(solution)/shard_map/ppermute | solution.py:399
  132.9 28.1 %collective-permute-start.24 = (bf16[256,1280]{1,0:T(8,128)(2,1)S(1)}, bf16[256,1280]{1,0:T(8,128)(2,1)S(1)}, u32[]{:S(2)}, u32[]{:S(2)}) collective-permute-start(bf16[256,1280]{1,0:T(8,128)(2,1)S(1)} %collective-permute-done.22.refs_17_), channel_id=1, source_target_pairs={{12,4},{20,12},{28,20},{24,28},{16,24},{8,16},{0,8},{4,0},{13,5},{... | collective-permute-start | bytes 1966088 | tf_op jit(solution)/shard_map/ppermute | solution.py:399
  135.1 54.0 %collective-permute-start.11 = (bf16[512,1024]{1,0:T(8,128)(2,1)S(1)}, bf16[512,1024]{1,0:T(8,128)(2,1)S(1)}, u32[]{:S(2)}, u32[]{:S(2)}) collective-permute-start(bf16[512,1024]{1,0:T(8,128)(2,1)S(1)} %pad_maximum_fusion), channel_id=1, source_target_pairs={{0,1},{1,0},{2,3},{3,2},{4,5},{5,4},{6,7},{7,6},{8,9},{9,8},{10,11... | collective-permute-start | bytes 3145736 | tf_op jit(solution)/shard_map/ppermute | solution.py:48
  146.9 28.2 %collective-permute-start.17 = (bf16[256,1280]{1,0:T(8,128)(2,1)S(1)}, bf16[256,1280]{1,0:T(8,128)(2,1)S(1)}, u32[]{:S(2)}, u32[]{:S(2)}) collective-permute-start(bf16[256,1280]{1,0:T(8,128)(2,1)S(1)} %collective-permute-done.15.refs_9_), channel_id=1, source_target_pairs={{12,4},{20,12},{28,20},{24,28},{16,24},{8,16},{0,8},{4,0},{13,5},{... | collective-permute-start | bytes 1966088 | tf_op jit(solution)/shard_map/ppermute | solution.py:399
  146.9 28.1 %collective-permute-start.23 = (bf16[256,1280]{1,0:T(8,128)(2,1)S(1)}, bf16[256,1280]{1,0:T(8,128)(2,1)S(1)}, u32[]{:S(2)}, u32[]{:S(2)}) collective-permute-start(bf16[256,1280]{1,0:T(8,128)(2,1)S(1)} %collective-permute-done.21.refs_16_), channel_id=1, source_target_pairs={{4,12},{12,20},{20,28},{28,24},{24,16},{16,8},{8,0},{0,4},{5,13},{... | collective-permute-start | bytes 1966088 | tf_op jit(solution)/shard_map/ppermute | solution.py:399
  160.9 28.1 %collective-permute-start.18 = (bf16[256,1280]{1,0:T(8,128)(2,1)S(1)}, bf16[256,1280]{1,0:T(8,128)(2,1)S(1)}, u32[]{:S(2)}, u32[]{:S(2)}) collective-permute-start(bf16[256,1280]{1,0:T(8,128)(2,1)S(1)} %collective-permute-done.16.refs_10_), channel_id=1, source_target_pairs={{4,12},{12,20},{20,28},{28,24},{24,16},{16,8},{8,0},{0,4},{5,13},{... | collective-permute-start | bytes 1966088 | tf_op jit(solution)/shard_map/ppermute | solution.py:399
  161.0 28.1 %collective-permute-start.25 = (bf16[256,1280]{1,0:T(8,128)(2,1)S(1)}, bf16[256,1280]{1,0:T(8,128)(2,1)S(1)}, u32[]{:S(2)}, u32[]{:S(2)}) collective-permute-start(bf16[256,1280]{1,0:T(8,128)(2,1)S(1)} %collective-permute-done.24.refs_19_), channel_id=1, source_target_pairs={{12,4},{20,12},{28,20},{24,28},{16,24},{8,16},{0,8},{4,0},{13,5},{... | collective-permute-start | bytes 1966088 | tf_op jit(solution)/shard_map/ppermute | solution.py:399
  175.0 37.8 %collective-permute-start.30 = (bf16[1280,256]{1,0:T(8,128)(2,1)S(1)}, bf16[1280,256]{1,0:T(8,128)(2,1)S(1)}, u32[]{:S(2)}, u32[]{:S(2)}) collective-permute-start(bf16[1280,256]{1,0:T(8,128)(2,1)S(1)} %collective-permute-done.29.refs_5_), channel_id=1, source_target_pairs={{4,12},{12,20},{20,28},{28,24},{24,16},{16,8},{8,0},{0,4},{5,13},{... | collective-permute-start | bytes 1966088 | tf_op jit(solution)/shard_map/ppermute | solution.py:399
  175.0 37.8 %collective-permute-start.33 = (bf16[1280,256]{1,0:T(8,128)(2,1)S(1)}, bf16[1280,256]{1,0:T(8,128)(2,1)S(1)}, u32[]{:S(2)}, u32[]{:S(2)}) collective-permute-start(bf16[1280,256]{1,0:T(8,128)(2,1)S(1)} %collective-permute-done.32.refs_6_), channel_id=1, source_target_pairs={{12,4},{20,12},{28,20},{24,28},{16,24},{8,16},{0,8},{4,0},{13,5},{... | collective-permute-start | bytes 1966088 | tf_op jit(solution)/shard_map/ppermute | solution.py:399
  196.6 3.9 %collective-permute-start.26 = (bf16[1,2560]{1,0:T(2,128)(2,1)S(1)}, bf16[1,2560]{1,0:T(2,128)(2,1)S(1)}, u32[]{:S(2)}, u32[]{:S(2)}) collective-permute-start(bf16[1,2560]{1,0:T(2,128)(2,1)S(1)} %pad_maximum_fusion.1), channel_id=1, source_target_pairs={{0,4},{4,8},{8,12},{12,16},{16,20},{20,24},{24,28},{1,5},{5,9},{9,... | collective-permute-start | bytes 15368 | tf_op jit(solution)/shard_map/ppermute | solution.py:359
  198.5 7.0 %collective-permute-start.27 = (bf16[1,2560]{1,0:T(2,128)(2,1)S(1)}, bf16[1,2560]{1,0:T(2,128)(2,1)S(1)}, u32[]{:S(2)}, u32[]{:S(2)}) collective-permute-start(bf16[1,2560]{1,0:T(2,128)(2,1)S(1)} %pad_maximum_fusion.2), channel_id=1, source_target_pairs={{4,0},{8,4},{12,8},{16,12},{20,16},{24,20},{28,24},{5,1},{9,5},{13... | collective-permute-start | bytes 15368 | tf_op jit(solution)/shard_map/ppermute | solution.py:360
  215.3 16.7 %collective-permute-start.34 = (bf16[512,1024]{1,0:T(8,128)(2,1)S(1)}, bf16[512,1024]{1,0:T(8,128)(2,1)S(1)}, u32[]{:S(2)}, u32[]{:S(2)}) collective-permute-start(bf16[512,1024]{1,0:T(8,128)(2,1)S(1)} %get-tuple-element.48), channel_id=1, source_target_pairs={{0,1},{1,0},{2,3},{3,2},{4,5},{5,4},{6,7},{7,6},{8,9},{9,8},{10,11... | collective-permute-start | bytes 3145736 | tf_op jit(solution)/shard_map/ppermute | solution.py:48
  215.4 10.6 %collective-permute-start.36 = (bf16[640,256]{1,0:T(8,128)(2,1)S(1)}, bf16[640,256]{1,0:T(8,128)(2,1)S(1)}, u32[]{:S(2)}, u32[]{:S(2)}) collective-permute-start(bf16[640,256]{1,0:T(8,128)(2,1)S(1)} %slice.338), channel_id=1, source_target_pairs={{4,12},{12,20},{20,28},{28,24},{24,16},{16,8},{8,0},{0,4},{5,13},{... | collective-permute-start | bytes 983048 | tf_op jit(solution)/shard_map/ppermute | solution.py:399
  218.4 9.9 %collective-permute-start.37 = (bf16[640,256]{1,0:T(8,128)(2,1)S(1)}, bf16[640,256]{1,0:T(8,128)(2,1)S(1)}, u32[]{:S(2)}, u32[]{:S(2)}) collective-permute-start(bf16[640,256]{1,0:T(8,128)(2,1)S(1)} %slice.339), channel_id=1, source_target_pairs={{12,4},{20,12},{28,20},{24,28},{16,24},{8,16},{0,8},{4,0},{13,5},{... | collective-permute-start | bytes 983048 | tf_op jit(solution)/shard_map/ppermute | solution.py:399
  228.9 2.4 collective-permute-start.38
  231.4 3.9 %collective-permute-start.39 = (bf16[512,256]{1,0:T(8,128)(2,1)S(1)}, bf16[512,256]{1,0:T(8,128)(2,1)S(1)}, u32[]{:S(2)}, u32[]{:S(2)}) collective-permute-start(bf16[512,256]{1,0:T(8,128)(2,1)S(1)} %fusion.29), channel_id=1, source_target_pairs={{1,3},{5,7},{8,10},{12,14},{19,17},{23,21},{26,24},{30,28}} | collective-permute-start | bytes 786440 | tf_op jit(solution)/shard_map/ppermute | solution.py:595
  232.5 13.8 %collective-permute-start.35 = (bf16[512,512]{1,0:T(8,128)(2,1)S(1)}, bf16[512,512]{1,0:T(8,128)(2,1)S(1)}, u32[]{:S(2)}, u32[]{:S(2)}) collective-permute-start(bf16[512,512]{1,0:T(8,128)(2,1)S(1)} %slice.527), channel_id=1, source_target_pairs={{0,2},{1,3},{2,0},{3,1},{4,6},{5,7},{6,4},{7,5},{8,10},{9,11},{10,... | collective-permute-start | bytes 1572872 | tf_op jit(solution)/shard_map/ppermute | solution.py:48

commit v2 on v1

--- a/solution.py
+++ b/solution.py
@@ -254,14 +254,14 @@
         target[:, at * block : (at + 1) * block] = term
 
 
-def up_kernel(sizes, plan, counts, *refs):
+def up_kernel(sizes, plan, counts, last, *refs):
     n_pieces, n_arrays = counts
     sp_count, tp_count = sizes
     info_ref, gain_ref = refs[:2]
     pieces = refs[2 : 2 + n_pieces]
     arrays = refs[2 + n_pieces : 2 + n_pieces + n_arrays]
     outs = refs[2 + n_pieces + n_arrays : 4 + n_pieces + n_arrays]
-    rows_scr, gain_scr = refs[4 + n_pieces + n_arrays :]
+    last_ref, rows_scr, gain_scr = refs[4 + n_pieces + n_arrays :]
     length, full = pieces[0].shape[0], gain_ref.shape[1]
     chunk, block = full // sp_count, full // tp_count
     for p in range(tp_count):
@@ -286,6 +286,7 @@
         return carry
 
     lax.fori_loop(0, length // band, norm, 0)
+    last_ref[...] = rows_scr[info_ref[last] // chunk]
     columns = outs[0].shape[1]
     tile = 256 if columns % 256 == 0 else columns
     for which in range(2):
@@ -299,7 +300,17 @@
                     preferred_element_type=jnp.float32,
                 )
                 total = term if total is None else total + term
-            outs[which][:, at] = total.astype(jnp.bfloat16)
+            outs[which][:, at] = total
+
+
+def up_last_kernel(gate_ref, value_ref, rows_ref, gate_map_ref, value_map_ref, gate_out, value_out):
+    columns = gate_ref.shape[1]
+    tile = 256 if columns % 256 == 0 else columns
+    for held, map_ref, out in ((gate_ref, gate_map_ref, gate_out), (value_ref, value_map_ref, value_out)):
+        for j in range(columns // tile):
+            at = slice(j * tile, (j + 1) * tile)
+            term = jnp.dot(rows_ref[...], map_ref[:, at], preferred_element_type=jnp.float32)
+            out[:, at] = (held[:, at] + term).astype(jnp.bfloat16)
 
 
 def down_kernel(sizes, plan, blank, n_arrays, *refs):
@@ -456,7 +467,11 @@
         hidden_cols = dense_valve_map.shape[1]
         chunk = dense_valve_map.shape[0]
         up_rings = [[(0, own, 0)] + ring(own, way) for own, way in ((dense_valve_map, "f"), (dense_payload_map, "b"))]
-        down_ring = [(0, dense_contract_map, 0)] + ring(dense_contract_map, "fb")
+        half_row = hidden_cols // 2
+        down_rings = [
+            [(0, own, 0)] + ring(own, way)
+            for own, way in ((dense_contract_map[:half_row], "f"), (dense_contract_map[half_row:], "b"))
+        ]
         info = jnp.asarray(table(chunk, own_cols))[lax.axis_index("sp") * tp_count + me]
 
         rows, cols, scale, last = call(
@@ -531,17 +546,26 @@
         middle = (skip_trunk_vector.astype(jnp.float32) + projected).astype(jnp.bfloat16)
         pieces = tp.gather(middle)
 
-        arrays = [array for entries in up_rings for _, array, _ in entries]
-        plan = [[steps % sp_count for steps, _, _ in entries] for entries in up_rings]
-        gate_rows, value_rows = call(
-            functools.partial(up_kernel, (sp_count, tp_count), plan, (len(pieces), len(arrays))),
-            [((length, hidden_cols), jnp.bfloat16)] * 2,
+        arrays = [array for entries in up_rings for _, array, _ in entries[:-1]]
+        plan = [[steps % sp_count for steps, _, _ in entries[:-1]] for entries in up_rings]
+        last = up_rings[0][-1][0] % sp_count
+        gate_sum, value_sum, last_rows = call(
+            functools.partial(up_kernel, (sp_count, tp_count), plan, (len(pieces), len(arrays)), last),
+            [((length, hidden_cols), jnp.float32)] * 2 + [((length, chunk), jnp.bfloat16)],
             info,
             dense_standardize_factor[None, :],
             *pieces,
             *arrays,
             scalars=1,
             scratch=[pltpu.VMEM((sp_count, length, chunk), jnp.bfloat16), pltpu.VMEM((1, full), jnp.float32)],
+        )
+        gate_rows, value_rows = call(
+            up_last_kernel,
+            [((length, hidden_cols), jnp.bfloat16)] * 2,
+            gate_sum,
+            value_sum,
+            last_rows,
+            *(entries[-1][1] for entries in up_rings),
         )
         margin = valve_series_smoother.shape[0] // 2
         low, high = edges(
@@ -569,20 +593,28 @@
 
         if chunk % 128:
             whole = jnp.zeros((hidden_cols, full), jnp.bfloat16)
-            for steps, array, first in down_ring:
-                whole = lax.dynamic_update_slice(whole, array, (first, info[sp_count + steps % sp_count]))
+            for part, entries in enumerate(down_rings):
+                for steps, array, _ in entries:
+                    corner = (part * half_row, info[sp_count + steps % sp_count])
+                    whole = lax.dynamic_update_slice(whole, array, corner)
             send, keep = down([(0, [(0, 0)])], None, [whole])
             down_sum = tp.reduce_scatter(send, keep)
             return (middle.astype(jnp.float32) + down_sum).astype(jnp.bfloat16)
 
         far = sp_count // 2
-        near_chunks = [(steps % sp_count, array) for steps, array, _ in down_ring if abs(steps) < far]
-        early, late = near_chunks[:-2], near_chunks[-2:]
-        held = down([(slot, [(n, 0)]) for n, (slot, _) in enumerate(early)], None, [a for _, a in early])
-        send, keep = down([(slot, [(n, 0)]) for n, (slot, _) in enumerate(late)], far, [a for _, a in late], held)
+        pairs = [
+            (steps % sp_count, (top, bottom)) for (steps, top, _), (_, bottom, _) in zip(*down_rings) if abs(steps) < far
+        ]
+
+        def part_of(chunks, blank, held=()):
+            plan = [(slot, [(2 * n, 0), (2 * n + 1, half_row)]) for n, (slot, _) in enumerate(chunks)]
+            return down(plan, blank, [array for _, both_parts in chunks for array in both_parts], held)
+
+        early = part_of(pairs[:-2], None)
+        send, keep = part_of(pairs[-2:], far, early)
         down_sum = tp.reduce_scatter(send, keep)
         (part,) = call(
-            far_kernel, [((length, chunk), jnp.bfloat16)], hidden, *(a for _, a, _ in down_ring[-2:])
+            far_kernel, [((length, chunk), jnp.bfloat16)], hidden, *(entries[-1][1] for entries in down_rings)
         )
         for bit in range(tp.bits):
             pairs = []

time: 251 us -> 256 us (1.020)
  waiting for transfers between devices: 149 us -> 157 us
  starting transfers between devices: 56.8 us -> 53.7 us
    ppermute x2, waiting for transfers between devices: 0.71 us -> 4.04 us  [edges(): low = lax.ppermute(last, 'sp', forward)]
    ppermute x6, waiting for transfers between devices: 10.9 us -> 14.1 us  [swap(): lax.ppermute(array, 'tp', [(i, i ^ 1 << bit) for i in range(self.count)])]
    ppermute x22 -> x28, starting transfers between devices: 23 us -> 19.9 us  [send_on(): return lax.ppermute(array, 'sp', pairs)]
    ppermute x22 -> x28, waiting for transfers between devices: 116 us -> 117 us  [send_on(): return lax.ppermute(array, 'sp', pairs)]
    pallas_call x11 -> x12, Pallas kernels: 23.2 us -> 24.2 us  [call(): pl.pallas_call(kernel, out_shape=[jax.ShapeDtypeStruct(shape, kind) for s...]
  transfers between devices with their start and end apart: 40 -> 46, of which waited for: 25 -> 25; matrix products, arithmetic and copies ran while one was open for 4% -> 3% of each run, Pallas kernels for 7% -> 7%
where the time goes in v2:
time: 256 us; the launch traced here: 253 us
  waiting for transfers between devices  157 us (61%)
  starting transfers between devices  53.7 us (21%)
  Pallas kernels  24.2 us (9%)
  other arithmetic  9.57 us (4%)
  local copies, waits for them, and re-layouts  7.38 us (3%)
    ppermute x28, waiting for transfers between devices, send_on(): return lax.ppermute(array, 'sp', pairs)  117 us
    pallas_call x12, Pallas kernels, call(): pl.pallas_call(kernel, out_shape=[jax.ShapeDtypeStruct(shape, kind) for s...  24.2 us
    ppermute x28, starting transfers between devices, send_on(): return lax.ppermute(array, 'sp', pairs)  19.9 us
    ppermute x6, waiting for transfers between devices, swap(): lax.ppermute(array, 'tp', [(i, i ^ 1 << bit) for i in range(self.count)])  14.1 us
    ppermute x3, starting transfers between devices, shards(): got_f = lax.ppermute(send_f, 'sp', forward)  13.8 us
    ppermute x3, waiting for transfers between devices, shards(): got_b = lax.ppermute(send_b, 'sp', [(b, a) for a, b in forward])  13.6 us
    ppermute x2, starting transfers between devices, edges(): low = lax.ppermute(last, 'sp', forward)  8.35 us
  transfers between devices with their start and end apart: 46, of which 25 were waited for; matrix products, arithmetic and copies ran while one was open for 3% of the time, Pallas kernels for 7%

profile of v2, /device:TPU:0, one launch (start us, length us, event | category | flops | bytes accessed | tf_op | source)
XLA Modules:
  0.0 253.2 jit_solution(1799823978316390651)
XLA Ops:
  1.5 4.9 %collective-permute-start = (bf16[3,1024]{1,0:T(4,128)(2,1)S(1)}, bf16[3,1024]{1,0:T(4,128)(2,1)S(1)}, u32[]{:S(2)}, u32[]{:S(2)}) collective-permute-start(bf16[3,1024]{1,0:T(4,128)(2,1)S(1)} %pad_maximum_fusion.3), channel_id=1, source_target_pairs={{0,4},{4,8},{8,12},{12,16},{16,20},{20,24},{24,28},{1,5},{5,9},{9,... | collective-permute-start | bytes 18440 | tf_op jit(solution)/shard_map/ppermute | solution.py:370
  6.4 1.3 collective-permute-start.1
  7.7 1.0 fusion.39
  8.7 1.0 fusion.45
  9.7 0.8 copy.21
  10.4 0.8 copy-done.4
  11.2 0.8 copy-done.5
  11.9 1.2 shard_map.190
  13.1 1.0 maximum_convert_fusion.3
  14.2 1.2 maximum_convert_fusion.2
  15.9 1.1 multiply_convert_fusion.values_ref
  17.4 4.6 %collective-permute-start.2 = (bf16[144,512]{1,0:T(8,128)(2,1)S(1)}, bf16[144,512]{1,0:T(8,128)(2,1)S(1)}, u32[]{:S(2)}, u32[]{:S(2)}) collective-permute-start(bf16[144,512]{1,0:T(8,128)(2,1)S(1)} %get-tuple-element.34), channel_id=1, source_target_pairs={{0,4},{4,8},{8,12},{12,16},{16,20},{20,24},{24,28},{1,5},{5,9},{9,... | collective-permute-start | bytes 442376 | tf_op jit(solution)/shard_map/ppermute | solution.py:511
  22.0 1.3 collective-permute-start.3
  23.3 1.3 collective-permute-done.2.refs_0_
  24.6 4.8 %collective-permute-done.3.refs_1_ = bf16[144,512]{1,0:T(8,128)(2,1)S(1)} collective-permute-done((bf16[144,512]{1,0:T(8,128)(2,1)S(1)}, bf16[144,512]{1,0:T(8,128)(2,1)S(1)}, u32[]{:S(2)}, u32[]{:S(2)}) %collective-permute-start.3) | collective-permute-done | bytes 147488 | tf_op jit(solution)/shard_map/ppermute | solution.py:512
  29.6 4.6 %collective-permute-start.4 = (bf16[144,512]{1,0:T(8,128)(2,1)S(1)}, bf16[144,512]{1,0:T(8,128)(2,1)S(1)}, u32[]{:S(2)}, u32[]{:S(2)}) collective-permute-start(bf16[144,512]{1,0:T(8,128)(2,1)S(1)} %get-tuple-element.37), channel_id=1, source_target_pairs={{0,8},{4,12},{8,16},{12,20},{16,24},{20,28},{1,9},{5,13},{9,17},{1... | collective-permute-start | bytes 442376 | tf_op jit(solution)/shard_map/ppermute | solution.py:511
  34.2 1.3 collective-permute-start.5
  36.2 0.8 collective-permute-done.4.refs_0_
  37.1 4.1 %collective-permute-done.5.refs_1_ = bf16[144,512]{1,0:T(8,128)(2,1)S(1)} collective-permute-done((bf16[144,512]{1,0:T(8,128)(2,1)S(1)}, bf16[144,512]{1,0:T(8,128)(2,1)S(1)}, u32[]{:S(2)}, u32[]{:S(2)}) %collective-permute-start.5) | collective-permute-done | bytes 147488 | tf_op jit(solution)/shard_map/ppermute | solution.py:512
  41.2 0.9 shard_map.194
  42.1 4.6 %collective-permute-start.6 = (bf16[144,512]{1,0:T(8,128)(2,1)S(1)}, bf16[144,512]{1,0:T(8,128)(2,1)S(1)}, u32[]{:S(2)}, u32[]{:S(2)}) collective-permute-start(bf16[144,512]{1,0:T(8,128)(2,1)S(1)} %get-tuple-element.41), channel_id=1, source_target_pairs={{0,16},{4,20},{8,24},{12,28},{1,17},{5,21},{9,25},{13,29},{2,18},{... | collective-permute-start | bytes 442376 | tf_op jit(solution)/shard_map/ppermute | solution.py:511
  46.8 1.3 collective-permute-start.7
  48.7 2.7 %shard_map.191.within_ref = f32[512,512]{1,0:T(8,128)S(1)} custom-call(bf16[512,512]{1,0:T(8,128)(2,1)S(1)} %multiply_convert_fusion.values_ref, bf16[512,256]{1,0:T(8,128)(2,1)S(1)} %multiply_convert_fusion.2.inputs_ref, bf16[512,256]{1,0:T(8,128)(2,1)S(1)} %multiply_convert_fusion.1.readout_ref, f32[3,8,512]{2,1,0:T(8,128)S(1)} %get-tuple-element.30.rows_ref, ...), custom_call_target="tpu_custom_call" | custom-call | tf_op jit(solution)/shard_map/pallas_call | solution.py:377
  51.4 4.6 %collective-permute-done.7.refs_1_ = bf16[144,512]{1,0:T(8,128)(2,1)S(1)} collective-permute-done((bf16[144,512]{1,0:T(8,128)(2,1)S(1)}, bf16[144,512]{1,0:T(8,128)(2,1)S(1)}, u32[]{:S(2)}, u32[]{:S(2)}) %collective-permute-start.7) | collective-permute-done | bytes 147488 | tf_op jit(solution)/shard_map/ppermute | solution.py:512
  56.1 2.8 %shard_map.196 = (bf16[512,1024]{1,0:T(8,128)(2,1)S(1)}, bf16[512,1024]{1,0:T(8,128)(2,1)S(1)}) custom-call(s32[24]{0:T(128)S(1)} %get-tuple-element.76.info_ref.refs_0_, f32[512,512]{1,0:T(8,128)S(1)} %shard_map.191.within_ref, bf16[512,256]{1,0:T(8,128)(2,1)S(1)} %multiply_convert_fusion.1.readout_ref, f32[2,512,8]{2,1,0:T(8,128)S(1)} %get-tuple-element.31.cols_ref, ...), custom_call_target="tpu_custom_call" | custom-call | tf_op jit(solution)/shard_map/pallas_call | solution.py:377
  58.9 2.6 %collective-permute-done.8 = bf16[512,1024]{1,0:T(8,128)(2,1)S(1)} collective-permute-done((bf16[512,1024]{1,0:T(8,128)(2,1)S(1)}, bf16[512,1024]{1,0:T(8,128)(2,1)S(1)}, u32[]{:S(2)}, u32[]{:S(2)}) %collective-permute-start.8) | collective-permute-done | bytes 1048608 | tf_op jit(solution)/shard_map/ppermute | solution.py:48
  62.1 1.5 collective-permute-start.9
  63.8 2.0 collective-permute-start.37
  65.9 8.5 %collective-permute-done.28.refs_4_ = bf16[640,256]{1,0:T(8,128)(2,1)S(1)} collective-permute-done((bf16[640,256]{1,0:T(8,128)(2,1)S(1)}, bf16[640,256]{1,0:T(8,128)(2,1)S(1)}, u32[]{:S(2)}, u32[]{:S(2)}) %collective-permute-start.28) | collective-permute-done | bytes 327712 | tf_op jit(solution)/shard_map/ppermute | solution.py:410
  75.0 6.4 %collective-permute-done.31.refs_5_ = bf16[640,256]{1,0:T(8,128)(2,1)S(1)} collective-permute-done((bf16[640,256]{1,0:T(8,128)(2,1)S(1)}, bf16[640,256]{1,0:T(8,128)(2,1)S(1)}, u32[]{:S(2)}, u32[]{:S(2)}) %collective-permute-start.31) | collective-permute-done | bytes 327712 | tf_op jit(solution)/shard_map/ppermute | solution.py:410
  81.4 2.0 collective-permute-start.18
  83.6 15.3 %collective-permute-done.34.refs_6_ = bf16[640,256]{1,0:T(8,128)(2,1)S(1)} collective-permute-done((bf16[640,256]{1,0:T(8,128)(2,1)S(1)}, bf16[640,256]{1,0:T(8,128)(2,1)S(1)}, u32[]{:S(2)}, u32[]{:S(2)}) %collective-permute-start.34) | collective-permute-done | bytes 327712 | tf_op jit(solution)/shard_map/ppermute | solution.py:410
  99.5 2.0 collective-permute-start.21
  101.5 11.5 %collective-permute-done.13.refs_7_ = bf16[256,1280]{1,0:T(8,128)(2,1)S(1)} collective-permute-done((bf16[256,1280]{1,0:T(8,128)(2,1)S(1)}, bf16[256,1280]{1,0:T(8,128)(2,1)S(1)}, u32[]{:S(2)}, u32[]{:S(2)}) %collective-permute-start.13) | collective-permute-done | bytes 655392 | tf_op jit(solution)/shard_map/ppermute | solution.py:410
  113.0 2.0 collective-permute-start.15
  115.2 15.3 %collective-permute-done.29.refs_8_ = bf16[640,256]{1,0:T(8,128)(2,1)S(1)} collective-permute-done((bf16[640,256]{1,0:T(8,128)(2,1)S(1)}, bf16[640,256]{1,0:T(8,128)(2,1)S(1)}, u32[]{:S(2)}, u32[]{:S(2)}) %collective-permute-start.29) | collective-permute-done | bytes 327712 | tf_op jit(solution)/shard_map/ppermute | solution.py:410
  130.5 2.0 collective-permute-start.23
  132.5 8.5 %collective-permute-done.15.refs_9_ = bf16[256,1280]{1,0:T(8,128)(2,1)S(1)} collective-permute-done((bf16[256,1280]{1,0:T(8,128)(2,1)S(1)}, bf16[256,1280]{1,0:T(8,128)(2,1)S(1)}, u32[]{:S(2)}, u32[]{:S(2)}) %collective-permute-start.15) | collective-permute-done | bytes 655392 | tf_op jit(solution)/shard_map/ppermute | solution.py:410
  141.1 3.5 %collective-permute-done.20.refs_15_ = bf16[256,1280]{1,0:T(8,128)(2,1)S(1)} collective-permute-done((bf16[256,1280]{1,0:T(8,128)(2,1)S(1)}, bf16[256,1280]{1,0:T(8,128)(2,1)S(1)}, u32[]{:S(2)}, u32[]{:S(2)}) %collective-permute-start.20) | collective-permute-done | bytes 655392 | tf_op jit(solution)/shard_map/ppermute | solution.py:410
  144.6 14.0 %collective-permute-done.16.refs_10_ = bf16[256,1280]{1,0:T(8,128)(2,1)S(1)} collective-permute-done((bf16[256,1280]{1,0:T(8,128)(2,1)S(1)}, bf16[256,1280]{1,0:T(8,128)(2,1)S(1)}, u32[]{:S(2)}, u32[]{:S(2)}) %collective-permute-start.16) | collective-permute-done | bytes 655392 | tf_op jit(solution)/shard_map/ppermute | solution.py:410
  158.6 2.0 collective-permute-start.25
  160.6 8.6 %collective-permute-done.17.refs_11_ = bf16[256,1280]{1,0:T(8,128)(2,1)S(1)} collective-permute-done((bf16[256,1280]{1,0:T(8,128)(2,1)S(1)}, bf16[256,1280]{1,0:T(8,128)(2,1)S(1)}, u32[]{:S(2)}, u32[]{:S(2)}) %collective-permute-start.17) | collective-permute-done | bytes 655392 | tf_op jit(solution)/shard_map/ppermute | solution.py:410
  169.2 3.5 %collective-permute-done.22.refs_17_ = bf16[256,1280]{1,0:T(8,128)(2,1)S(1)} collective-permute-done((bf16[256,1280]{1,0:T(8,128)(2,1)S(1)}, bf16[256,1280]{1,0:T(8,128)(2,1)S(1)}, u32[]{:S(2)}, u32[]{:S(2)}) %collective-permute-start.22) | collective-permute-done | bytes 655392 | tf_op jit(solution)/shard_map/ppermute | solution.py:410
  172.7 2.0 collective-permute-start.35
  174.8 6.8 %shard_map.197 = (f32[512,1280]{1,0:T(8,128)S(1)}, f32[512,1280]{1,0:T(8,128)S(1)}, bf16[512,256]{1,0:T(8,128)(2,1)S(1)}) custom-call(s32[24]{0:T(128)S(1)} %get-tuple-element.76.info_ref.refs_0_, f32[1,2048]{1,0:T(1,128)S(1)} %bitcast.33, bf16[512,512]{1,0:T(8,128)(2,1)S(1)} %fusion.10.refs_2_, bf16[512,512]{1,0:T(8,128)(2,1)S(1)} %collective-permute-done.10.refs_3_, ...), custom_call_target="tpu_custom_call" | custom-call | tf_op jit(solution)/shard_map/pallas_call | solution.py:377
  181.6 8.6 %collective-permute-done.38.refs_11_ = bf16[640,256]{1,0:T(8,128)(2,1)S(1)} collective-permute-done((bf16[640,256]{1,0:T(8,128)(2,1)S(1)}, bf16[640,256]{1,0:T(8,128)(2,1)S(1)}, u32[]{:S(2)}, u32[]{:S(2)}) %collective-permute-start.38) | collective-permute-done | bytes 327712 | tf_op jit(solution)/shard_map/ppermute | solution.py:410
  190.3 3.5 %collective-permute-done.32.refs_9_ = bf16[640,256]{1,0:T(8,128)(2,1)S(1)} collective-permute-done((bf16[640,256]{1,0:T(8,128)(2,1)S(1)}, bf16[640,256]{1,0:T(8,128)(2,1)S(1)}, u32[]{:S(2)}, u32[]{:S(2)}) %collective-permute-start.32) | collective-permute-done | bytes 327712 | tf_op jit(solution)/shard_map/ppermute | solution.py:410
  194.2 1.6 collective-permute-start.33
  196.2 0.8 shard_map.198
  197.1 3.5 %collective-permute-start.26 = (bf16[1,2560]{1,0:T(2,128)(2,1)S(1)}, bf16[1,2560]{1,0:T(2,128)(2,1)S(1)}, u32[]{:S(2)}, u32[]{:S(2)}) collective-permute-start(bf16[1,2560]{1,0:T(2,128)(2,1)S(1)} %pad_maximum_fusion.1), channel_id=1, source_target_pairs={{0,4},{4,8},{8,12},{12,16},{16,20},{20,24},{24,28},{1,5},{5,9},{9,... | collective-permute-start | bytes 15368 | tf_op jit(solution)/shard_map/ppermute | solution.py:370
  200.6 4.0 %collective-permute-done.26 = bf16[1,2560]{1,0:T(2,128)(2,1)S(1)} collective-permute-done((bf16[1,2560]{1,0:T(2,128)(2,1)S(1)}, bf16[1,2560]{1,0:T(2,128)(2,1)S(1)}, u32[]{:S(2)}, u32[]{:S(2)}) %collective-permute-start.26) | collective-permute-done | bytes 5152 | tf_op jit(solution)/shard_map/ppermute | solution.py:370
  204.7 1.3 collective-permute-start.27
  206.0 4.7 %collective-permute-done.27 = bf16[1,2560]{1,0:T(2,128)(2,1)S(1)} collective-permute-done((bf16[1,2560]{1,0:T(2,128)(2,1)S(1)}, bf16[1,2560]{1,0:T(2,128)(2,1)S(1)}, u32[]{:S(2)}, u32[]{:S(2)}) %collective-permute-start.27) | collective-permute-done | bytes 5152 | tf_op jit(solution)/shard_map/ppermute | solution.py:371
  211.3 2.1 fusion.2.refs_1_.hidden_ref
  213.4 5.1 %shard_map.199 = (bf16[512,1024]{1,0:T(8,128)(2,1)S(1)}, bf16[512,1024]{1,0:T(8,128)(2,1)S(1)}) custom-call(s32[24]{0:T(128)S(1)} %get-tuple-element.76.info_ref.refs_0_, bf16[512,1280]{1,0:T(8,128)(2,1)S(1)} %fusion.2.refs_1_.hidden_ref, bf16[640,256]{1,0:T(8,128)(2,1)S(1)} %get-tuple-element.68.refs_2_, bf16[640,256]{1,0:T(8,128)(2,1)S(1)} %get-tuple-element.67.refs_3_, ...), custom_call_target="tpu_custom_call" | custom-call | tf_op jit(solution)/shard_map/pallas_call | solution.py:377
  218.6 2.7 %shard_map.200 = (bf16[512,1024]{1,0:T(8,128)(2,1)S(1)}, bf16[512,1024]{1,0:T(8,128)(2,1)S(1)}) custom-call(s32[24]{0:T(128)S(1)} %get-tuple-element.76.info_ref.refs_0_, bf16[512,1280]{1,0:T(8,128)(2,1)S(1)} %fusion.2.refs_1_.hidden_ref, bf16[640,256]{1,0:T(8,128)(2,1)S(1)} %collective-permute-done.30.refs_2_, ...), custom_call_target="tpu_custom_call" | custom-call | tf_op jit(solution)/shard_map/pallas_call | solution.py:377
  221.4 3.0 %collective-permute-start.42 = (bf16[640,256]{1,0:T(8,128)(2,1)S(1)}, bf16[640,256]{1,0:T(8,128)(2,1)S(1)}, u32[]{:S(2)}, u32[]{:S(2)}) collective-permute-start(bf16[640,256]{1,0:T(8,128)(2,1)S(1)} %collective-permute-done.30.refs_2_), channel_id=1, source_target_pairs={{4,12},{12,20},{20,28},{28,24},{24,16},{16,8},{8,0},{0,4},{5,13},{... | collective-permute-start | bytes 983048 | tf_op jit(solution)/shard_map/ppermute | solution.py:410
  224.3 7.6 %collective-permute-done.42.top_ref = bf16[640,256]{1,0:T(8,128)(2,1)S(1)} collective-permute-done((bf16[640,256]{1,0:T(8,128)(2,1)S(1)}, bf16[640,256]{1,0:T(8,128)(2,1)S(1)}, u32[]{:S(2)}, u32[]{:S(2)}) %collective-permute-start.42) | collective-permute-done | bytes 327712 | tf_op jit(solution)/shard_map/ppermute | solution.py:410
  231.9 2.2 collective-permute-done.43.bottom_ref
  234.7 1.3 collective-permute-start.44
  236.0 1.1 collective-permute-done.44
  238.3 0.9 collective-permute-start.41
  240.6 11.4 %collective-permute-done.41 = bf16[512,512]{1,0:T(8,128)(2,1)S(1)} collective-permute-done((bf16[512,512]{1,0:T(8,128)(2,1)S(1)}, bf16[512,512]{1,0:T(8,128)(2,1)S(1)}, u32[]{:S(2)}, u32[]{:S(2)}) %collective-permute-start.41) | collective-permute-done | bytes 524320 | tf_op jit(solution)/shard_map/ppermute | solution.py:48
  252.0 1.1 fusion.8
  (108 shorter events, 10.6 us)
Async XLA Ops:
  1.5 11.6 %collective-permute-start = (bf16[3,1024]{1,0:T(4,128)(2,1)S(1)}, bf16[3,1024]{1,0:T(4,128)(2,1)S(1)}, u32[]{:S(2)}, u32[]{:S(2)}) collective-permute-start(bf16[3,1024]{1,0:T(4,128)(2,1)S(1)} %pad_maximum_fusion.3), channel_id=1, source_target_pairs={{0,4},{4,8},{8,12},{12,16},{16,20},{20,24},{24,28},{1,5},{5,9},{9,... | collective-permute-start | bytes 18440 | tf_op jit(solution)/shard_map/ppermute | solution.py:370
  6.4 6.7 %collective-permute-start.1 = (bf16[3,1024]{1,0:T(4,128)(2,1)S(1)}, bf16[3,1024]{1,0:T(4,128)(2,1)S(1)}, u32[]{:S(2)}, u32[]{:S(2)}) collective-permute-start(bf16[3,1024]{1,0:T(4,128)(2,1)S(1)} %pad_maximum_fusion.4), channel_id=1, source_target_pairs={{4,0},{8,4},{12,8},{16,12},{20,16},{24,20},{28,24},{5,1},{9,5},{13... | collective-permute-start | bytes 18440 | tf_op jit(solution)/shard_map/ppermute | solution.py:371
  10.4 0.8 copy-start.4
  11.2 0.8 copy-start.5
  17.0 6.3 %copy-start.13 = (f32[7,256]{1,0:T(8,128)S(1)}, f32[7,256]{1,0:T(8,128)}, u32[]{:S(2)}) copy-start(f32[7,256]{1,0:T(8,128)} %param.30) | copy-start | bytes 21508
  17.0 19.2 %copy-start.10 = (bf16[512,256]{1,0:T(8,128)(2,1)S(1)}, bf16[512,256]{1,0:T(8,128)(2,1)}, u32[]{:S(2)}) copy-start(bf16[512,256]{1,0:T(8,128)(2,1)} %param.24) | copy-start | bytes 786436
  17.4 7.2 %collective-permute-start.2 = (bf16[144,512]{1,0:T(8,128)(2,1)S(1)}, bf16[144,512]{1,0:T(8,128)(2,1)S(1)}, u32[]{:S(2)}, u32[]{:S(2)}) collective-permute-start(bf16[144,512]{1,0:T(8,128)(2,1)S(1)} %get-tuple-element.34), channel_id=1, source_target_pairs={{0,4},{4,8},{8,12},{12,16},{16,20},{20,24},{24,28},{1,5},{5,9},{9,... | collective-permute-start | bytes 442376 | tf_op jit(solution)/shard_map/ppermute | solution.py:511
  22.0 7.4 %collective-permute-start.3 = (bf16[144,512]{1,0:T(8,128)(2,1)S(1)}, bf16[144,512]{1,0:T(8,128)(2,1)S(1)}, u32[]{:S(2)}, u32[]{:S(2)}) collective-permute-start(bf16[144,512]{1,0:T(8,128)(2,1)S(1)} %get-tuple-element.35), channel_id=1, source_target_pairs={{4,0},{8,4},{12,8},{16,12},{20,16},{24,20},{28,24},{5,1},{9,5},{13... | collective-permute-start | bytes 442376 | tf_op jit(solution)/shard_map/ppermute | solution.py:512
  29.6 7.5 %collective-permute-start.4 = (bf16[144,512]{1,0:T(8,128)(2,1)S(1)}, bf16[144,512]{1,0:T(8,128)(2,1)S(1)}, u32[]{:S(2)}, u32[]{:S(2)}) collective-permute-start(bf16[144,512]{1,0:T(8,128)(2,1)S(1)} %get-tuple-element.37), channel_id=1, source_target_pairs={{0,8},{4,12},{8,16},{12,20},{16,24},{20,28},{1,9},{5,13},{9,17},{1... | collective-permute-start | bytes 442376 | tf_op jit(solution)/shard_map/ppermute | solution.py:511
  34.2 7.0 %collective-permute-start.5 = (bf16[144,512]{1,0:T(8,128)(2,1)S(1)}, bf16[144,512]{1,0:T(8,128)(2,1)S(1)}, u32[]{:S(2)}, u32[]{:S(2)}) collective-permute-start(bf16[144,512]{1,0:T(8,128)(2,1)S(1)} %get-tuple-element.38), channel_id=1, source_target_pairs={{8,0},{12,4},{16,8},{20,12},{24,16},{28,20},{9,1},{13,5},{17,9},{2... | collective-permute-start | bytes 442376 | tf_op jit(solution)/shard_map/ppermute | solution.py:512
  42.1 9.2 %collective-permute-start.6 = (bf16[144,512]{1,0:T(8,128)(2,1)S(1)}, bf16[144,512]{1,0:T(8,128)(2,1)S(1)}, u32[]{:S(2)}, u32[]{:S(2)}) collective-permute-start(bf16[144,512]{1,0:T(8,128)(2,1)S(1)} %get-tuple-element.41), channel_id=1, source_target_pairs={{0,16},{4,20},{8,24},{12,28},{1,17},{5,21},{9,25},{13,29},{2,18},{... | collective-permute-start | bytes 442376 | tf_op jit(solution)/shard_map/ppermute | solution.py:511
  46.8 9.2 %collective-permute-start.7 = (bf16[144,512]{1,0:T(8,128)(2,1)S(1)}, bf16[144,512]{1,0:T(8,128)(2,1)S(1)}, u32[]{:S(2)}, u32[]{:S(2)}) collective-permute-start(bf16[144,512]{1,0:T(8,128)(2,1)S(1)} %get-tuple-element.42), channel_id=1, source_target_pairs={{16,0},{20,4},{24,8},{28,12},{17,1},{21,5},{25,9},{29,13},{18,2},{... | collective-permute-start | bytes 442376 | tf_op jit(solution)/shard_map/ppermute | solution.py:512
  48.6 7.5 %copy-start = (bf16[512,2048]{1,0:T(8,128)(2,1)S(1)}, bf16[512,2048]{1,0:T(8,128)(2,1)}, u32[]{:S(2)}) copy-start(bf16[512,2048]{1,0:T(8,128)(2,1)} %map_ref.1) | copy-start | bytes 6291460
  48.6 7.4 %copy-start.3 = (bf16[512,512]{1,0:T(8,128)(2,1)S(1)}, bf16[512,512]{1,0:T(8,128)(2,1)}, u32[]{:S(2)}) copy-start(bf16[512,512]{1,0:T(8,128)(2,1)} %valve_ref.1) | copy-start | bytes 1572868
  48.6 7.4 %copy-start.7 = (f32[512]{0:T(512)S(1)}, f32[512]{0:T(512)}, u32[]{:S(2)}) copy-start(f32[512]{0:T(512)} %param.31) | copy-start | bytes 6148
  58.9 2.7 %collective-permute-start.8 = (bf16[512,1024]{1,0:T(8,128)(2,1)S(1)}, bf16[512,1024]{1,0:T(8,128)(2,1)S(1)}, u32[]{:S(2)}, u32[]{:S(2)}) collective-permute-start(bf16[512,1024]{1,0:T(8,128)(2,1)S(1)} %get-tuple-element.45), channel_id=1, source_target_pairs={{0,1},{1,0},{2,3},{3,2},{4,5},{5,4},{6,7},{7,6},{8,9},{9,8},{10,11... | collective-permute-start | bytes 3145736 | tf_op jit(solution)/shard_map/ppermute | solution.py:48
  61.6 2.0 copy-start.8
  61.6 4.3 %copy-start.1 = (bf16[256,1280]{1,0:T(8,128)(2,1)S(1)}, bf16[256,1280]{1,0:T(8,128)(2,1)}, u32[]{:S(2)}) copy-start(bf16[256,1280]{1,0:T(8,128)(2,1)} %refs_5_.1) | copy-start | bytes 1966084
  61.6 12.7 %copy-start.2 = (bf16[256,1280]{1,0:T(8,128)(2,1)S(1)}, bf16[256,1280]{1,0:T(8,128)(2,1)}, u32[]{:S(2)}) copy-start(bf16[256,1280]{1,0:T(8,128)(2,1)} %refs_12_.1) | copy-start | bytes 1966084
  61.6 21.8 %copy-start.9 = (bf16[512,512]{1,0:T(8,128)(2,1)S(1)}, bf16[512,512]{1,0:T(8,128)(2,1)}, u32[]{:S(2)}) copy-start(bf16[512,512]{1,0:T(8,128)(2,1)} %param.20) | copy-start | bytes 1572868
  62.1 19.3 %collective-permute-start.9 = (bf16[512,512]{1,0:T(8,128)(2,1)S(1)}, bf16[512,512]{1,0:T(8,128)(2,1)S(1)}, u32[]{:S(2)}, u32[]{:S(2)}) collective-permute-start(bf16[512,512]{1,0:T(8,128)(2,1)S(1)} %slice.526), channel_id=1, source_target_pairs={{0,2},{1,3},{2,0},{3,1},{4,6},{5,7},{6,4},{7,5},{8,10},{9,11},{10,... | collective-permute-start | bytes 1572872 | tf_op jit(solution)/shard_map/ppermute | solution.py:48
  63.7 111.0 %copy-start.11 = (f32[3,1280]{1,0:T(4,128)S(1)}, f32[3,1280]{1,0:T(4,128)}, u32[]{:S(2)}) copy-start(f32[3,1280]{1,0:T(4,128)} %param.37) | copy-start | bytes 46084
  63.7 111.0 %copy-start.12 = (f32[3,1280]{1,0:T(4,128)S(1)}, f32[3,1280]{1,0:T(4,128)}, u32[]{:S(2)}) copy-start(f32[3,1280]{1,0:T(4,128)} %param.36) | copy-start | bytes 46084
  63.7 111.1 %copy-start.6 = (f32[2048]{0:T(1024)S(1)}, f32[2048]{0:T(1024)}, u32[]{:S(2)}) copy-start(f32[2048]{0:T(1024)} %param.33) | copy-start | bytes 24580
  63.7 10.6 %collective-permute-start.28 = (bf16[640,256]{1,0:T(8,128)(2,1)S(1)}, bf16[640,256]{1,0:T(8,128)(2,1)S(1)}, u32[]{:S(2)}, u32[]{:S(2)}) collective-permute-start(bf16[640,256]{1,0:T(8,128)(2,1)S(1)} %get-tuple-element.68.refs_2_), channel_id=1, source_target_pairs={{4,12},{12,20},{20,28},{28,24},{24,16},{16,8},{8,0},{0,4},{5,13},{... | collective-permute-start | bytes 983048 | tf_op jit(solution)/shard_map/ppermute | solution.py:410
  63.8 10.6 %collective-permute-start.37 = (bf16[640,256]{1,0:T(8,128)(2,1)S(1)}, bf16[640,256]{1,0:T(8,128)(2,1)S(1)}, u32[]{:S(2)}, u32[]{:S(2)}) collective-permute-start(bf16[640,256]{1,0:T(8,128)(2,1)S(1)} %get-tuple-element.67.refs_3_), channel_id=1, source_target_pairs={{12,4},{20,12},{28,20},{24,28},{16,24},{8,16},{0,8},{4,0},{13,5},{... | collective-permute-start | bytes 983048 | tf_op jit(solution)/shard_map/ppermute | solution.py:410
  65.8 15.6 %collective-permute-start.31 = (bf16[640,256]{1,0:T(8,128)(2,1)S(1)}, bf16[640,256]{1,0:T(8,128)(2,1)S(1)}, u32[]{:S(2)}, u32[]{:S(2)}) collective-permute-start(bf16[640,256]{1,0:T(8,128)(2,1)S(1)} %get-tuple-element.67.refs_3_), channel_id=1, source_target_pairs={{4,12},{12,20},{20,28},{28,24},{24,16},{16,8},{8,0},{0,4},{5,13},{... | collective-permute-start | bytes 983048 | tf_op jit(solution)/shard_map/ppermute | solution.py:410
  65.8 33.7 %collective-permute-start.12 = (bf16[256,1280]{1,0:T(8,128)(2,1)S(1)}, bf16[256,1280]{1,0:T(8,128)(2,1)S(1)}, u32[]{:S(2)}, u32[]{:S(2)}) collective-permute-start(bf16[256,1280]{1,0:T(8,128)(2,1)S(1)} %copy-done.1), channel_id=1, source_target_pairs={{4,12},{12,20},{20,28},{28,24},{24,16},{16,8},{8,0},{0,4},{5,13},{... | collective-permute-start | bytes 1966088 | tf_op jit(solution)/shard_map/ppermute | solution.py:410
  74.3 25.2 %collective-permute-start.19 = (bf16[256,1280]{1,0:T(8,128)(2,1)S(1)}, bf16[256,1280]{1,0:T(8,128)(2,1)S(1)}, u32[]{:S(2)}, u32[]{:S(2)}) collective-permute-start(bf16[256,1280]{1,0:T(8,128)(2,1)S(1)} %copy-done.2), channel_id=1, source_target_pairs={{12,4},{20,12},{28,20},{24,28},{16,24},{8,16},{0,8},{4,0},{13,5},{... | collective-permute-start | bytes 1966088 | tf_op jit(solution)/shard_map/ppermute | solution.py:410
  74.3 24.6 %collective-permute-start.34 = (bf16[640,256]{1,0:T(8,128)(2,1)S(1)}, bf16[640,256]{1,0:T(8,128)(2,1)S(1)}, u32[]{:S(2)}, u32[]{:S(2)}) collective-permute-start(bf16[640,256]{1,0:T(8,128)(2,1)S(1)} %get-tuple-element.68.refs_2_), channel_id=1, source_target_pairs={{12,4},{20,12},{28,20},{24,28},{16,24},{8,16},{0,8},{4,0},{13,5},{... | collective-permute-start | bytes 983048 | tf_op jit(solution)/shard_map/ppermute | solution.py:410
  81.4 31.7 %collective-permute-start.13 = (bf16[256,1280]{1,0:T(8,128)(2,1)S(1)}, bf16[256,1280]{1,0:T(8,128)(2,1)S(1)}, u32[]{:S(2)}, u32[]{:S(2)}) collective-permute-start(bf16[256,1280]{1,0:T(8,128)(2,1)S(1)} %copy-done.1), channel_id=1, source_target_pairs={{12,4},{20,12},{28,20},{24,28},{16,24},{8,16},{0,8},{4,0},{13,5},{... | collective-permute-start | bytes 1966088 | tf_op jit(solution)/shard_map/ppermute | solution.py:410
  81.4 31.7 %collective-permute-start.18 = (bf16[256,1280]{1,0:T(8,128)(2,1)S(1)}, bf16[256,1280]{1,0:T(8,128)(2,1)S(1)}, u32[]{:S(2)}, u32[]{:S(2)}) collective-permute-start(bf16[256,1280]{1,0:T(8,128)(2,1)S(1)} %copy-done.2), channel_id=1, source_target_pairs={{4,12},{12,20},{20,28},{28,24},{24,16},{16,8},{8,0},{0,4},{5,13},{... | collective-permute-start | bytes 1966088 | tf_op jit(solution)/shard_map/ppermute | solution.py:410
  99.0 16.1 %collective-permute-start.10 = (bf16[512,512]{1,0:T(8,128)(2,1)S(1)}, bf16[512,512]{1,0:T(8,128)(2,1)S(1)}, u32[]{:S(2)}, u32[]{:S(2)}) collective-permute-start(bf16[512,512]{1,0:T(8,128)(2,1)S(1)} %fusion.10.refs_2_), channel_id=1, source_target_pairs={{0,2},{1,3},{2,0},{3,1},{4,6},{5,7},{6,4},{7,5},{8,10},{9,11},{10,... | collective-permute-start | bytes 1572872 | tf_op jit(solution)/shard_map/ppermute | solution.py:48
  99.5 31.0 %collective-permute-start.14 = (bf16[256,1280]{1,0:T(8,128)(2,1)S(1)}, bf16[256,1280]{1,0:T(8,128)(2,1)S(1)}, u32[]{:S(2)}, u32[]{:S(2)}) collective-permute-start(bf16[256,1280]{1,0:T(8,128)(2,1)S(1)} %collective-permute-done.12.refs_6_), channel_id=1, source_target_pairs={{4,12},{12,20},{20,28},{28,24},{24,16},{16,8},{8,0},{0,4},{5,13},{... | collective-permute-start | bytes 1966088 | tf_op jit(solution)/shard_map/ppermute | solution.py:410
  99.5 31.0 %collective-permute-start.21 = (bf16[256,1280]{1,0:T(8,128)(2,1)S(1)}, bf16[256,1280]{1,0:T(8,128)(2,1)S(1)}, u32[]{:S(2)}, u32[]{:S(2)}) collective-permute-start(bf16[256,1280]{1,0:T(8,128)(2,1)S(1)} %collective-permute-done.19.refs_14_), channel_id=1, source_target_pairs={{12,4},{20,12},{28,20},{24,28},{16,24},{8,16},{0,8},{4,0},{13,5},{... | collective-permute-start | bytes 1966088 | tf_op jit(solution)/shard_map/ppermute | solution.py:410
  113.0 17.5 %collective-permute-start.29 = (bf16[640,256]{1,0:T(8,128)(2,1)S(1)}, bf16[640,256]{1,0:T(8,128)(2,1)S(1)}, u32[]{:S(2)}, u32[]{:S(2)}) collective-permute-start(bf16[640,256]{1,0:T(8,128)(2,1)S(1)} %collective-permute-done.28.refs_4_), channel_id=1, source_target_pairs={{4,12},{12,20},{20,28},{28,24},{24,16},{16,8},{8,0},{0,4},{5,13},{... | collective-permute-start | bytes 983048 | tf_op jit(solution)/shard_map/ppermute | solution.py:410
  113.0 28.1 %collective-permute-start.15 = (bf16[256,1280]{1,0:T(8,128)(2,1)S(1)}, bf16[256,1280]{1,0:T(8,128)(2,1)S(1)}, u32[]{:S(2)}, u32[]{:S(2)}) collective-permute-start(bf16[256,1280]{1,0:T(8,128)(2,1)S(1)} %collective-permute-done.13.refs_7_), channel_id=1, source_target_pairs={{12,4},{20,12},{28,20},{24,28},{16,24},{8,16},{0,8},{4,0},{13,5},{... | collective-permute-start | bytes 1966088 | tf_op jit(solution)/shard_map/ppermute | solution.py:410
  115.0 29.5 %collective-permute-start.20 = (bf16[256,1280]{1,0:T(8,128)(2,1)S(1)}, bf16[256,1280]{1,0:T(8,128)(2,1)S(1)}, u32[]{:S(2)}, u32[]{:S(2)}) collective-permute-start(bf16[256,1280]{1,0:T(8,128)(2,1)S(1)} %collective-permute-done.18.refs_13_), channel_id=1, source_target_pairs={{4,12},{12,20},{20,28},{28,24},{24,16},{16,8},{8,0},{0,4},{5,13},{... | collective-permute-start | bytes 1966088 | tf_op jit(solution)/shard_map/ppermute | solution.py:410
  130.5 42.1 %collective-permute-start.11 = (bf16[512,1024]{1,0:T(8,128)(2,1)S(1)}, bf16[512,1024]{1,0:T(8,128)(2,1)S(1)}, u32[]{:S(2)}, u32[]{:S(2)}) collective-permute-start(bf16[512,1024]{1,0:T(8,128)(2,1)S(1)} %pad_maximum_fusion), channel_id=1, source_target_pairs={{0,1},{1,0},{2,3},{3,2},{4,5},{5,4},{6,7},{7,6},{8,9},{9,8},{10,11... | collective-permute-start | bytes 3145736 | tf_op jit(solution)/shard_map/ppermute | solution.py:48
  130.5 28.1 %collective-permute-start.16 = (bf16[256,1280]{1,0:T(8,128)(2,1)S(1)}, bf16[256,1280]{1,0:T(8,128)(2,1)S(1)}, u32[]{:S(2)}, u32[]{:S(2)}) collective-permute-start(bf16[256,1280]{1,0:T(8,128)(2,1)S(1)} %collective-permute-done.14.refs_8_), channel_id=1, source_target_pairs={{4,12},{12,20},{20,28},{28,24},{24,16},{16,8},{8,0},{0,4},{5,13},{... | collective-permute-start | bytes 1966088 | tf_op jit(solution)/shard_map/ppermute | solution.py:410
  130.5 28.1 %collective-permute-start.23 = (bf16[256,1280]{1,0:T(8,128)(2,1)S(1)}, bf16[256,1280]{1,0:T(8,128)(2,1)S(1)}, u32[]{:S(2)}, u32[]{:S(2)}) collective-permute-start(bf16[256,1280]{1,0:T(8,128)(2,1)S(1)} %collective-permute-done.21.refs_16_), channel_id=1, source_target_pairs={{12,4},{20,12},{28,20},{24,28},{16,24},{8,16},{0,8},{4,0},{13,5},{... | collective-permute-start | bytes 1966088 | tf_op jit(solution)/shard_map/ppermute | solution.py:410
  141.1 28.1 %collective-permute-start.17 = (bf16[256,1280]{1,0:T(8,128)(2,1)S(1)}, bf16[256,1280]{1,0:T(8,128)(2,1)S(1)}, u32[]{:S(2)}, u32[]{:S(2)}) collective-permute-start(bf16[256,1280]{1,0:T(8,128)(2,1)S(1)} %collective-permute-done.15.refs_9_), channel_id=1, source_target_pairs={{12,4},{20,12},{28,20},{24,28},{16,24},{8,16},{0,8},{4,0},{13,5},{... | collective-permute-start | bytes 1966088 | tf_op jit(solution)/shard_map/ppermute | solution.py:410
  144.6 28.1 %collective-permute-start.22 = (bf16[256,1280]{1,0:T(8,128)(2,1)S(1)}, bf16[256,1280]{1,0:T(8,128)(2,1)S(1)}, u32[]{:S(2)}, u32[]{:S(2)}) collective-permute-start(bf16[256,1280]{1,0:T(8,128)(2,1)S(1)} %collective-permute-done.20.refs_15_), channel_id=1, source_target_pairs={{4,12},{12,20},{20,28},{28,24},{24,16},{16,8},{8,0},{0,4},{5,13},{... | collective-permute-start | bytes 1966088 | tf_op jit(solution)/shard_map/ppermute | solution.py:410
  158.6 37.1 %collective-permute-start.24 = (bf16[256,1280]{1,0:T(8,128)(2,1)S(1)}, bf16[256,1280]{1,0:T(8,128)(2,1)S(1)}, u32[]{:S(2)}, u32[]{:S(2)}) collective-permute-start(bf16[256,1280]{1,0:T(8,128)(2,1)S(1)} %collective-permute-done.16.refs_10_), channel_id=1, source_target_pairs={{4,12},{12,20},{20,28},{28,24},{24,16},{16,8},{8,0},{0,4},{5,13},{... | collective-permute-start | bytes 1966088 | tf_op jit(solution)/shard_map/ppermute | solution.py:410
  158.6 37.6 %collective-permute-start.25 = (bf16[256,1280]{1,0:T(8,128)(2,1)S(1)}, bf16[256,1280]{1,0:T(8,128)(2,1)S(1)}, u32[]{:S(2)}, u32[]{:S(2)}) collective-permute-start(bf16[256,1280]{1,0:T(8,128)(2,1)S(1)} %collective-permute-done.23.refs_18_), channel_id=1, source_target_pairs={{12,4},{20,12},{28,20},{24,28},{16,24},{8,16},{0,8},{4,0},{13,5},{... | collective-permute-start | bytes 1966088 | tf_op jit(solution)/shard_map/ppermute | solution.py:410
  169.2 21.1 %collective-permute-start.38 = (bf16[640,256]{1,0:T(8,128)(2,1)S(1)}, bf16[640,256]{1,0:T(8,128)(2,1)S(1)}, u32[]{:S(2)}, u32[]{:S(2)}) collective-permute-start(bf16[640,256]{1,0:T(8,128)(2,1)S(1)} %collective-permute-done.37.refs_7_), channel_id=1, source_target_pairs={{12,4},{20,12},{28,20},{24,28},{16,24},{8,16},{0,8},{4,0},{13,5},{... | collective-permute-start | bytes 983048 | tf_op jit(solution)/shard_map/ppermute | solution.py:410
  172.6 21.1 %collective-permute-start.32 = (bf16[640,256]{1,0:T(8,128)(2,1)S(1)}, bf16[640,256]{1,0:T(8,128)(2,1)S(1)}, u32[]{:S(2)}, u32[]{:S(2)}) collective-permute-start(bf16[640,256]{1,0:T(8,128)(2,1)S(1)} %collective-permute-done.31.refs_5_), channel_id=1, source_target_pairs={{4,12},{12,20},{20,28},{28,24},{24,16},{16,8},{8,0},{0,4},{5,13},{... | collective-permute-start | bytes 983048 | tf_op jit(solution)/shard_map/ppermute | solution.py:410
  172.7 21.5 %collective-permute-start.35 = (bf16[640,256]{1,0:T(8,128)(2,1)S(1)}, bf16[640,256]{1,0:T(8,128)(2,1)S(1)}, u32[]{:S(2)}, u32[]{:S(2)}) collective-permute-start(bf16[640,256]{1,0:T(8,128)(2,1)S(1)} %collective-permute-done.34.refs_6_), channel_id=1, source_target_pairs={{12,4},{20,12},{28,20},{24,28},{16,24},{8,16},{0,8},{4,0},{13,5},{... | collective-permute-start | bytes 983048 | tf_op jit(solution)/shard_map/ppermute | solution.py:410
  190.2 28.3 %collective-permute-start.30 = (bf16[640,256]{1,0:T(8,128)(2,1)S(1)}, bf16[640,256]{1,0:T(8,128)(2,1)S(1)}, u32[]{:S(2)}, u32[]{:S(2)}) collective-permute-start(bf16[640,256]{1,0:T(8,128)(2,1)S(1)} %collective-permute-done.29.refs_8_), channel_id=1, source_target_pairs={{4,12},{12,20},{20,28},{28,24},{24,16},{16,8},{8,0},{0,4},{5,13},{... | collective-permute-start | bytes 983048 | tf_op jit(solution)/shard_map/ppermute | solution.py:410
  193.7 24.8 %collective-permute-start.39 = (bf16[640,256]{1,0:T(8,128)(2,1)S(1)}, bf16[640,256]{1,0:T(8,128)(2,1)S(1)}, u32[]{:S(2)}, u32[]{:S(2)}) collective-permute-start(bf16[640,256]{1,0:T(8,128)(2,1)S(1)} %collective-permute-done.38.refs_11_), channel_id=1, source_target_pairs={{12,4},{20,12},{28,20},{24,28},{16,24},{8,16},{0,8},{4,0},{13,5},{... | collective-permute-start | bytes 983048 | tf_op jit(solution)/shard_map/ppermute | solution.py:410
  194.2 24.4 %collective-permute-start.33 = (bf16[640,256]{1,0:T(8,128)(2,1)S(1)}, bf16[640,256]{1,0:T(8,128)(2,1)S(1)}, u32[]{:S(2)}, u32[]{:S(2)}) collective-permute-start(bf16[640,256]{1,0:T(8,128)(2,1)S(1)} %collective-permute-done.32.refs_9_), channel_id=1, source_target_pairs={{4,12},{12,20},{20,28},{28,24},{24,16},{16,8},{8,0},{0,4},{5,13},{... | collective-permute-start | bytes 983048 | tf_op jit(solution)/shard_map/ppermute | solution.py:410
  195.7 22.8 %collective-permute-start.36 = (bf16[640,256]{1,0:T(8,128)(2,1)S(1)}, bf16[640,256]{1,0:T(8,128)(2,1)S(1)}, u32[]{:S(2)}, u32[]{:S(2)}) collective-permute-start(bf16[640,256]{1,0:T(8,128)(2,1)S(1)} %collective-permute-done.35.refs_10_), channel_id=1, source_target_pairs={{12,4},{20,12},{28,20},{24,28},{16,24},{8,16},{0,8},{4,0},{13,5},{... | collective-permute-start | bytes 983048 | tf_op jit(solution)/shard_map/ppermute | solution.py:410
  197.1 7.5 %collective-permute-start.26 = (bf16[1,2560]{1,0:T(2,128)(2,1)S(1)}, bf16[1,2560]{1,0:T(2,128)(2,1)S(1)}, u32[]{:S(2)}, u32[]{:S(2)}) collective-permute-start(bf16[1,2560]{1,0:T(2,128)(2,1)S(1)} %pad_maximum_fusion.1), channel_id=1, source_target_pairs={{0,4},{4,8},{8,12},{12,16},{16,20},{20,24},{24,28},{1,5},{5,9},{9,... | collective-permute-start | bytes 15368 | tf_op jit(solution)/shard_map/ppermute | solution.py:370
  204.7 6.0 %collective-permute-start.27 = (bf16[1,2560]{1,0:T(2,128)(2,1)S(1)}, bf16[1,2560]{1,0:T(2,128)(2,1)S(1)}, u32[]{:S(2)}, u32[]{:S(2)}) collective-permute-start(bf16[1,2560]{1,0:T(2,128)(2,1)S(1)} %pad_maximum_fusion.2), channel_id=1, source_target_pairs={{4,0},{8,4},{12,8},{16,12},{20,16},{24,20},{28,24},{5,1},{9,5},{13... | collective-permute-start | bytes 15368 | tf_op jit(solution)/shard_map/ppermute | solution.py:371
  221.3 16.6 %collective-permute-start.40 = (bf16[512,1024]{1,0:T(8,128)(2,1)S(1)}, bf16[512,1024]{1,0:T(8,128)(2,1)S(1)}, u32[]{:S(2)}, u32[]{:S(2)}) collective-permute-start(bf16[512,1024]{1,0:T(8,128)(2,1)S(1)} %get-tuple-element.54), channel_id=1, source_target_pairs={{0,1},{1,0},{2,3},{3,2},{4,5},{5,4},{6,7},{7,6},{8,9},{9,8},{10,11... | collective-permute-start | bytes 3145736 | tf_op jit(solution)/shard_map/ppermute | solution.py:48
  221.4 10.5 %collective-permute-start.42 = (bf16[640,256]{1,0:T(8,128)(2,1)S(1)}, bf16[640,256]{1,0:T(8,128)(2,1)S(1)}, u32[]{:S(2)}, u32[]{:S(2)}) collective-permute-start(bf16[640,256]{1,0:T(8,128)(2,1)S(1)} %collective-permute-done.30.refs_2_), channel_id=1, source_target_pairs={{4,12},{12,20},{20,28},{28,24},{24,16},{16,8},{8,0},{0,4},{5,13},{... | collective-permute-start | bytes 983048 | tf_op jit(solution)/shard_map/ppermute | solution.py:410
  224.3 9.8 %collective-permute-start.43 = (bf16[640,256]{1,0:T(8,128)(2,1)S(1)}, bf16[640,256]{1,0:T(8,128)(2,1)S(1)}, u32[]{:S(2)}, u32[]{:S(2)}) collective-permute-start(bf16[640,256]{1,0:T(8,128)(2,1)S(1)} %collective-permute-done.39.refs_5_), channel_id=1, source_target_pairs={{12,4},{20,12},{28,20},{24,28},{16,24},{8,16},{0,8},{4,0},{13,5},{... | collective-permute-start | bytes 983048 | tf_op jit(solution)/shard_map/ppermute | solution.py:410
  234.7 2.4 collective-permute-start.44
  237.2 3.3 %collective-permute-start.45 = (bf16[512,256]{1,0:T(8,128)(2,1)S(1)}, bf16[512,256]{1,0:T(8,128)(2,1)S(1)}, u32[]{:S(2)}, u32[]{:S(2)}) collective-permute-start(bf16[512,256]{1,0:T(8,128)(2,1)S(1)} %fusion.29), channel_id=1, source_target_pairs={{1,3},{5,7},{8,10},{12,14},{19,17},{23,21},{26,24},{30,28}} | collective-permute-start | bytes 786440 | tf_op jit(solution)/shard_map/ppermute | solution.py:627
  238.3 13.7 %collective-permute-start.41 = (bf16[512,512]{1,0:T(8,128)(2,1)S(1)}, bf16[512,512]{1,0:T(8,128)(2,1)S(1)}, u32[]{:S(2)}, u32[]{:S(2)}) collective-permute-start(bf16[512,512]{1,0:T(8,128)(2,1)S(1)} %slice.525), channel_id=1, source_target_pairs={{0,2},{1,3},{2,0},{3,1},{4,6},{5,7},{6,4},{7,5},{8,10},{9,11},{10,... | collective-permute-start | bytes 1572872 | tf_op jit(solution)/shard_map/ppermute | solution.py:48

commit v3 on v2

--- a/solution.py
+++ b/solution.py
@@ -313,33 +313,36 @@
             out[:, at] = (held[:, at] + term).astype(jnp.bfloat16)
 
 
-def down_kernel(sizes, plan, blank, n_arrays, *refs):
+def down_kernel(sizes, plan, n_arrays, *refs):
     info_ref, hidden_ref = refs[:2]
     arrays = refs[2 : 2 + n_arrays]
-    held = refs[2 + n_arrays : -2]
-    outs = refs[-2:]
-    half = outs[0].shape[1]
-    for held_ref, out_ref in zip(held, outs):
-        out_ref[...] = held_ref[...]
-
-    def put(source, term):
-        at = info_ref[sizes[0] + source]
-        for side in range(2):
-
-            @pl.when((at >= half) if side else (at < half))
-            def _():
-                columns = pl.ds(pl.multiple_of(at - side * half, term.shape[1]), term.shape[1])
-                outs[side][:, columns] = term
-
+    out_ref = refs[-1]
     for source, parts in plan:
         term = down_term(hidden_ref, [(arrays[array], row) for array, row in parts])
-        if term.shape[1] == 2 * half:
-            outs[0][...] = term[:, :half]
-            outs[1][...] = term[:, half:]
-        else:
-            put(source, term)
-    if blank is not None:
-        put(blank, jnp.zeros_like(term))
+        out_ref[info_ref[sizes[0] + source] // term.shape[1]] = term
+
+
+def down_last_kernel(sizes, plan, blank, rows, n_arrays, *refs):
+    info_ref, hidden_ref, held_ref = refs[:3]
+    arrays = refs[3 : 3 + n_arrays]
+    outs = refs[-2:]
+    count, _, chunk = held_ref.shape
+    spots = [info_ref[sizes[0] + source] // chunk for source, _ in plan]
+    terms = [down_term(hidden_ref.at[rows], [(arrays[array], row) for array, row in parts]) for _, parts in plan]
+    spots.append(info_ref[sizes[0] + blank] // chunk)
+    terms.append(jnp.zeros_like(terms[0]))
+    for p in range(count):
+        value = held_ref[p, rows]
+        for spot, term in zip(spots, terms):
+            value = jnp.where(spot == p, term, value)
+        side, at = divmod(p * chunk, outs[0].shape[1])
+        outs[side][:, at : at + chunk] = value
+
+
+def down_whole_kernel(hidden_ref, map_ref, send_ref, keep_ref):
+    half = send_ref.shape[1]
+    for out_ref, first in ((send_ref, 0), (keep_ref, half)):
+        out_ref[...] = down_term(hidden_ref, [(map_ref.at[:, first : first + half], 0)])
 
 
 def down_term(hidden_ref, parts):
@@ -580,24 +583,14 @@
         value = smooth(value_rows, low[:, hidden_cols:], high[:, hidden_cols:], payload_series_smoother)
         hidden = (jax.nn.silu(gate) * value).astype(jnp.bfloat16)
 
-        def down(plan, blank, arrays, held=()):
-            return call(
-                functools.partial(down_kernel, (sp_count, tp_count), plan, blank, len(arrays)),
-                [((length, half_full), jnp.bfloat16)] * 2,
-                info,
-                hidden,
-                *arrays,
-                *held,
-                scalars=1,
-            )
-
+        halves = [((length, half_full), jnp.bfloat16)] * 2
         if chunk % 128:
             whole = jnp.zeros((hidden_cols, full), jnp.bfloat16)
             for part, entries in enumerate(down_rings):
                 for steps, array, _ in entries:
                     corner = (part * half_row, info[sp_count + steps % sp_count])
                     whole = lax.dynamic_update_slice(whole, array, corner)
-            send, keep = down([(0, [(0, 0)])], None, [whole])
+            send, keep = call(down_whole_kernel, halves, hidden, whole)
             down_sum = tp.reduce_scatter(send, keep)
             return (middle.astype(jnp.float32) + down_sum).astype(jnp.bfloat16)
 
@@ -606,13 +599,28 @@
             (steps % sp_count, (top, bottom)) for (steps, top, _), (_, bottom, _) in zip(*down_rings) if abs(steps) < far
         ]
 
-        def part_of(chunks, blank, held=()):
+        def part_of(kernel, chunks, outs, *given):
             plan = [(slot, [(2 * n, 0), (2 * n + 1, half_row)]) for n, (slot, _) in enumerate(chunks)]
-            return down(plan, blank, [array for _, both_parts in chunks for array in both_parts], held)
-
-        early = part_of(pairs[:-2], None)
-        send, keep = part_of(pairs[-2:], far, early)
-        down_sum = tp.reduce_scatter(send, keep)
+            arrays = [array for _, both_parts in chunks for array in both_parts]
+            return call(kernel(plan, len(arrays)), outs, info, hidden, *given, *arrays, scalars=1)
+
+        sizes = (sp_count, tp_count)
+        (early,) = part_of(
+            lambda plan, count: functools.partial(down_kernel, sizes, plan, count),
+            pairs[:-2],
+            [((sp_count, length, chunk), jnp.bfloat16)],
+        )
+        sums = []
+        for band in range(2):
+            rows = slice(band * length // 2, (band + 1) * length // 2)
+            send, keep = part_of(
+                lambda plan, count: functools.partial(down_last_kernel, sizes, plan, far, rows, count),
+                pairs[-2:],
+                [((length // 2, half_full), jnp.bfloat16)] * 2,
+                early,
+            )
+            sums.append(tp.reduce_scatter(send, keep))
+        down_sum = jnp.concatenate(sums, axis=0)
         (part,) = call(
             far_kernel, [((length, chunk), jnp.bfloat16)], hidden, *(entries[-1][1] for entries in down_rings)
         )

time: 256 us -> 253 us (0.988)
  waiting for transfers between devices: 157 us -> 151 us
  starting transfers between devices: 53.7 us -> 58.6 us
  Pallas kernels: 24.2 us -> 21.6 us
    ppermute x28, waiting for transfers between devices: 117 us -> 114 us  [send_on(): return lax.ppermute(array, 'sp', pairs)]
    pallas_call x12 -> x13, Pallas kernels: 24.2 us -> 21.6 us  [call(): pl.pallas_call(kernel, out_shape=[jax.ShapeDtypeStruct(shape, kind) for s...]
    ppermute x6 -> x8, waiting for transfers between devices: 14.1 us -> 14 us  [swap(): lax.ppermute(array, 'tp', [(i, i ^ 1 << bit) for i in range(self.count)])]
  transfers between devices with their start and end apart: 46 -> 48, of which waited for: 25 -> 22; matrix products, arithmetic and copies ran while one was open for 3% -> 3% of each run, Pallas kernels for 7% -> 7%
where the time goes in v3:
time: 253 us; the launch traced here: 250 us
  waiting for transfers between devices  151 us (60%)
  starting transfers between devices  58.6 us (23%)
  Pallas kernels  21.6 us (9%)
  other arithmetic  9.57 us (4%)
  local copies, waits for them, and re-layouts  7.38 us (3%)
    ppermute x28, waiting for transfers between devices, send_on(): return lax.ppermute(array, 'sp', pairs)  114 us
    ppermute x28, starting transfers between devices, send_on(): return lax.ppermute(array, 'sp', pairs)  21.7 us
    pallas_call x13, Pallas kernels, call(): pl.pallas_call(kernel, out_shape=[jax.ShapeDtypeStruct(shape, kind) for s...  21.6 us
    ppermute x8, waiting for transfers between devices, swap(): lax.ppermute(array, 'tp', [(i, i ^ 1 << bit) for i in range(self.count)])  14 us
    ppermute x3, starting transfers between devices, shards(): got_f = lax.ppermute(send_f, 'sp', forward)  13.8 us
    ppermute x3, waiting for transfers between devices, shards(): got_b = lax.ppermute(send_b, 'sp', [(b, a) for a, b in forward])  13.6 us
    ppermute x2, starting transfers between devices, edges(): low = lax.ppermute(last, 'sp', forward)  8.55 us
  transfers between devices with their start and end apart: 48, of which 22 were waited for; matrix products, arithmetic and copies ran while one was open for 3% of the time, Pallas kernels for 7%

profile of v3, /device:TPU:0, one launch (start us, length us, event | category | flops | bytes accessed | tf_op | source)
XLA Modules:
  0.0 249.6 jit_solution(16902707340205447190)
XLA Ops:
  1.5 4.9 %collective-permute-start = (bf16[3,1024]{1,0:T(4,128)(2,1)S(1)}, bf16[3,1024]{1,0:T(4,128)(2,1)S(1)}, u32[]{:S(2)}, u32[]{:S(2)}) collective-permute-start(bf16[3,1024]{1,0:T(4,128)(2,1)S(1)} %pad_maximum_fusion.3), channel_id=1, source_target_pairs={{0,4},{4,8},{8,12},{12,16},{16,20},{20,24},{24,28},{1,5},{5,9},{9,... | collective-permute-start | bytes 18440 | tf_op jit(solution)/shard_map/ppermute | solution.py:373
  6.4 1.3 collective-permute-start.1
  7.7 1.0 fusion.38
  8.7 1.0 fusion.44
  9.7 0.8 copy.21
  10.4 0.8 copy-done.4
  11.2 0.8 copy-done.5
  11.9 1.2 shard_map.190
  13.1 1.0 maximum_convert_fusion.3
  14.2 1.2 maximum_convert_fusion.2
  15.9 1.1 multiply_convert_fusion.values_ref
  17.4 4.6 %collective-permute-start.2 = (bf16[144,512]{1,0:T(8,128)(2,1)S(1)}, bf16[144,512]{1,0:T(8,128)(2,1)S(1)}, u32[]{:S(2)}, u32[]{:S(2)}) collective-permute-start(bf16[144,512]{1,0:T(8,128)(2,1)S(1)} %get-tuple-element.34), channel_id=1, source_target_pairs={{0,4},{4,8},{8,12},{12,16},{16,20},{20,24},{24,28},{1,5},{5,9},{9,... | collective-permute-start | bytes 442376 | tf_op jit(solution)/shard_map/ppermute | solution.py:514
  22.0 1.3 collective-permute-start.3
  23.3 1.3 collective-permute-done.2.refs_0_
  24.6 4.8 %collective-permute-done.3.refs_1_ = bf16[144,512]{1,0:T(8,128)(2,1)S(1)} collective-permute-done((bf16[144,512]{1,0:T(8,128)(2,1)S(1)}, bf16[144,512]{1,0:T(8,128)(2,1)S(1)}, u32[]{:S(2)}, u32[]{:S(2)}) %collective-permute-start.3) | collective-permute-done | bytes 147488 | tf_op jit(solution)/shard_map/ppermute | solution.py:515
  29.6 4.6 %collective-permute-start.4 = (bf16[144,512]{1,0:T(8,128)(2,1)S(1)}, bf16[144,512]{1,0:T(8,128)(2,1)S(1)}, u32[]{:S(2)}, u32[]{:S(2)}) collective-permute-start(bf16[144,512]{1,0:T(8,128)(2,1)S(1)} %get-tuple-element.37), channel_id=1, source_target_pairs={{0,8},{4,12},{8,16},{12,20},{16,24},{20,28},{1,9},{5,13},{9,17},{1... | collective-permute-start | bytes 442376 | tf_op jit(solution)/shard_map/ppermute | solution.py:514
  34.2 1.3 collective-permute-start.5
  36.2 0.8 collective-permute-done.4.refs_0_
  37.1 4.1 %collective-permute-done.5.refs_1_ = bf16[144,512]{1,0:T(8,128)(2,1)S(1)} collective-permute-done((bf16[144,512]{1,0:T(8,128)(2,1)S(1)}, bf16[144,512]{1,0:T(8,128)(2,1)S(1)}, u32[]{:S(2)}, u32[]{:S(2)}) %collective-permute-start.5) | collective-permute-done | bytes 147488 | tf_op jit(solution)/shard_map/ppermute | solution.py:515
  41.2 0.9 shard_map.194
  42.1 4.6 %collective-permute-start.6 = (bf16[144,512]{1,0:T(8,128)(2,1)S(1)}, bf16[144,512]{1,0:T(8,128)(2,1)S(1)}, u32[]{:S(2)}, u32[]{:S(2)}) collective-permute-start(bf16[144,512]{1,0:T(8,128)(2,1)S(1)} %get-tuple-element.41), channel_id=1, source_target_pairs={{0,16},{4,20},{8,24},{12,28},{1,17},{5,21},{9,25},{13,29},{2,18},{... | collective-permute-start | bytes 442376 | tf_op jit(solution)/shard_map/ppermute | solution.py:514
  46.8 1.3 collective-permute-start.7
  48.6 2.7 %shard_map.191.within_ref = f32[512,512]{1,0:T(8,128)S(1)} custom-call(bf16[512,512]{1,0:T(8,128)(2,1)S(1)} %multiply_convert_fusion.values_ref, bf16[512,256]{1,0:T(8,128)(2,1)S(1)} %multiply_convert_fusion.2.inputs_ref, bf16[512,256]{1,0:T(8,128)(2,1)S(1)} %multiply_convert_fusion.1.readout_ref, f32[3,8,512]{2,1,0:T(8,128)S(1)} %get-tuple-element.30.rows_ref, ...), custom_call_target="tpu_custom_call" | custom-call | tf_op jit(solution)/shard_map/pallas_call | solution.py:380
  51.4 4.6 %collective-permute-done.7.refs_1_ = bf16[144,512]{1,0:T(8,128)(2,1)S(1)} collective-permute-done((bf16[144,512]{1,0:T(8,128)(2,1)S(1)}, bf16[144,512]{1,0:T(8,128)(2,1)S(1)}, u32[]{:S(2)}, u32[]{:S(2)}) %collective-permute-start.7) | collective-permute-done | bytes 147488 | tf_op jit(solution)/shard_map/ppermute | solution.py:515
  56.1 2.8 %shard_map.196 = (bf16[512,1024]{1,0:T(8,128)(2,1)S(1)}, bf16[512,1024]{1,0:T(8,128)(2,1)S(1)}) custom-call(s32[24]{0:T(128)S(1)} %get-tuple-element.76.info_ref.refs_0_, f32[512,512]{1,0:T(8,128)S(1)} %shard_map.191.within_ref, bf16[512,256]{1,0:T(8,128)(2,1)S(1)} %multiply_convert_fusion.1.readout_ref, f32[2,512,8]{2,1,0:T(8,128)S(1)} %get-tuple-element.31.cols_ref, ...), custom_call_target="tpu_custom_call" | custom-call | tf_op jit(solution)/shard_map/pallas_call | solution.py:380
  58.9 2.6 %collective-permute-done.8 = bf16[512,1024]{1,0:T(8,128)(2,1)S(1)} collective-permute-done((bf16[512,1024]{1,0:T(8,128)(2,1)S(1)}, bf16[512,1024]{1,0:T(8,128)(2,1)S(1)}, u32[]{:S(2)}, u32[]{:S(2)}) %collective-permute-start.8) | collective-permute-done | bytes 1048608 | tf_op jit(solution)/shard_map/ppermute | solution.py:48
  62.1 1.5 collective-permute-start.9
  63.7 2.0 collective-permute-start.31
  65.9 8.5 %collective-permute-done.28.refs_4_ = bf16[640,256]{1,0:T(8,128)(2,1)S(1)} collective-permute-done((bf16[640,256]{1,0:T(8,128)(2,1)S(1)}, bf16[640,256]{1,0:T(8,128)(2,1)S(1)}, u32[]{:S(2)}, u32[]{:S(2)}) %collective-permute-start.28) | collective-permute-done | bytes 327712 | tf_op jit(solution)/shard_map/ppermute | solution.py:413
  75.0 6.4 %collective-permute-done.29.refs_5_ = bf16[640,256]{1,0:T(8,128)(2,1)S(1)} collective-permute-done((bf16[640,256]{1,0:T(8,128)(2,1)S(1)}, bf16[640,256]{1,0:T(8,128)(2,1)S(1)}, u32[]{:S(2)}, u32[]{:S(2)}) %collective-permute-start.29) | collective-permute-done | bytes 327712 | tf_op jit(solution)/shard_map/ppermute | solution.py:413
  81.3 2.0 collective-permute-start.30
  83.6 26.3 %collective-permute-done.30.refs_6_ = bf16[640,256]{1,0:T(8,128)(2,1)S(1)} collective-permute-done((bf16[640,256]{1,0:T(8,128)(2,1)S(1)}, bf16[640,256]{1,0:T(8,128)(2,1)S(1)}, u32[]{:S(2)}, u32[]{:S(2)}) %collective-permute-start.30) | collective-permute-done | bytes 327712 | tf_op jit(solution)/shard_map/ppermute | solution.py:413
  109.9 1.1 collective-permute-start.10
  111.6 1.5 collective-permute-start.35
  113.6 1.5 collective-permute-start.21
  115.1 6.5 %collective-permute-done.32.refs_8_ = bf16[640,256]{1,0:T(8,128)(2,1)S(1)} collective-permute-done((bf16[640,256]{1,0:T(8,128)(2,1)S(1)}, bf16[640,256]{1,0:T(8,128)(2,1)S(1)}, u32[]{:S(2)}, u32[]{:S(2)}) %collective-permute-start.32) | collective-permute-done | bytes 327712 | tf_op jit(solution)/shard_map/ppermute | solution.py:413
  122.2 1.5 collective-permute-start.15
  124.3 18.3 %collective-permute-done.33.refs_9_ = bf16[640,256]{1,0:T(8,128)(2,1)S(1)} collective-permute-done((bf16[640,256]{1,0:T(8,128)(2,1)S(1)}, bf16[640,256]{1,0:T(8,128)(2,1)S(1)}, u32[]{:S(2)}, u32[]{:S(2)}) %collective-permute-start.33) | collective-permute-done | bytes 327712 | tf_op jit(solution)/shard_map/ppermute | solution.py:413
  143.2 1.5 collective-permute-start.23
  144.7 2.9 %collective-permute-done.15.refs_9_ = bf16[256,1280]{1,0:T(8,128)(2,1)S(1)} collective-permute-done((bf16[256,1280]{1,0:T(8,128)(2,1)S(1)}, bf16[256,1280]{1,0:T(8,128)(2,1)S(1)}, u32[]{:S(2)}, u32[]{:S(2)}) %collective-permute-start.15) | collective-permute-done | bytes 655392 | tf_op jit(solution)/shard_map/ppermute | solution.py:413
  148.0 8.7 %collective-permute-done.20.refs_15_ = bf16[256,1280]{1,0:T(8,128)(2,1)S(1)} collective-permute-done((bf16[256,1280]{1,0:T(8,128)(2,1)S(1)}, bf16[256,1280]{1,0:T(8,128)(2,1)S(1)}, u32[]{:S(2)}, u32[]{:S(2)}) %collective-permute-start.20) | collective-permute-done | bytes 655392 | tf_op jit(solution)/shard_map/ppermute | solution.py:413
  157.3 13.5 %collective-permute-done.16.refs_10_ = bf16[256,1280]{1,0:T(8,128)(2,1)S(1)} collective-permute-done((bf16[256,1280]{1,0:T(8,128)(2,1)S(1)}, bf16[256,1280]{1,0:T(8,128)(2,1)S(1)}, u32[]{:S(2)}, u32[]{:S(2)}) %collective-permute-start.16) | collective-permute-done | bytes 655392 | tf_op jit(solution)/shard_map/ppermute | solution.py:413
  171.3 1.5 collective-permute-start.25
  172.8 2.9 %collective-permute-done.17.refs_11_ = bf16[256,1280]{1,0:T(8,128)(2,1)S(1)} collective-permute-done((bf16[256,1280]{1,0:T(8,128)(2,1)S(1)}, bf16[256,1280]{1,0:T(8,128)(2,1)S(1)}, u32[]{:S(2)}, u32[]{:S(2)}) %collective-permute-start.17) | collective-permute-done | bytes 655392 | tf_op jit(solution)/shard_map/ppermute | solution.py:413
  176.3 8.4 %collective-permute-done.22.refs_17_ = bf16[256,1280]{1,0:T(8,128)(2,1)S(1)} collective-permute-done((bf16[256,1280]{1,0:T(8,128)(2,1)S(1)}, bf16[256,1280]{1,0:T(8,128)(2,1)S(1)}, u32[]{:S(2)}, u32[]{:S(2)}) %collective-permute-start.22) | collective-permute-done | bytes 655392 | tf_op jit(solution)/shard_map/ppermute | solution.py:413
  185.4 1.5 collective-permute-start.39
  186.9 6.8 %shard_map.197 = (f32[512,1280]{1,0:T(8,128)S(1)}, f32[512,1280]{1,0:T(8,128)S(1)}, bf16[512,256]{1,0:T(8,128)(2,1)S(1)}) custom-call(s32[24]{0:T(128)S(1)} %get-tuple-element.76.info_ref.refs_0_, f32[1,2048]{1,0:T(1,128)S(1)} %bitcast.33, bf16[512,512]{1,0:T(8,128)(2,1)S(1)} %fusion.7.refs_2_, bf16[512,512]{1,0:T(8,128)(2,1)S(1)} %collective-permute-done.10.refs_3_, ...), custom_call_target="tpu_custom_call" | custom-call | tf_op jit(solution)/shard_map/pallas_call | solution.py:380
  193.8 3.0 %collective-permute-done.34.refs_10_ = bf16[640,256]{1,0:T(8,128)(2,1)S(1)} collective-permute-done((bf16[640,256]{1,0:T(8,128)(2,1)S(1)}, bf16[640,256]{1,0:T(8,128)(2,1)S(1)}, u32[]{:S(2)}, u32[]{:S(2)}) %collective-permute-start.34) | collective-permute-done | bytes 327712 | tf_op jit(solution)/shard_map/ppermute | solution.py:413
  197.1 8.7 %collective-permute-done.36.refs_3_ = bf16[640,256]{1,0:T(8,128)(2,1)S(1)} collective-permute-done((bf16[640,256]{1,0:T(8,128)(2,1)S(1)}, bf16[640,256]{1,0:T(8,128)(2,1)S(1)}, u32[]{:S(2)}, u32[]{:S(2)}) %collective-permute-start.36) | collective-permute-done | bytes 327712 | tf_op jit(solution)/shard_map/ppermute | solution.py:413
  206.1 1.7 collective-permute-start.44
  208.2 0.8 shard_map.198
  209.1 3.6 %collective-permute-start.26 = (bf16[1,2560]{1,0:T(2,128)(2,1)S(1)}, bf16[1,2560]{1,0:T(2,128)(2,1)S(1)}, u32[]{:S(2)}, u32[]{:S(2)}) collective-permute-start(bf16[1,2560]{1,0:T(2,128)(2,1)S(1)} %pad_maximum_fusion.1), channel_id=1, source_target_pairs={{0,4},{4,8},{8,12},{12,16},{16,20},{20,24},{24,28},{1,5},{5,9},{9,... | collective-permute-start | bytes 15368 | tf_op jit(solution)/shard_map/ppermute | solution.py:373
  212.8 2.3 collective-permute-done.26
  215.1 1.3 collective-permute-start.27
  216.4 4.7 %collective-permute-done.27 = bf16[1,2560]{1,0:T(2,128)(2,1)S(1)} collective-permute-done((bf16[1,2560]{1,0:T(2,128)(2,1)S(1)}, bf16[1,2560]{1,0:T(2,128)(2,1)S(1)}, u32[]{:S(2)}, u32[]{:S(2)}) %collective-permute-start.27) | collective-permute-done | bytes 5152 | tf_op jit(solution)/shard_map/ppermute | solution.py:374
  221.7 2.1 fusion.2.refs_1_.hidden_ref
  223.8 2.7 %shard_map.199.refs_2_ = bf16[8,512,256]{2,1,0:T(8,128)(2,1)S(1)} custom-call(s32[24]{0:T(128)S(1)} %get-tuple-element.76.info_ref.refs_0_, bf16[512,1280]{1,0:T(8,128)(2,1)S(1)} %fusion.2.refs_1_.hidden_ref, bf16[640,256]{1,0:T(8,128)(2,1)S(1)} %get-tuple-element.68.refs_2_, bf16[640,256]{1,0:T(8,128)(2,1)S(1)} %get-tuple-element.67.refs_3_, ...), custom_call_target="tpu_custom_call" | custom-call | tf_op jit(solution)/shard_map/pallas_call | solution.py:380
  226.6 1.3 shard_map.200
  228.5 2.4 collective-permute-start.46
  230.9 1.3 shard_map.201
  235.2 1.7 collective-permute-start.43
  237.0 5.8 %collective-permute-done.41 = bf16[256,512]{1,0:T(8,128)(2,1)S(1)} collective-permute-done((bf16[256,512]{1,0:T(8,128)(2,1)S(1)}, bf16[256,512]{1,0:T(8,128)(2,1)S(1)}, u32[]{:S(2)}, u32[]{:S(2)}) %collective-permute-start.41) | collective-permute-done | bytes 262176 | tf_op jit(solution)/shard_map/ppermute | solution.py:48
  242.9 5.5 %collective-permute-done.43 = bf16[256,512]{1,0:T(8,128)(2,1)S(1)} collective-permute-done((bf16[256,512]{1,0:T(8,128)(2,1)S(1)}, bf16[256,512]{1,0:T(8,128)(2,1)S(1)}, u32[]{:S(2)}, u32[]{:S(2)}) %collective-permute-start.43) | collective-permute-done | bytes 262176 | tf_op jit(solution)/shard_map/ppermute | solution.py:48
  248.6 1.0 fusion.15
  (117 shorter events, 16.0 us)
Async XLA Ops:
  1.5 11.6 %collective-permute-start = (bf16[3,1024]{1,0:T(4,128)(2,1)S(1)}, bf16[3,1024]{1,0:T(4,128)(2,1)S(1)}, u32[]{:S(2)}, u32[]{:S(2)}) collective-permute-start(bf16[3,1024]{1,0:T(4,128)(2,1)S(1)} %pad_maximum_fusion.3), channel_id=1, source_target_pairs={{0,4},{4,8},{8,12},{12,16},{16,20},{20,24},{24,28},{1,5},{5,9},{9,... | collective-permute-start | bytes 18440 | tf_op jit(solution)/shard_map/ppermute | solution.py:373
  6.4 6.7 %collective-permute-start.1 = (bf16[3,1024]{1,0:T(4,128)(2,1)S(1)}, bf16[3,1024]{1,0:T(4,128)(2,1)S(1)}, u32[]{:S(2)}, u32[]{:S(2)}) collective-permute-start(bf16[3,1024]{1,0:T(4,128)(2,1)S(1)} %pad_maximum_fusion.4), channel_id=1, source_target_pairs={{4,0},{8,4},{12,8},{16,12},{20,16},{24,20},{28,24},{5,1},{9,5},{13... | collective-permute-start | bytes 18440 | tf_op jit(solution)/shard_map/ppermute | solution.py:374
  10.4 0.8 copy-start.4
  11.2 0.8 copy-start.5
  17.0 6.3 %copy-start.13 = (f32[7,256]{1,0:T(8,128)S(1)}, f32[7,256]{1,0:T(8,128)}, u32[]{:S(2)}) copy-start(f32[7,256]{1,0:T(8,128)} %param.30) | copy-start | bytes 21508
  17.0 19.2 %copy-start.10 = (bf16[512,256]{1,0:T(8,128)(2,1)S(1)}, bf16[512,256]{1,0:T(8,128)(2,1)}, u32[]{:S(2)}) copy-start(bf16[512,256]{1,0:T(8,128)(2,1)} %param.24) | copy-start | bytes 786436
  17.4 7.2 %collective-permute-start.2 = (bf16[144,512]{1,0:T(8,128)(2,1)S(1)}, bf16[144,512]{1,0:T(8,128)(2,1)S(1)}, u32[]{:S(2)}, u32[]{:S(2)}) collective-permute-start(bf16[144,512]{1,0:T(8,128)(2,1)S(1)} %get-tuple-element.34), channel_id=1, source_target_pairs={{0,4},{4,8},{8,12},{12,16},{16,20},{20,24},{24,28},{1,5},{5,9},{9,... | collective-permute-start | bytes 442376 | tf_op jit(solution)/shard_map/ppermute | solution.py:514
  22.0 7.4 %collective-permute-start.3 = (bf16[144,512]{1,0:T(8,128)(2,1)S(1)}, bf16[144,512]{1,0:T(8,128)(2,1)S(1)}, u32[]{:S(2)}, u32[]{:S(2)}) collective-permute-start(bf16[144,512]{1,0:T(8,128)(2,1)S(1)} %get-tuple-element.35), channel_id=1, source_target_pairs={{4,0},{8,4},{12,8},{16,12},{20,16},{24,20},{28,24},{5,1},{9,5},{13... | collective-permute-start | bytes 442376 | tf_op jit(solution)/shard_map/ppermute | solution.py:515
  29.6 7.5 %collective-permute-start.4 = (bf16[144,512]{1,0:T(8,128)(2,1)S(1)}, bf16[144,512]{1,0:T(8,128)(2,1)S(1)}, u32[]{:S(2)}, u32[]{:S(2)}) collective-permute-start(bf16[144,512]{1,0:T(8,128)(2,1)S(1)} %get-tuple-element.37), channel_id=1, source_target_pairs={{0,8},{4,12},{8,16},{12,20},{16,24},{20,28},{1,9},{5,13},{9,17},{1... | collective-permute-start | bytes 442376 | tf_op jit(solution)/shard_map/ppermute | solution.py:514
  34.2 7.0 %collective-permute-start.5 = (bf16[144,512]{1,0:T(8,128)(2,1)S(1)}, bf16[144,512]{1,0:T(8,128)(2,1)S(1)}, u32[]{:S(2)}, u32[]{:S(2)}) collective-permute-start(bf16[144,512]{1,0:T(8,128)(2,1)S(1)} %get-tuple-element.38), channel_id=1, source_target_pairs={{8,0},{12,4},{16,8},{20,12},{24,16},{28,20},{9,1},{13,5},{17,9},{2... | collective-permute-start | bytes 442376 | tf_op jit(solution)/shard_map/ppermute | solution.py:515
  42.1 9.2 %collective-permute-start.6 = (bf16[144,512]{1,0:T(8,128)(2,1)S(1)}, bf16[144,512]{1,0:T(8,128)(2,1)S(1)}, u32[]{:S(2)}, u32[]{:S(2)}) collective-permute-start(bf16[144,512]{1,0:T(8,128)(2,1)S(1)} %get-tuple-element.41), channel_id=1, source_target_pairs={{0,16},{4,20},{8,24},{12,28},{1,17},{5,21},{9,25},{13,29},{2,18},{... | collective-permute-start | bytes 442376 | tf_op jit(solution)/shard_map/ppermute | solution.py:514
  46.8 9.2 %collective-permute-start.7 = (bf16[144,512]{1,0:T(8,128)(2,1)S(1)}, bf16[144,512]{1,0:T(8,128)(2,1)S(1)}, u32[]{:S(2)}, u32[]{:S(2)}) collective-permute-start(bf16[144,512]{1,0:T(8,128)(2,1)S(1)} %get-tuple-element.42), channel_id=1, source_target_pairs={{16,0},{20,4},{24,8},{28,12},{17,1},{21,5},{25,9},{29,13},{18,2},{... | collective-permute-start | bytes 442376 | tf_op jit(solution)/shard_map/ppermute | solution.py:515
  48.6 7.5 %copy-start = (bf16[512,2048]{1,0:T(8,128)(2,1)S(1)}, bf16[512,2048]{1,0:T(8,128)(2,1)}, u32[]{:S(2)}) copy-start(bf16[512,2048]{1,0:T(8,128)(2,1)} %map_ref.1) | copy-start | bytes 6291460
  48.6 7.4 %copy-start.3 = (bf16[512,512]{1,0:T(8,128)(2,1)S(1)}, bf16[512,512]{1,0:T(8,128)(2,1)}, u32[]{:S(2)}) copy-start(bf16[512,512]{1,0:T(8,128)(2,1)} %valve_ref.1) | copy-start | bytes 1572868
  48.6 7.4 %copy-start.7 = (f32[512]{0:T(512)S(1)}, f32[512]{0:T(512)}, u32[]{:S(2)}) copy-start(f32[512]{0:T(512)} %param.31) | copy-start | bytes 6148
  58.8 2.7 %collective-permute-start.8 = (bf16[512,1024]{1,0:T(8,128)(2,1)S(1)}, bf16[512,1024]{1,0:T(8,128)(2,1)S(1)}, u32[]{:S(2)}, u32[]{:S(2)}) collective-permute-start(bf16[512,1024]{1,0:T(8,128)(2,1)S(1)} %get-tuple-element.45), channel_id=1, source_target_pairs={{0,1},{1,0},{2,3},{3,2},{4,5},{5,4},{6,7},{7,6},{8,9},{9,8},{10,11... | collective-permute-start | bytes 3145736 | tf_op jit(solution)/shard_map/ppermute | solution.py:48
  61.6 2.0 copy-start.8
  61.6 4.3 %copy-start.1 = (bf16[256,1280]{1,0:T(8,128)(2,1)S(1)}, bf16[256,1280]{1,0:T(8,128)(2,1)}, u32[]{:S(2)}) copy-start(bf16[256,1280]{1,0:T(8,128)(2,1)} %refs_5_.1) | copy-start | bytes 1966084
  61.6 12.7 %copy-start.2 = (bf16[256,1280]{1,0:T(8,128)(2,1)S(1)}, bf16[256,1280]{1,0:T(8,128)(2,1)}, u32[]{:S(2)}) copy-start(bf16[256,1280]{1,0:T(8,128)(2,1)} %refs_12_.1) | copy-start | bytes 1966084
  61.6 21.8 %copy-start.9 = (bf16[512,512]{1,0:T(8,128)(2,1)S(1)}, bf16[512,512]{1,0:T(8,128)(2,1)}, u32[]{:S(2)}) copy-start(bf16[512,512]{1,0:T(8,128)(2,1)} %param.20) | copy-start | bytes 1572868
  62.1 19.3 %collective-permute-start.9 = (bf16[512,512]{1,0:T(8,128)(2,1)S(1)}, bf16[512,512]{1,0:T(8,128)(2,1)S(1)}, u32[]{:S(2)}, u32[]{:S(2)}) collective-permute-start(bf16[512,512]{1,0:T(8,128)(2,1)S(1)} %slice.532), channel_id=1, source_target_pairs={{0,2},{1,3},{2,0},{3,1},{4,6},{5,7},{6,4},{7,5},{8,10},{9,11},{10,... | collective-permute-start | bytes 1572872 | tf_op jit(solution)/shard_map/ppermute | solution.py:48
  63.6 123.2 %copy-start.11 = (f32[3,1280]{1,0:T(4,128)S(1)}, f32[3,1280]{1,0:T(4,128)}, u32[]{:S(2)}) copy-start(f32[3,1280]{1,0:T(4,128)} %param.37) | copy-start | bytes 46084
  63.7 123.2 %copy-start.12 = (f32[3,1280]{1,0:T(4,128)S(1)}, f32[3,1280]{1,0:T(4,128)}, u32[]{:S(2)}) copy-start(f32[3,1280]{1,0:T(4,128)} %param.36) | copy-start | bytes 46084
  63.7 123.2 %copy-start.6 = (f32[2048]{0:T(1024)S(1)}, f32[2048]{0:T(1024)}, u32[]{:S(2)}) copy-start(f32[2048]{0:T(1024)} %param.33) | copy-start | bytes 24580
  63.7 10.6 %collective-permute-start.28 = (bf16[640,256]{1,0:T(8,128)(2,1)S(1)}, bf16[640,256]{1,0:T(8,128)(2,1)S(1)}, u32[]{:S(2)}, u32[]{:S(2)}) collective-permute-start(bf16[640,256]{1,0:T(8,128)(2,1)S(1)} %get-tuple-element.68.refs_2_), channel_id=1, source_target_pairs={{4,12},{12,20},{20,28},{28,24},{24,16},{16,8},{8,0},{0,4},{5,13},{... | collective-permute-start | bytes 983048 | tf_op jit(solution)/shard_map/ppermute | solution.py:413
  63.7 10.6 %collective-permute-start.31 = (bf16[640,256]{1,0:T(8,128)(2,1)S(1)}, bf16[640,256]{1,0:T(8,128)(2,1)S(1)}, u32[]{:S(2)}, u32[]{:S(2)}) collective-permute-start(bf16[640,256]{1,0:T(8,128)(2,1)S(1)} %get-tuple-element.67.refs_3_), channel_id=1, source_target_pairs={{12,4},{20,12},{28,20},{24,28},{16,24},{8,16},{0,8},{4,0},{13,5},{... | collective-permute-start | bytes 983048 | tf_op jit(solution)/shard_map/ppermute | solution.py:413
  65.8 15.6 %collective-permute-start.29 = (bf16[640,256]{1,0:T(8,128)(2,1)S(1)}, bf16[640,256]{1,0:T(8,128)(2,1)S(1)}, u32[]{:S(2)}, u32[]{:S(2)}) collective-permute-start(bf16[640,256]{1,0:T(8,128)(2,1)S(1)} %get-tuple-element.67.refs_3_), channel_id=1, source_target_pairs={{4,12},{12,20},{20,28},{28,24},{24,16},{16,8},{8,0},{0,4},{5,13},{... | collective-permute-start | bytes 983048 | tf_op jit(solution)/shard_map/ppermute | solution.py:413
  65.8 45.2 %collective-permute-start.12 = (bf16[256,1280]{1,0:T(8,128)(2,1)S(1)}, bf16[256,1280]{1,0:T(8,128)(2,1)S(1)}, u32[]{:S(2)}, u32[]{:S(2)}) collective-permute-start(bf16[256,1280]{1,0:T(8,128)(2,1)S(1)} %copy-done.1), channel_id=1, source_target_pairs={{4,12},{12,20},{20,28},{28,24},{24,16},{16,8},{8,0},{0,4},{5,13},{... | collective-permute-start | bytes 1966088 | tf_op jit(solution)/shard_map/ppermute | solution.py:413
  74.3 37.3 %collective-permute-start.19 = (bf16[256,1280]{1,0:T(8,128)(2,1)S(1)}, bf16[256,1280]{1,0:T(8,128)(2,1)S(1)}, u32[]{:S(2)}, u32[]{:S(2)}) collective-permute-start(bf16[256,1280]{1,0:T(8,128)(2,1)S(1)} %copy-done.2), channel_id=1, source_target_pairs={{12,4},{20,12},{28,20},{24,28},{16,24},{8,16},{0,8},{4,0},{13,5},{... | collective-permute-start | bytes 1966088 | tf_op jit(solution)/shard_map/ppermute | solution.py:413
  74.3 38.7 %collective-permute-start.13 = (bf16[256,1280]{1,0:T(8,128)(2,1)S(1)}, bf16[256,1280]{1,0:T(8,128)(2,1)S(1)}, u32[]{:S(2)}, u32[]{:S(2)}) collective-permute-start(bf16[256,1280]{1,0:T(8,128)(2,1)S(1)} %copy-done.1), channel_id=1, source_target_pairs={{12,4},{20,12},{28,20},{24,28},{16,24},{8,16},{0,8},{4,0},{13,5},{... | collective-permute-start | bytes 1966088 | tf_op jit(solution)/shard_map/ppermute | solution.py:413
  81.3 32.3 %collective-permute-start.18 = (bf16[256,1280]{1,0:T(8,128)(2,1)S(1)}, bf16[256,1280]{1,0:T(8,128)(2,1)S(1)}, u32[]{:S(2)}, u32[]{:S(2)}) collective-permute-start(bf16[256,1280]{1,0:T(8,128)(2,1)S(1)} %copy-done.2), channel_id=1, source_target_pairs={{4,12},{12,20},{20,28},{28,24},{24,16},{16,8},{8,0},{0,4},{5,13},{... | collective-permute-start | bytes 1966088 | tf_op jit(solution)/shard_map/ppermute | solution.py:413
  81.3 28.6 %collective-permute-start.30 = (bf16[640,256]{1,0:T(8,128)(2,1)S(1)}, bf16[640,256]{1,0:T(8,128)(2,1)S(1)}, u32[]{:S(2)}, u32[]{:S(2)}) collective-permute-start(bf16[640,256]{1,0:T(8,128)(2,1)S(1)} %get-tuple-element.68.refs_2_), channel_id=1, source_target_pairs={{12,4},{20,12},{28,20},{24,28},{16,24},{8,16},{0,8},{4,0},{13,5},{... | collective-permute-start | bytes 983048 | tf_op jit(solution)/shard_map/ppermute | solution.py:413
  109.9 13.7 %collective-permute-start.10 = (bf16[512,512]{1,0:T(8,128)(2,1)S(1)}, bf16[512,512]{1,0:T(8,128)(2,1)S(1)}, u32[]{:S(2)}, u32[]{:S(2)}) collective-permute-start(bf16[512,512]{1,0:T(8,128)(2,1)S(1)} %fusion.7.refs_2_), channel_id=1, source_target_pairs={{0,2},{1,3},{2,0},{3,1},{4,6},{5,7},{6,4},{7,5},{8,10},{9,11},{10,... | collective-permute-start | bytes 1572872 | tf_op jit(solution)/shard_map/ppermute | solution.py:48
  111.0 10.6 %collective-permute-start.32 = (bf16[640,256]{1,0:T(8,128)(2,1)S(1)}, bf16[640,256]{1,0:T(8,128)(2,1)S(1)}, u32[]{:S(2)}, u32[]{:S(2)}) collective-permute-start(bf16[640,256]{1,0:T(8,128)(2,1)S(1)} %collective-permute-done.28.refs_4_), channel_id=1, source_target_pairs={{4,12},{12,20},{20,28},{28,24},{24,16},{16,8},{8,0},{0,4},{5,13},{... | collective-permute-start | bytes 983048 | tf_op jit(solution)/shard_map/ppermute | solution.py:413
  111.6 10.6 %collective-permute-start.35 = (bf16[640,256]{1,0:T(8,128)(2,1)S(1)}, bf16[640,256]{1,0:T(8,128)(2,1)S(1)}, u32[]{:S(2)}, u32[]{:S(2)}) collective-permute-start(bf16[640,256]{1,0:T(8,128)(2,1)S(1)} %collective-permute-done.31.refs_7_), channel_id=1, source_target_pairs={{12,4},{20,12},{28,20},{24,28},{16,24},{8,16},{0,8},{4,0},{13,5},{... | collective-permute-start | bytes 983048 | tf_op jit(solution)/shard_map/ppermute | solution.py:413
  113.0 29.6 %collective-permute-start.14 = (bf16[256,1280]{1,0:T(8,128)(2,1)S(1)}, bf16[256,1280]{1,0:T(8,128)(2,1)S(1)}, u32[]{:S(2)}, u32[]{:S(2)}) collective-permute-start(bf16[256,1280]{1,0:T(8,128)(2,1)S(1)} %collective-permute-done.12.refs_6_), channel_id=1, source_target_pairs={{4,12},{12,20},{20,28},{28,24},{24,16},{16,8},{8,0},{0,4},{5,13},{... | collective-permute-start | bytes 1966088 | tf_op jit(solution)/shard_map/ppermute | solution.py:413
  113.6 29.6 %collective-permute-start.21 = (bf16[256,1280]{1,0:T(8,128)(2,1)S(1)}, bf16[256,1280]{1,0:T(8,128)(2,1)S(1)}, u32[]{:S(2)}, u32[]{:S(2)}) collective-permute-start(bf16[256,1280]{1,0:T(8,128)(2,1)S(1)} %collective-permute-done.19.refs_14_), channel_id=1, source_target_pairs={{12,4},{20,12},{28,20},{24,28},{16,24},{8,16},{0,8},{4,0},{13,5},{... | collective-permute-start | bytes 1966088 | tf_op jit(solution)/shard_map/ppermute | solution.py:413
  121.6 21.1 %collective-permute-start.33 = (bf16[640,256]{1,0:T(8,128)(2,1)S(1)}, bf16[640,256]{1,0:T(8,128)(2,1)S(1)}, u32[]{:S(2)}, u32[]{:S(2)}) collective-permute-start(bf16[640,256]{1,0:T(8,128)(2,1)S(1)} %collective-permute-done.29.refs_5_), channel_id=1, source_target_pairs={{4,12},{12,20},{20,28},{28,24},{24,16},{16,8},{8,0},{0,4},{5,13},{... | collective-permute-start | bytes 983048 | tf_op jit(solution)/shard_map/ppermute | solution.py:413
  122.2 25.5 %collective-permute-start.15 = (bf16[256,1280]{1,0:T(8,128)(2,1)S(1)}, bf16[256,1280]{1,0:T(8,128)(2,1)S(1)}, u32[]{:S(2)}, u32[]{:S(2)}) collective-permute-start(bf16[256,1280]{1,0:T(8,128)(2,1)S(1)} %collective-permute-done.13.refs_7_), channel_id=1, source_target_pairs={{12,4},{20,12},{28,20},{24,28},{16,24},{8,16},{0,8},{4,0},{13,5},{... | collective-permute-start | bytes 1966088 | tf_op jit(solution)/shard_map/ppermute | solution.py:413
  123.6 33.1 %collective-permute-start.20 = (bf16[256,1280]{1,0:T(8,128)(2,1)S(1)}, bf16[256,1280]{1,0:T(8,128)(2,1)S(1)}, u32[]{:S(2)}, u32[]{:S(2)}) collective-permute-start(bf16[256,1280]{1,0:T(8,128)(2,1)S(1)} %collective-permute-done.18.refs_13_), channel_id=1, source_target_pairs={{4,12},{12,20},{20,28},{28,24},{24,16},{16,8},{8,0},{0,4},{5,13},{... | collective-permute-start | bytes 1966088 | tf_op jit(solution)/shard_map/ppermute | solution.py:413
  142.7 42.7 %collective-permute-start.11 = (bf16[512,1024]{1,0:T(8,128)(2,1)S(1)}, bf16[512,1024]{1,0:T(8,128)(2,1)S(1)}, u32[]{:S(2)}, u32[]{:S(2)}) collective-permute-start(bf16[512,1024]{1,0:T(8,128)(2,1)S(1)} %pad_maximum_fusion), channel_id=1, source_target_pairs={{0,1},{1,0},{2,3},{3,2},{4,5},{5,4},{6,7},{7,6},{8,9},{9,8},{10,11... | collective-permute-start | bytes 3145736 | tf_op jit(solution)/shard_map/ppermute | solution.py:48
  142.7 28.1 %collective-permute-start.16 = (bf16[256,1280]{1,0:T(8,128)(2,1)S(1)}, bf16[256,1280]{1,0:T(8,128)(2,1)S(1)}, u32[]{:S(2)}, u32[]{:S(2)}) collective-permute-start(bf16[256,1280]{1,0:T(8,128)(2,1)S(1)} %collective-permute-done.14.refs_8_), channel_id=1, source_target_pairs={{4,12},{12,20},{20,28},{28,24},{24,16},{16,8},{8,0},{0,4},{5,13},{... | collective-permute-start | bytes 1966088 | tf_op jit(solution)/shard_map/ppermute | solution.py:413
  143.2 28.1 %collective-permute-start.23 = (bf16[256,1280]{1,0:T(8,128)(2,1)S(1)}, bf16[256,1280]{1,0:T(8,128)(2,1)S(1)}, u32[]{:S(2)}, u32[]{:S(2)}) collective-permute-start(bf16[256,1280]{1,0:T(8,128)(2,1)S(1)} %collective-permute-done.21.refs_16_), channel_id=1, source_target_pairs={{12,4},{20,12},{28,20},{24,28},{16,24},{8,16},{0,8},{4,0},{13,5},{... | collective-permute-start | bytes 1966088 | tf_op jit(solution)/shard_map/ppermute | solution.py:413
  147.6 28.1 %collective-permute-start.17 = (bf16[256,1280]{1,0:T(8,128)(2,1)S(1)}, bf16[256,1280]{1,0:T(8,128)(2,1)S(1)}, u32[]{:S(2)}, u32[]{:S(2)}) collective-permute-start(bf16[256,1280]{1,0:T(8,128)(2,1)S(1)} %collective-permute-done.15.refs_9_), channel_id=1, source_target_pairs={{12,4},{20,12},{28,20},{24,28},{16,24},{8,16},{0,8},{4,0},{13,5},{... | collective-permute-start | bytes 1966088 | tf_op jit(solution)/shard_map/ppermute | solution.py:413
  156.7 28.1 %collective-permute-start.22 = (bf16[256,1280]{1,0:T(8,128)(2,1)S(1)}, bf16[256,1280]{1,0:T(8,128)(2,1)S(1)}, u32[]{:S(2)}, u32[]{:S(2)}) collective-permute-start(bf16[256,1280]{1,0:T(8,128)(2,1)S(1)} %collective-permute-done.20.refs_15_), channel_id=1, source_target_pairs={{4,12},{12,20},{20,28},{28,24},{24,16},{16,8},{8,0},{0,4},{5,13},{... | collective-permute-start | bytes 1966088 | tf_op jit(solution)/shard_map/ppermute | solution.py:413
  170.7 37.1 %collective-permute-start.24 = (bf16[256,1280]{1,0:T(8,128)(2,1)S(1)}, bf16[256,1280]{1,0:T(8,128)(2,1)S(1)}, u32[]{:S(2)}, u32[]{:S(2)}) collective-permute-start(bf16[256,1280]{1,0:T(8,128)(2,1)S(1)} %collective-permute-done.16.refs_10_), channel_id=1, source_target_pairs={{4,12},{12,20},{20,28},{28,24},{24,16},{16,8},{8,0},{0,4},{5,13},{... | collective-permute-start | bytes 1966088 | tf_op jit(solution)/shard_map/ppermute | solution.py:413
  171.3 36.9 %collective-permute-start.25 = (bf16[256,1280]{1,0:T(8,128)(2,1)S(1)}, bf16[256,1280]{1,0:T(8,128)(2,1)S(1)}, u32[]{:S(2)}, u32[]{:S(2)}) collective-permute-start(bf16[256,1280]{1,0:T(8,128)(2,1)S(1)} %collective-permute-done.23.refs_18_), channel_id=1, source_target_pairs={{12,4},{20,12},{28,20},{24,28},{16,24},{8,16},{0,8},{4,0},{13,5},{... | collective-permute-start | bytes 1966088 | tf_op jit(solution)/shard_map/ppermute | solution.py:413
  175.7 21.1 %collective-permute-start.34 = (bf16[640,256]{1,0:T(8,128)(2,1)S(1)}, bf16[640,256]{1,0:T(8,128)(2,1)S(1)}, u32[]{:S(2)}, u32[]{:S(2)}) collective-permute-start(bf16[640,256]{1,0:T(8,128)(2,1)S(1)} %collective-permute-done.30.refs_6_), channel_id=1, source_target_pairs={{12,4},{20,12},{28,20},{24,28},{16,24},{8,16},{0,8},{4,0},{13,5},{... | collective-permute-start | bytes 983048 | tf_op jit(solution)/shard_map/ppermute | solution.py:413
  184.8 21.1 %collective-permute-start.36 = (bf16[640,256]{1,0:T(8,128)(2,1)S(1)}, bf16[640,256]{1,0:T(8,128)(2,1)S(1)}, u32[]{:S(2)}, u32[]{:S(2)}) collective-permute-start(bf16[640,256]{1,0:T(8,128)(2,1)S(1)} %collective-permute-done.32.refs_8_), channel_id=1, source_target_pairs={{4,12},{12,20},{20,28},{28,24},{24,16},{16,8},{8,0},{0,4},{5,13},{... | collective-permute-start | bytes 983048 | tf_op jit(solution)/shard_map/ppermute | solution.py:413
  185.4 20.8 %collective-permute-start.39 = (bf16[640,256]{1,0:T(8,128)(2,1)S(1)}, bf16[640,256]{1,0:T(8,128)(2,1)S(1)}, u32[]{:S(2)}, u32[]{:S(2)}) collective-permute-start(bf16[640,256]{1,0:T(8,128)(2,1)S(1)} %collective-permute-done.35.refs_11_), channel_id=1, source_target_pairs={{12,4},{20,12},{28,20},{24,28},{16,24},{8,16},{0,8},{4,0},{13,5},{... | collective-permute-start | bytes 983048 | tf_op jit(solution)/shard_map/ppermute | solution.py:413
  196.8 29.8 %collective-permute-start.37 = (bf16[640,256]{1,0:T(8,128)(2,1)S(1)}, bf16[640,256]{1,0:T(8,128)(2,1)S(1)}, u32[]{:S(2)}, u32[]{:S(2)}) collective-permute-start(bf16[640,256]{1,0:T(8,128)(2,1)S(1)} %collective-permute-done.33.refs_9_), channel_id=1, source_target_pairs={{4,12},{12,20},{20,28},{28,24},{24,16},{16,8},{8,0},{0,4},{5,13},{... | collective-permute-start | bytes 983048 | tf_op jit(solution)/shard_map/ppermute | solution.py:413
  205.8 20.7 %collective-permute-start.38 = (bf16[640,256]{1,0:T(8,128)(2,1)S(1)}, bf16[640,256]{1,0:T(8,128)(2,1)S(1)}, u32[]{:S(2)}, u32[]{:S(2)}) collective-permute-start(bf16[640,256]{1,0:T(8,128)(2,1)S(1)} %collective-permute-done.34.refs_10_), channel_id=1, source_target_pairs={{12,4},{20,12},{28,20},{24,28},{16,24},{8,16},{0,8},{4,0},{13,5},{... | collective-permute-start | bytes 983048 | tf_op jit(solution)/shard_map/ppermute | solution.py:413
  206.1 21.8 %collective-permute-start.44 = (bf16[640,256]{1,0:T(8,128)(2,1)S(1)}, bf16[640,256]{1,0:T(8,128)(2,1)S(1)}, u32[]{:S(2)}, u32[]{:S(2)}) collective-permute-start(bf16[640,256]{1,0:T(8,128)(2,1)S(1)} %collective-permute-done.36.refs_3_), channel_id=1, source_target_pairs={{4,12},{12,20},{20,28},{28,24},{24,16},{16,8},{8,0},{0,4},{5,13},{... | collective-permute-start | bytes 983048 | tf_op jit(solution)/shard_map/ppermute | solution.py:413
  207.9 20.1 %collective-permute-start.45 = (bf16[640,256]{1,0:T(8,128)(2,1)S(1)}, bf16[640,256]{1,0:T(8,128)(2,1)S(1)}, u32[]{:S(2)}, u32[]{:S(2)}) collective-permute-start(bf16[640,256]{1,0:T(8,128)(2,1)S(1)} %collective-permute-done.39.refs_6_), channel_id=1, source_target_pairs={{12,4},{20,12},{28,20},{24,28},{16,24},{8,16},{0,8},{4,0},{13,5},{... | collective-permute-start | bytes 983048 | tf_op jit(solution)/shard_map/ppermute | solution.py:413
  209.1 6.0 %collective-permute-start.26 = (bf16[1,2560]{1,0:T(2,128)(2,1)S(1)}, bf16[1,2560]{1,0:T(2,128)(2,1)S(1)}, u32[]{:S(2)}, u32[]{:S(2)}) collective-permute-start(bf16[1,2560]{1,0:T(2,128)(2,1)S(1)} %pad_maximum_fusion.1), channel_id=1, source_target_pairs={{0,4},{4,8},{8,12},{12,16},{16,20},{20,24},{24,28},{1,5},{5,9},{9,... | collective-permute-start | bytes 15368 | tf_op jit(solution)/shard_map/ppermute | solution.py:373
  215.1 6.0 %collective-permute-start.27 = (bf16[1,2560]{1,0:T(2,128)(2,1)S(1)}, bf16[1,2560]{1,0:T(2,128)(2,1)S(1)}, u32[]{:S(2)}, u32[]{:S(2)}) collective-permute-start(bf16[1,2560]{1,0:T(2,128)(2,1)S(1)} %pad_maximum_fusion.2), channel_id=1, source_target_pairs={{4,0},{8,4},{12,8},{16,12},{20,16},{24,20},{28,24},{5,1},{9,5},{13... | collective-permute-start | bytes 15368 | tf_op jit(solution)/shard_map/ppermute | solution.py:374
  227.9 6.4 %collective-permute-start.40 = (bf16[256,1024]{1,0:T(8,128)(2,1)S(1)}, bf16[256,1024]{1,0:T(8,128)(2,1)S(1)}, u32[]{:S(2)}, u32[]{:S(2)}) collective-permute-start(bf16[256,1024]{1,0:T(8,128)(2,1)S(1)} %get-tuple-element.52), channel_id=1, source_target_pairs={{0,1},{1,0},{2,3},{3,2},{4,5},{5,4},{6,7},{7,6},{8,9},{9,8},{10,11... | collective-permute-start | bytes 1572872 | tf_op jit(solution)/shard_map/ppermute | solution.py:48
  228.5 5.0 %collective-permute-start.46 = (bf16[512,256]{1,0:T(8,128)(2,1)S(1)}, bf16[512,256]{1,0:T(8,128)(2,1)S(1)}, u32[]{:S(2)}, u32[]{:S(2)}) collective-permute-start(bf16[512,256]{1,0:T(8,128)(2,1)S(1)} %shard_map.202), channel_id=1, source_target_pairs={{0,1},{2,3},{4,5},{6,7},{9,8},{11,10},{13,12},{15,14},{16,17},{18,... | collective-permute-start | bytes 786440 | tf_op jit(solution)/shard_map/ppermute | solution.py:635
  232.2 2.8 %collective-permute-start.42 = (bf16[256,1024]{1,0:T(8,128)(2,1)S(1)}, bf16[256,1024]{1,0:T(8,128)(2,1)S(1)}, u32[]{:S(2)}, u32[]{:S(2)}) collective-permute-start(bf16[256,1024]{1,0:T(8,128)(2,1)S(1)} %get-tuple-element.54), channel_id=1, source_target_pairs={{0,1},{1,0},{2,3},{3,2},{4,5},{5,4},{6,7},{7,6},{8,9},{9,8},{10,11... | collective-permute-start | bytes 1572872 | tf_op jit(solution)/shard_map/ppermute | solution.py:48
  233.6 3.3 %collective-permute-start.47 = (bf16[512,256]{1,0:T(8,128)(2,1)S(1)}, bf16[512,256]{1,0:T(8,128)(2,1)S(1)}, u32[]{:S(2)}, u32[]{:S(2)}) collective-permute-start(bf16[512,256]{1,0:T(8,128)(2,1)S(1)} %fusion.28), channel_id=1, source_target_pairs={{1,3},{5,7},{8,10},{12,14},{19,17},{23,21},{26,24},{30,28}} | collective-permute-start | bytes 786440 | tf_op jit(solution)/shard_map/ppermute | solution.py:635
  234.5 8.4 %collective-permute-start.41 = (bf16[256,512]{1,0:T(8,128)(2,1)S(1)}, bf16[256,512]{1,0:T(8,128)(2,1)S(1)}, u32[]{:S(2)}, u32[]{:S(2)}) collective-permute-start(bf16[256,512]{1,0:T(8,128)(2,1)S(1)} %slice.534), channel_id=1, source_target_pairs={{0,2},{1,3},{2,0},{3,1},{4,6},{5,7},{6,4},{7,5},{8,10},{9,11},{10,... | collective-permute-start | bytes 786440 | tf_op jit(solution)/shard_map/ppermute | solution.py:48
  235.2 13.3 %collective-permute-start.43 = (bf16[256,512]{1,0:T(8,128)(2,1)S(1)}, bf16[256,512]{1,0:T(8,128)(2,1)S(1)}, u32[]{:S(2)}, u32[]{:S(2)}) collective-permute-start(bf16[256,512]{1,0:T(8,128)(2,1)S(1)} %slice.533), channel_id=1, source_target_pairs={{0,2},{1,3},{2,0},{3,1},{4,6},{5,7},{6,4},{7,5},{8,10},{9,11},{10,... | collective-permute-start | bytes 786440 | tf_op jit(solution)/shard_map/ppermute | solution.py:48

commit v4 on v3

--- a/solution.py
+++ b/solution.py
@@ -11,7 +11,7 @@
 
 STATE = 128
 EPSILON = 1e-06
-TAIL = 16
+TAIL = 8
 LIMIT = 16
 
 
@@ -313,50 +313,46 @@
             out[:, at] = (held[:, at] + term).astype(jnp.bfloat16)
 
 
-def down_kernel(sizes, plan, n_arrays, *refs):
+def down_kernel(sizes, plan, *refs):
     info_ref, hidden_ref = refs[:2]
-    arrays = refs[2 : 2 + n_arrays]
-    out_ref = refs[-1]
-    for source, parts in plan:
-        term = down_term(hidden_ref, [(arrays[array], row) for array, row in parts])
+    arrays, out_ref = refs[2:-1], refs[-1]
+    for n, source in enumerate(plan):
+        term = down_term(hidden_ref, arrays[2 * n : 2 * n + 2])
         out_ref[info_ref[sizes[0] + source] // term.shape[1]] = term
 
 
-def down_last_kernel(sizes, plan, blank, rows, n_arrays, *refs):
+def down_last_kernel(sizes, plan, blank, band, *refs):
     info_ref, hidden_ref, held_ref = refs[:3]
-    arrays = refs[3 : 3 + n_arrays]
-    outs = refs[-2:]
-    count, _, chunk = held_ref.shape
-    spots = [info_ref[sizes[0] + source] // chunk for source, _ in plan]
-    terms = [down_term(hidden_ref.at[rows], [(arrays[array], row) for array, row in parts]) for _, parts in plan]
-    spots.append(info_ref[sizes[0] + blank] // chunk)
+    arrays, outs = refs[3:-2], refs[-2:]
+    count, width = held_ref.shape[0], arrays[0].shape[1]
+    columns = slice(band * width, (band + 1) * width)
+    both_terms = down_term(hidden_ref, arrays)
+    spots = [info_ref[sizes[0] + source] // held_ref.shape[2] for source in plan]
+    terms = [both_terms[:, n * width : (n + 1) * width] for n in range(len(plan))]
+    spots.append(info_ref[sizes[0] + blank] // held_ref.shape[2])
     terms.append(jnp.zeros_like(terms[0]))
     for p in range(count):
-        value = held_ref[p, rows]
+        value = held_ref[p, :, columns]
         for spot, term in zip(spots, terms):
             value = jnp.where(spot == p, term, value)
-        side, at = divmod(p * chunk, outs[0].shape[1])
-        outs[side][:, at : at + chunk] = value
+        side, at = divmod(p * width, outs[0].shape[1])
+        outs[side][:, at : at + width] = value
 
 
 def down_whole_kernel(hidden_ref, map_ref, send_ref, keep_ref):
     half = send_ref.shape[1]
     for out_ref, first in ((send_ref, 0), (keep_ref, half)):
-        out_ref[...] = down_term(hidden_ref, [(map_ref.at[:, first : first + half], 0)])
+        out_ref[...] = down_term(hidden_ref, [map_ref.at[:, first : first + half]])
 
 
 def down_term(hidden_ref, parts):
-    term = None
-    for array, row in parts:
-        part = jnp.dot(
-            hidden_ref[:, row : row + array.shape[0]], array[...], preferred_element_type=jnp.float32
-        )
-        term = part if term is None else term + part
-    return term.astype(jnp.bfloat16)
-
-
-def far_kernel(hidden_ref, top_ref, bottom_ref, out_ref):
-    out_ref[...] = down_term(hidden_ref, [(top_ref, 0), (bottom_ref, top_ref.shape[0])])
+    side_by_side = [part[...] for part in parts]
+    whole = side_by_side[0] if len(parts) == 1 else jnp.concatenate(side_by_side, axis=1)
+    return jnp.dot(hidden_ref[...], whole, preferred_element_type=jnp.float32).astype(jnp.bfloat16)
+
+
+def far_kernel(hidden_ref, left_ref, right_ref, out_ref):
+    out_ref[...] = down_term(hidden_ref, [left_ref, right_ref])
 
 
 def conv_rows(padded, kernel, length):
@@ -470,10 +466,10 @@
         hidden_cols = dense_valve_map.shape[1]
         chunk = dense_valve_map.shape[0]
         up_rings = [[(0, own, 0)] + ring(own, way) for own, way in ((dense_valve_map, "f"), (dense_payload_map, "b"))]
-        half_row = hidden_cols // 2
+        half_col = chunk // 2
         down_rings = [
             [(0, own, 0)] + ring(own, way)
-            for own, way in ((dense_contract_map[:half_row], "f"), (dense_contract_map[half_row:], "b"))
+            for own, way in ((dense_contract_map[:, :half_col], "f"), (dense_contract_map[:, half_col:], "b"))
         ]
         info = jnp.asarray(table(chunk, own_cols))[lax.axis_index("sp") * tp_count + me]
 
@@ -584,43 +580,49 @@
         hidden = (jax.nn.silu(gate) * value).astype(jnp.bfloat16)
 
         halves = [((length, half_full), jnp.bfloat16)] * 2
-        if chunk % 128:
+        if chunk % 256:
             whole = jnp.zeros((hidden_cols, full), jnp.bfloat16)
             for part, entries in enumerate(down_rings):
                 for steps, array, _ in entries:
-                    corner = (part * half_row, info[sp_count + steps % sp_count])
+                    corner = (0, info[sp_count + steps % sp_count] + part * half_col)
                     whole = lax.dynamic_update_slice(whole, array, corner)
             send, keep = call(down_whole_kernel, halves, hidden, whole)
             down_sum = tp.reduce_scatter(send, keep)
             return (middle.astype(jnp.float32) + down_sum).astype(jnp.bfloat16)
 
         far = sp_count // 2
-        pairs = [
-            (steps % sp_count, (top, bottom)) for (steps, top, _), (_, bottom, _) in zip(*down_rings) if abs(steps) < far
-        ]
-
-        def part_of(kernel, chunks, outs, *given):
-            plan = [(slot, [(2 * n, 0), (2 * n + 1, half_row)]) for n, (slot, _) in enumerate(chunks)]
-            arrays = [array for _, both_parts in chunks for array in both_parts]
-            return call(kernel(plan, len(arrays)), outs, info, hidden, *given, *arrays, scalars=1)
-
+        near_steps = [steps for steps, _, _ in down_rings[0][:-1]]
+        held_by = [[array for _, array, _ in entries[:-1]] for entries in down_rings]
+        plan = [steps % sp_count for steps in near_steps]
         sizes = (sp_count, tp_count)
-        (early,) = part_of(
-            lambda plan, count: functools.partial(down_kernel, sizes, plan, count),
-            pairs[:-2],
+        (early,) = call(
+            functools.partial(down_kernel, sizes, plan[:-2]),
             [((sp_count, length, chunk), jnp.bfloat16)],
+            info,
+            hidden,
+            *(array for pair in list(zip(*held_by))[:-2] for array in pair),
+            scalars=1,
         )
         sums = []
         for band in range(2):
-            rows = slice(band * length // 2, (band + 1) * length // 2)
-            send, keep = part_of(
-                lambda plan, count: functools.partial(down_last_kernel, sizes, plan, far, rows, count),
-                pairs[-2:],
-                [((length // 2, half_full), jnp.bfloat16)] * 2,
+            send, keep = call(
+                functools.partial(down_last_kernel, sizes, plan[-2:], far, band),
+                [((length, half_full // 2), jnp.bfloat16)] * 2,
+                info,
+                hidden,
                 early,
+                *held_by[band][-2:],
+                scalars=1,
             )
             sums.append(tp.reduce_scatter(send, keep))
-        down_sum = jnp.concatenate(sums, axis=0)
+        down_sum = jnp.concatenate(
+            [
+                band[:, at : at + half_col]
+                for at in range(0, own_cols // 2, half_col)
+                for band in sums
+            ],
+            axis=1,
+        )
         (part,) = call(
             far_kernel, [((length, chunk), jnp.bfloat16)], hidden, *(entries[-1][1] for entries in down_rings)
         )
@@ -632,7 +634,10 @@
                     apart = t ^ owner
                     if apart >> bit & 1 and apart % (1 << bit) == 0:
                         pairs.append((s * tp_count + t, s * tp_count + (t ^ (1 << bit))))
-            received = lax.ppermute(part.astype(jnp.bfloat16), ("sp", "tp"), pairs)
+            if bit == 0:
+                received = tp.swap(part, bit)
+            else:
+                received = lax.ppermute(part.astype(jnp.bfloat16), ("sp", "tp"), pairs)
             part = part.astype(jnp.float32) + received.astype(jnp.float32)
         at = info[sp_count + far] - (tp_count - 1) * own_cols
         spots = range(0, own_cols, chunk)

time: 253 us -> 249 us (0.984)
  waiting for transfers between devices: 151 us -> 147 us
    ppermute x28, waiting for transfers between devices: 114 us -> 108 us  [send_on(): return lax.ppermute(array, 'sp', pairs)]
    ppermute x28, starting transfers between devices: 21.7 us -> 25.6 us  [send_on(): return lax.ppermute(array, 'sp', pairs)]
    ppermute x2, waiting for transfers between devices: 2.31 us -> 5.22 us  [edges(): low = lax.ppermute(last, 'sp', forward)]
    ppermute x8 -> x9, starting transfers between devices: 5 us -> 5.57 us  [swap(): lax.ppermute(array, 'tp', [(i, i ^ 1 << bit) for i in range(self.count)])]
    ppermute x8 -> x9, waiting for transfers between devices: 14 us -> 14.1 us  [swap(): lax.ppermute(array, 'tp', [(i, i ^ 1 << bit) for i in range(self.count)])]
where the time goes in v4:
time: 249 us; the launch traced here: 246 us
  waiting for transfers between devices  147 us (59%)
  starting transfers between devices  59.1 us (24%)
  Pallas kernels  21.2 us (9%)
  other arithmetic  9.46 us (4%)
  local copies, waits for them, and re-layouts  7.46 us (3%)
    ppermute x28, waiting for transfers between devices, send_on(): return lax.ppermute(array, 'sp', pairs)  108 us
    ppermute x28, starting transfers between devices, send_on(): return lax.ppermute(array, 'sp', pairs)  25.6 us
    pallas_call x13, Pallas kernels, call(): pl.pallas_call(kernel, out_shape=[jax.ShapeDtypeStruct(shape, kind) for s...  21.2 us
    ppermute x9, waiting for transfers between devices, swap(): lax.ppermute(array, 'tp', [(i, i ^ 1 << bit) for i in range(self.count)])  14.1 us
    ppermute x3, starting transfers between devices, shards(): got_f = lax.ppermute(send_f, 'sp', forward)  13.3 us
    ppermute x3, waiting for transfers between devices, shards(): got_b = lax.ppermute(send_b, 'sp', [(b, a) for a, b in forward])  13.2 us
    ppermute x2, starting transfers between devices, edges(): low = lax.ppermute(last, 'sp', forward)  7.53 us
    ppermute x9, starting transfers between devices, swap(): lax.ppermute(array, 'tp', [(i, i ^ 1 << bit) for i in range(self.count)])  5.57 us
  transfers between devices with their start and end apart: 48, of which 22 were waited for; matrix products, arithmetic and copies ran while one was open for 3% of the time, Pallas kernels for 7%

profile of v4, /device:TPU:0, one launch (start us, length us, event | category | flops | bytes accessed | tf_op | source)
XLA Modules:
  0.0 245.7 jit_solution(16606749627459083348)
XLA Ops:
  1.5 4.9 %collective-permute-start = (bf16[3,1024]{1,0:T(4,128)(2,1)S(1)}, bf16[3,1024]{1,0:T(4,128)(2,1)S(1)}, u32[]{:S(2)}, u32[]{:S(2)}) collective-permute-start(bf16[3,1024]{1,0:T(4,128)(2,1)S(1)} %pad_maximum_fusion.3), channel_id=1, source_target_pairs={{0,4},{4,8},{8,12},{12,16},{16,20},{20,24},{24,28},{1,5},{5,9},{9,... | collective-permute-start | bytes 18440 | tf_op jit(solution)/shard_map/ppermute | solution.py:369
  6.4 1.3 collective-permute-start.1
  7.7 1.0 fusion.40
  8.7 1.0 fusion.46
  9.7 0.8 copy.21
  10.4 0.8 copy-done.4
  11.9 1.2 shard_map.190
  13.1 1.0 maximum_convert_fusion.3
  14.2 1.2 maximum_convert_fusion.2
  15.9 1.1 multiply_convert_fusion.values_ref
  17.4 4.6 %collective-permute-start.2 = (bf16[136,512]{1,0:T(8,128)(2,1)S(1)}, bf16[136,512]{1,0:T(8,128)(2,1)S(1)}, u32[]{:S(2)}, u32[]{:S(2)}) collective-permute-start(bf16[136,512]{1,0:T(8,128)(2,1)S(1)} %get-tuple-element.34), channel_id=1, source_target_pairs={{0,4},{4,8},{8,12},{12,16},{16,20},{20,24},{24,28},{1,5},{5,9},{9,... | collective-permute-start | bytes 417800 | tf_op jit(solution)/shard_map/ppermute | solution.py:510
  22.0 1.3 collective-permute-start.3
  23.3 1.2 collective-permute-done.2.refs_0_
  24.6 4.8 %collective-permute-done.3.refs_1_ = bf16[136,512]{1,0:T(8,128)(2,1)S(1)} collective-permute-done((bf16[136,512]{1,0:T(8,128)(2,1)S(1)}, bf16[136,512]{1,0:T(8,128)(2,1)S(1)}, u32[]{:S(2)}, u32[]{:S(2)}) %collective-permute-start.3) | collective-permute-done | bytes 139296 | tf_op jit(solution)/shard_map/ppermute | solution.py:511
  29.5 4.4 %collective-permute-start.4 = (bf16[136,512]{1,0:T(8,128)(2,1)S(1)}, bf16[136,512]{1,0:T(8,128)(2,1)S(1)}, u32[]{:S(2)}, u32[]{:S(2)}) collective-permute-start(bf16[136,512]{1,0:T(8,128)(2,1)S(1)} %get-tuple-element.37), channel_id=1, source_target_pairs={{0,8},{4,12},{8,16},{12,20},{16,24},{20,28},{1,9},{5,13},{9,17},{1... | collective-permute-start | bytes 417800 | tf_op jit(solution)/shard_map/ppermute | solution.py:510
  33.9 1.3 collective-permute-start.5
  36.5 4.3 %collective-permute-done.5.refs_1_ = bf16[136,512]{1,0:T(8,128)(2,1)S(1)} collective-permute-done((bf16[136,512]{1,0:T(8,128)(2,1)S(1)}, bf16[136,512]{1,0:T(8,128)(2,1)S(1)}, u32[]{:S(2)}, u32[]{:S(2)}) %collective-permute-start.5) | collective-permute-done | bytes 139296 | tf_op jit(solution)/shard_map/ppermute | solution.py:511
  40.9 0.9 shard_map.194
  41.8 4.3 %collective-permute-start.6 = (bf16[136,512]{1,0:T(8,128)(2,1)S(1)}, bf16[136,512]{1,0:T(8,128)(2,1)S(1)}, u32[]{:S(2)}, u32[]{:S(2)}) collective-permute-start(bf16[136,512]{1,0:T(8,128)(2,1)S(1)} %get-tuple-element.41), channel_id=1, source_target_pairs={{0,16},{4,20},{8,24},{12,28},{1,17},{5,21},{9,25},{13,29},{2,18},{... | collective-permute-start | bytes 417800 | tf_op jit(solution)/shard_map/ppermute | solution.py:510
  46.1 1.3 collective-permute-start.7
  48.0 2.7 %shard_map.191.within_ref = f32[512,512]{1,0:T(8,128)S(1)} custom-call(bf16[512,512]{1,0:T(8,128)(2,1)S(1)} %multiply_convert_fusion.values_ref, bf16[512,256]{1,0:T(8,128)(2,1)S(1)} %multiply_convert_fusion.2.inputs_ref, bf16[512,256]{1,0:T(8,128)(2,1)S(1)} %multiply_convert_fusion.1.readout_ref, f32[3,8,512]{2,1,0:T(8,128)S(1)} %get-tuple-element.30.rows_ref, ...), custom_call_target="tpu_custom_call" | custom-call | tf_op jit(solution)/shard_map/pallas_call | solution.py:376
  50.7 4.1 %collective-permute-done.7.refs_1_ = bf16[136,512]{1,0:T(8,128)(2,1)S(1)} collective-permute-done((bf16[136,512]{1,0:T(8,128)(2,1)S(1)}, bf16[136,512]{1,0:T(8,128)(2,1)S(1)}, u32[]{:S(2)}, u32[]{:S(2)}) %collective-permute-start.7) | collective-permute-done | bytes 139296 | tf_op jit(solution)/shard_map/ppermute | solution.py:511
  54.9 2.8 %shard_map.196 = (bf16[512,1024]{1,0:T(8,128)(2,1)S(1)}, bf16[512,1024]{1,0:T(8,128)(2,1)S(1)}) custom-call(s32[24]{0:T(128)S(1)} %get-tuple-element.80.info_ref.refs_0_, f32[512,512]{1,0:T(8,128)S(1)} %shard_map.191.within_ref, bf16[512,256]{1,0:T(8,128)(2,1)S(1)} %multiply_convert_fusion.1.readout_ref, f32[2,512,8]{2,1,0:T(8,128)S(1)} %get-tuple-element.31.cols_ref, ...), custom_call_target="tpu_custom_call" | custom-call | tf_op jit(solution)/shard_map/pallas_call | solution.py:376
  57.7 2.6 %collective-permute-done.8 = bf16[512,1024]{1,0:T(8,128)(2,1)S(1)} collective-permute-done((bf16[512,1024]{1,0:T(8,128)(2,1)S(1)}, bf16[512,1024]{1,0:T(8,128)(2,1)S(1)}, u32[]{:S(2)}, u32[]{:S(2)}) %collective-permute-start.8) | collective-permute-done | bytes 1048608 | tf_op jit(solution)/shard_map/ppermute | solution.py:48
  60.9 1.5 collective-permute-start.9
  63.2 1.4 collective-permute-start.31
  65.3 7.9 %collective-permute-done.28.refs_4_ = bf16[1280,128]{1,0:T(8,128)(2,1)S(1)} collective-permute-done((bf16[1280,128]{1,0:T(8,128)(2,1)S(1)}, bf16[1280,128]{1,0:T(8,128)(2,1)S(1)}, u32[]{:S(2)}, u32[]{:S(2)}) %collective-permute-start.28) | collective-permute-done | bytes 327712 | tf_op jit(solution)/shard_map/ppermute | solution.py:409
  73.8 6.4 %collective-permute-done.29.refs_5_ = bf16[1280,128]{1,0:T(8,128)(2,1)S(1)} collective-permute-done((bf16[1280,128]{1,0:T(8,128)(2,1)S(1)}, bf16[1280,128]{1,0:T(8,128)(2,1)S(1)}, u32[]{:S(2)}, u32[]{:S(2)}) %collective-permute-start.29) | collective-permute-done | bytes 327712 | tf_op jit(solution)/shard_map/ppermute | solution.py:409
  80.8 1.4 collective-permute-start.30
  82.4 26.3 %collective-permute-done.30.refs_6_ = bf16[1280,128]{1,0:T(8,128)(2,1)S(1)} collective-permute-done((bf16[1280,128]{1,0:T(8,128)(2,1)S(1)}, bf16[1280,128]{1,0:T(8,128)(2,1)S(1)}, u32[]{:S(2)}, u32[]{:S(2)}) %collective-permute-start.30) | collective-permute-done | bytes 327712 | tf_op jit(solution)/shard_map/ppermute | solution.py:409
  108.7 1.1 collective-permute-start.10
  110.5 1.4 collective-permute-start.35
  112.5 1.4 collective-permute-start.21
  113.9 6.5 %collective-permute-done.32.refs_8_ = bf16[1280,128]{1,0:T(8,128)(2,1)S(1)} collective-permute-done((bf16[1280,128]{1,0:T(8,128)(2,1)S(1)}, bf16[1280,128]{1,0:T(8,128)(2,1)S(1)}, u32[]{:S(2)}, u32[]{:S(2)}) %collective-permute-start.32) | collective-permute-done | bytes 327712 | tf_op jit(solution)/shard_map/ppermute | solution.py:409
  121.0 1.4 collective-permute-start.15
  123.2 18.2 %collective-permute-done.33.refs_9_ = bf16[1280,128]{1,0:T(8,128)(2,1)S(1)} collective-permute-done((bf16[1280,128]{1,0:T(8,128)(2,1)S(1)}, bf16[1280,128]{1,0:T(8,128)(2,1)S(1)}, u32[]{:S(2)}, u32[]{:S(2)}) %collective-permute-start.33) | collective-permute-done | bytes 327712 | tf_op jit(solution)/shard_map/ppermute | solution.py:409
  142.1 1.4 collective-permute-start.23
  143.5 2.0 collective-permute-done.15.refs_9_
  145.5 1.3 collective-permute-start.17
  146.8 8.7 %collective-permute-done.20.refs_15_ = bf16[256,1280]{1,0:T(8,128)(2,1)S(1)} collective-permute-done((bf16[256,1280]{1,0:T(8,128)(2,1)S(1)}, bf16[256,1280]{1,0:T(8,128)(2,1)S(1)}, u32[]{:S(2)}, u32[]{:S(2)}) %collective-permute-start.20) | collective-permute-done | bytes 655392 | tf_op jit(solution)/shard_map/ppermute | solution.py:409
  156.1 13.4 %collective-permute-done.16.refs_10_ = bf16[256,1280]{1,0:T(8,128)(2,1)S(1)} collective-permute-done((bf16[256,1280]{1,0:T(8,128)(2,1)S(1)}, bf16[256,1280]{1,0:T(8,128)(2,1)S(1)}, u32[]{:S(2)}, u32[]{:S(2)}) %collective-permute-start.16) | collective-permute-done | bytes 655392 | tf_op jit(solution)/shard_map/ppermute | solution.py:409
  170.2 1.4 collective-permute-start.25
  171.6 2.2 collective-permute-done.17.refs_11_
  173.8 1.4 collective-permute-start.34
  175.1 8.4 %collective-permute-done.22.refs_17_ = bf16[256,1280]{1,0:T(8,128)(2,1)S(1)} collective-permute-done((bf16[256,1280]{1,0:T(8,128)(2,1)S(1)}, bf16[256,1280]{1,0:T(8,128)(2,1)S(1)}, u32[]{:S(2)}, u32[]{:S(2)}) %collective-permute-start.22) | collective-permute-done | bytes 655392 | tf_op jit(solution)/shard_map/ppermute | solution.py:409
  184.2 1.4 collective-permute-start.41
  185.7 6.8 %shard_map.197 = (f32[512,1280]{1,0:T(8,128)S(1)}, f32[512,1280]{1,0:T(8,128)S(1)}, bf16[512,256]{1,0:T(8,128)(2,1)S(1)}) custom-call(s32[24]{0:T(128)S(1)} %get-tuple-element.80.info_ref.refs_0_, f32[1,2048]{1,0:T(1,128)S(1)} %bitcast.33, bf16[512,512]{1,0:T(8,128)(2,1)S(1)} %fusion.7.refs_2_, bf16[512,512]{1,0:T(8,128)(2,1)S(1)} %collective-permute-done.10.refs_3_, ...), custom_call_target="tpu_custom_call" | custom-call | tf_op jit(solution)/shard_map/pallas_call | solution.py:376
  192.6 2.3 collective-permute-done.34.refs_10_
  194.8 1.4 collective-permute-start.37
  196.2 5.7 %collective-permute-done.36.refs_3_ = bf16[1280,128]{1,0:T(8,128)(2,1)S(1)} collective-permute-done((bf16[1280,128]{1,0:T(8,128)(2,1)S(1)}, bf16[1280,128]{1,0:T(8,128)(2,1)S(1)}, u32[]{:S(2)}, u32[]{:S(2)}) %collective-permute-start.36) | collective-permute-done | bytes 327712 | tf_op jit(solution)/shard_map/ppermute | solution.py:409
  203.3 1.3 collective-permute-start.45
  204.6 0.8 shard_map.198
  205.6 2.6 %collective-permute-start.26 = (bf16[1,2560]{1,0:T(2,128)(2,1)S(1)}, bf16[1,2560]{1,0:T(2,128)(2,1)S(1)}, u32[]{:S(2)}, u32[]{:S(2)}) collective-permute-start(bf16[1,2560]{1,0:T(2,128)(2,1)S(1)} %pad_maximum_fusion.1), channel_id=1, source_target_pairs={{0,4},{4,8},{8,12},{12,16},{16,20},{20,24},{24,28},{1,5},{5,9},{9,... | collective-permute-start | bytes 15368 | tf_op jit(solution)/shard_map/ppermute | solution.py:369
  208.2 5.2 %collective-permute-done.26 = bf16[1,2560]{1,0:T(2,128)(2,1)S(1)} collective-permute-done((bf16[1,2560]{1,0:T(2,128)(2,1)S(1)}, bf16[1,2560]{1,0:T(2,128)(2,1)S(1)}, u32[]{:S(2)}, u32[]{:S(2)}) %collective-permute-start.26) | collective-permute-done | bytes 5152 | tf_op jit(solution)/shard_map/ppermute | solution.py:369
  213.4 1.3 collective-permute-start.27
  214.7 4.7 %collective-permute-done.27 = bf16[1,2560]{1,0:T(2,128)(2,1)S(1)} collective-permute-done((bf16[1,2560]{1,0:T(2,128)(2,1)S(1)}, bf16[1,2560]{1,0:T(2,128)(2,1)S(1)}, u32[]{:S(2)}, u32[]{:S(2)}) %collective-permute-start.27) | collective-permute-done | bytes 5152 | tf_op jit(solution)/shard_map/ppermute | solution.py:370
  220.0 2.1 fusion.2.refs_1_.hidden_ref
  222.2 2.5 %shard_map.199.refs_2_ = bf16[8,512,256]{2,1,0:T(8,128)(2,1)S(1)} custom-call(s32[24]{0:T(128)S(1)} %get-tuple-element.80.info_ref.refs_0_, bf16[512,1280]{1,0:T(8,128)(2,1)S(1)} %fusion.2.refs_1_.hidden_ref, bf16[1280,128]{1,0:T(8,128)(2,1)S(1)} %get-tuple-element.68.refs_2_, bf16[1280,128]{1,0:T(8,128)(2,1)S(1)} %get-tuple-element.67.refs_3_, ...), custom_call_target="tpu_custom_call" | custom-call | tf_op jit(solution)/shard_map/pallas_call | solution.py:376
  224.7 1.2 shard_map.200
  227.0 1.2 shard_map.201
  231.2 1.7 collective-permute-start.43
  233.0 5.9 %collective-permute-done.39 = bf16[512,256]{1,0:T(8,128)(2,1)S(1)} collective-permute-done((bf16[512,256]{1,0:T(8,128)(2,1)S(1)}, bf16[512,256]{1,0:T(8,128)(2,1)S(1)}, u32[]{:S(2)}, u32[]{:S(2)}) %collective-permute-start.39) | collective-permute-done | bytes 262176 | tf_op jit(solution)/shard_map/ppermute | solution.py:48
  239.1 5.5 %collective-permute-done.43 = bf16[512,256]{1,0:T(8,128)(2,1)S(1)} collective-permute-done((bf16[512,256]{1,0:T(8,128)(2,1)S(1)}, bf16[512,256]{1,0:T(8,128)(2,1)S(1)}, u32[]{:S(2)}, u32[]{:S(2)}) %collective-permute-start.43) | collective-permute-done | bytes 262176 | tf_op jit(solution)/shard_map/ppermute | solution.py:48
  244.7 1.0 fusion.15
  (119 shorter events, 19.9 us)
Async XLA Ops:
  1.5 11.6 %collective-permute-start = (bf16[3,1024]{1,0:T(4,128)(2,1)S(1)}, bf16[3,1024]{1,0:T(4,128)(2,1)S(1)}, u32[]{:S(2)}, u32[]{:S(2)}) collective-permute-start(bf16[3,1024]{1,0:T(4,128)(2,1)S(1)} %pad_maximum_fusion.3), channel_id=1, source_target_pairs={{0,4},{4,8},{8,12},{12,16},{16,20},{20,24},{24,28},{1,5},{5,9},{9,... | collective-permute-start | bytes 18440 | tf_op jit(solution)/shard_map/ppermute | solution.py:369
  6.4 6.7 %collective-permute-start.1 = (bf16[3,1024]{1,0:T(4,128)(2,1)S(1)}, bf16[3,1024]{1,0:T(4,128)(2,1)S(1)}, u32[]{:S(2)}, u32[]{:S(2)}) collective-permute-start(bf16[3,1024]{1,0:T(4,128)(2,1)S(1)} %pad_maximum_fusion.4), channel_id=1, source_target_pairs={{4,0},{8,4},{12,8},{16,12},{20,16},{24,20},{28,24},{5,1},{9,5},{13... | collective-permute-start | bytes 18440 | tf_op jit(solution)/shard_map/ppermute | solution.py:370
  10.4 0.8 copy-start.4
  11.2 0.8 copy-start.5
  17.0 6.3 %copy-start.13 = (f32[7,256]{1,0:T(8,128)S(1)}, f32[7,256]{1,0:T(8,128)}, u32[]{:S(2)}) copy-start(f32[7,256]{1,0:T(8,128)} %param.30) | copy-start | bytes 21508
  17.0 18.9 %copy-start.10 = (bf16[512,256]{1,0:T(8,128)(2,1)S(1)}, bf16[512,256]{1,0:T(8,128)(2,1)}, u32[]{:S(2)}) copy-start(bf16[512,256]{1,0:T(8,128)(2,1)} %param.24) | copy-start | bytes 786436
  17.4 7.1 %collective-permute-start.2 = (bf16[136,512]{1,0:T(8,128)(2,1)S(1)}, bf16[136,512]{1,0:T(8,128)(2,1)S(1)}, u32[]{:S(2)}, u32[]{:S(2)}) collective-permute-start(bf16[136,512]{1,0:T(8,128)(2,1)S(1)} %get-tuple-element.34), channel_id=1, source_target_pairs={{0,4},{4,8},{8,12},{12,16},{16,20},{20,24},{24,28},{1,5},{5,9},{9,... | collective-permute-start | bytes 417800 | tf_op jit(solution)/shard_map/ppermute | solution.py:510
  22.0 7.4 %collective-permute-start.3 = (bf16[136,512]{1,0:T(8,128)(2,1)S(1)}, bf16[136,512]{1,0:T(8,128)(2,1)S(1)}, u32[]{:S(2)}, u32[]{:S(2)}) collective-permute-start(bf16[136,512]{1,0:T(8,128)(2,1)S(1)} %get-tuple-element.35), channel_id=1, source_target_pairs={{4,0},{8,4},{12,8},{16,12},{20,16},{24,20},{28,24},{5,1},{9,5},{13... | collective-permute-start | bytes 417800 | tf_op jit(solution)/shard_map/ppermute | solution.py:511
  29.5 7.1 %collective-permute-start.4 = (bf16[136,512]{1,0:T(8,128)(2,1)S(1)}, bf16[136,512]{1,0:T(8,128)(2,1)S(1)}, u32[]{:S(2)}, u32[]{:S(2)}) collective-permute-start(bf16[136,512]{1,0:T(8,128)(2,1)S(1)} %get-tuple-element.37), channel_id=1, source_target_pairs={{0,8},{4,12},{8,16},{12,20},{16,24},{20,28},{1,9},{5,13},{9,17},{1... | collective-permute-start | bytes 417800 | tf_op jit(solution)/shard_map/ppermute | solution.py:510
  33.9 6.9 %collective-permute-start.5 = (bf16[136,512]{1,0:T(8,128)(2,1)S(1)}, bf16[136,512]{1,0:T(8,128)(2,1)S(1)}, u32[]{:S(2)}, u32[]{:S(2)}) collective-permute-start(bf16[136,512]{1,0:T(8,128)(2,1)S(1)} %get-tuple-element.38), channel_id=1, source_target_pairs={{8,0},{12,4},{16,8},{20,12},{24,16},{28,20},{9,1},{13,5},{17,9},{2... | collective-permute-start | bytes 417800 | tf_op jit(solution)/shard_map/ppermute | solution.py:511
  41.8 8.9 %collective-permute-start.6 = (bf16[136,512]{1,0:T(8,128)(2,1)S(1)}, bf16[136,512]{1,0:T(8,128)(2,1)S(1)}, u32[]{:S(2)}, u32[]{:S(2)}) collective-permute-start(bf16[136,512]{1,0:T(8,128)(2,1)S(1)} %get-tuple-element.41), channel_id=1, source_target_pairs={{0,16},{4,20},{8,24},{12,28},{1,17},{5,21},{9,25},{13,29},{2,18},{... | collective-permute-start | bytes 417800 | tf_op jit(solution)/shard_map/ppermute | solution.py:510
  46.1 8.7 %collective-permute-start.7 = (bf16[136,512]{1,0:T(8,128)(2,1)S(1)}, bf16[136,512]{1,0:T(8,128)(2,1)S(1)}, u32[]{:S(2)}, u32[]{:S(2)}) collective-permute-start(bf16[136,512]{1,0:T(8,128)(2,1)S(1)} %get-tuple-element.42), channel_id=1, source_target_pairs={{16,0},{20,4},{24,8},{28,12},{17,1},{21,5},{25,9},{29,13},{18,2},{... | collective-permute-start | bytes 417800 | tf_op jit(solution)/shard_map/ppermute | solution.py:511
  47.9 6.9 %copy-start = (bf16[512,2048]{1,0:T(8,128)(2,1)S(1)}, bf16[512,2048]{1,0:T(8,128)(2,1)}, u32[]{:S(2)}) copy-start(bf16[512,2048]{1,0:T(8,128)(2,1)} %map_ref.1) | copy-start | bytes 6291460
  47.9 6.9 %copy-start.3 = (bf16[512,512]{1,0:T(8,128)(2,1)S(1)}, bf16[512,512]{1,0:T(8,128)(2,1)}, u32[]{:S(2)}) copy-start(bf16[512,512]{1,0:T(8,128)(2,1)} %valve_ref.1) | copy-start | bytes 1572868
  47.9 6.9 %copy-start.7 = (f32[512]{0:T(512)S(1)}, f32[512]{0:T(512)}, u32[]{:S(2)}) copy-start(f32[512]{0:T(512)} %param.31) | copy-start | bytes 6148
  57.7 2.7 %collective-permute-start.8 = (bf16[512,1024]{1,0:T(8,128)(2,1)S(1)}, bf16[512,1024]{1,0:T(8,128)(2,1)S(1)}, u32[]{:S(2)}, u32[]{:S(2)}) collective-permute-start(bf16[512,1024]{1,0:T(8,128)(2,1)S(1)} %get-tuple-element.45), channel_id=1, source_target_pairs={{0,1},{1,0},{2,3},{3,2},{4,5},{5,4},{6,7},{7,6},{8,9},{9,8},{10,11... | collective-permute-start | bytes 3145736 | tf_op jit(solution)/shard_map/ppermute | solution.py:48
  60.4 2.0 copy-start.8
  60.4 4.8 %copy-start.1 = (bf16[256,1280]{1,0:T(8,128)(2,1)S(1)}, bf16[256,1280]{1,0:T(8,128)(2,1)}, u32[]{:S(2)}) copy-start(bf16[256,1280]{1,0:T(8,128)(2,1)} %refs_5_.1) | copy-start | bytes 1966084
  60.4 12.7 %copy-start.2 = (bf16[256,1280]{1,0:T(8,128)(2,1)S(1)}, bf16[256,1280]{1,0:T(8,128)(2,1)}, u32[]{:S(2)}) copy-start(bf16[256,1280]{1,0:T(8,128)(2,1)} %refs_12_.1) | copy-start | bytes 1966084
  60.4 21.8 %copy-start.9 = (bf16[512,512]{1,0:T(8,128)(2,1)S(1)}, bf16[512,512]{1,0:T(8,128)(2,1)}, u32[]{:S(2)}) copy-start(bf16[512,512]{1,0:T(8,128)(2,1)} %param.20) | copy-start | bytes 1572868
  60.9 19.9 %collective-permute-start.9 = (bf16[512,512]{1,0:T(8,128)(2,1)S(1)}, bf16[512,512]{1,0:T(8,128)(2,1)S(1)}, u32[]{:S(2)}, u32[]{:S(2)}) collective-permute-start(bf16[512,512]{1,0:T(8,128)(2,1)S(1)} %slice.552), channel_id=1, source_target_pairs={{0,2},{1,3},{2,0},{3,1},{4,6},{5,7},{6,4},{7,5},{8,10},{9,11},{10,... | collective-permute-start | bytes 1572872 | tf_op jit(solution)/shard_map/ppermute | solution.py:48
  62.5 123.2 %copy-start.11 = (f32[3,1280]{1,0:T(4,128)S(1)}, f32[3,1280]{1,0:T(4,128)}, u32[]{:S(2)}) copy-start(f32[3,1280]{1,0:T(4,128)} %param.37) | copy-start | bytes 46084
  62.5 123.2 %copy-start.12 = (f32[3,1280]{1,0:T(4,128)S(1)}, f32[3,1280]{1,0:T(4,128)}, u32[]{:S(2)}) copy-start(f32[3,1280]{1,0:T(4,128)} %param.36) | copy-start | bytes 46084
  62.5 123.2 %copy-start.6 = (f32[2048]{0:T(1024)S(1)}, f32[2048]{0:T(1024)}, u32[]{:S(2)}) copy-start(f32[2048]{0:T(1024)} %param.33) | copy-start | bytes 24580
  62.5 10.6 %collective-permute-start.28 = (bf16[1280,128]{1,0:T(8,128)(2,1)S(1)}, bf16[1280,128]{1,0:T(8,128)(2,1)S(1)}, u32[]{:S(2)}, u32[]{:S(2)}) collective-permute-start(bf16[1280,128]{1,0:T(8,128)(2,1)S(1)} %get-tuple-element.68.refs_2_), channel_id=1, source_target_pairs={{4,12},{12,20},{20,28},{28,24},{24,16},{16,8},{8,0},{0,4},{5,13},{... | collective-permute-start | bytes 983048 | tf_op jit(solution)/shard_map/ppermute | solution.py:409
  63.2 10.0 %collective-permute-start.31 = (bf16[1280,128]{1,0:T(8,128)(2,1)S(1)}, bf16[1280,128]{1,0:T(8,128)(2,1)S(1)}, u32[]{:S(2)}, u32[]{:S(2)}) collective-permute-start(bf16[1280,128]{1,0:T(8,128)(2,1)S(1)} %get-tuple-element.67.refs_3_), channel_id=1, source_target_pairs={{12,4},{20,12},{28,20},{24,28},{16,24},{8,16},{0,8},{4,0},{13,5},{... | collective-permute-start | bytes 983048 | tf_op jit(solution)/shard_map/ppermute | solution.py:409
  64.6 15.6 %collective-permute-start.29 = (bf16[1280,128]{1,0:T(8,128)(2,1)S(1)}, bf16[1280,128]{1,0:T(8,128)(2,1)S(1)}, u32[]{:S(2)}, u32[]{:S(2)}) collective-permute-start(bf16[1280,128]{1,0:T(8,128)(2,1)S(1)} %get-tuple-element.67.refs_3_), channel_id=1, source_target_pairs={{4,12},{12,20},{20,28},{28,24},{24,16},{16,8},{8,0},{0,4},{5,13},{... | collective-permute-start | bytes 983048 | tf_op jit(solution)/shard_map/ppermute | solution.py:409
  65.2 44.6 %collective-permute-start.12 = (bf16[256,1280]{1,0:T(8,128)(2,1)S(1)}, bf16[256,1280]{1,0:T(8,128)(2,1)S(1)}, u32[]{:S(2)}, u32[]{:S(2)}) collective-permute-start(bf16[256,1280]{1,0:T(8,128)(2,1)S(1)} %copy-done.1), channel_id=1, source_target_pairs={{4,12},{12,20},{20,28},{28,24},{24,16},{16,8},{8,0},{0,4},{5,13},{... | collective-permute-start | bytes 1966088 | tf_op jit(solution)/shard_map/ppermute | solution.py:409
  73.1 37.3 %collective-permute-start.19 = (bf16[256,1280]{1,0:T(8,128)(2,1)S(1)}, bf16[256,1280]{1,0:T(8,128)(2,1)S(1)}, u32[]{:S(2)}, u32[]{:S(2)}) collective-permute-start(bf16[256,1280]{1,0:T(8,128)(2,1)S(1)} %copy-done.2), channel_id=1, source_target_pairs={{12,4},{20,12},{28,20},{24,28},{16,24},{8,16},{0,8},{4,0},{13,5},{... | collective-permute-start | bytes 1966088 | tf_op jit(solution)/shard_map/ppermute | solution.py:409
  73.1 38.7 %collective-permute-start.13 = (bf16[256,1280]{1,0:T(8,128)(2,1)S(1)}, bf16[256,1280]{1,0:T(8,128)(2,1)S(1)}, u32[]{:S(2)}, u32[]{:S(2)}) collective-permute-start(bf16[256,1280]{1,0:T(8,128)(2,1)S(1)} %copy-done.1), channel_id=1, source_target_pairs={{12,4},{20,12},{28,20},{24,28},{16,24},{8,16},{0,8},{4,0},{13,5},{... | collective-permute-start | bytes 1966088 | tf_op jit(solution)/shard_map/ppermute | solution.py:409
  80.1 32.3 %collective-permute-start.18 = (bf16[256,1280]{1,0:T(8,128)(2,1)S(1)}, bf16[256,1280]{1,0:T(8,128)(2,1)S(1)}, u32[]{:S(2)}, u32[]{:S(2)}) collective-permute-start(bf16[256,1280]{1,0:T(8,128)(2,1)S(1)} %copy-done.2), channel_id=1, source_target_pairs={{4,12},{12,20},{20,28},{28,24},{24,16},{16,8},{8,0},{0,4},{5,13},{... | collective-permute-start | bytes 1966088 | tf_op jit(solution)/shard_map/ppermute | solution.py:409
  80.8 27.9 %collective-permute-start.30 = (bf16[1280,128]{1,0:T(8,128)(2,1)S(1)}, bf16[1280,128]{1,0:T(8,128)(2,1)S(1)}, u32[]{:S(2)}, u32[]{:S(2)}) collective-permute-start(bf16[1280,128]{1,0:T(8,128)(2,1)S(1)} %get-tuple-element.68.refs_2_), channel_id=1, source_target_pairs={{12,4},{20,12},{28,20},{24,28},{16,24},{8,16},{0,8},{4,0},{13,5},{... | collective-permute-start | bytes 983048 | tf_op jit(solution)/shard_map/ppermute | solution.py:409
  108.7 13.7 %collective-permute-start.10 = (bf16[512,512]{1,0:T(8,128)(2,1)S(1)}, bf16[512,512]{1,0:T(8,128)(2,1)S(1)}, u32[]{:S(2)}, u32[]{:S(2)}) collective-permute-start(bf16[512,512]{1,0:T(8,128)(2,1)S(1)} %fusion.7.refs_2_), channel_id=1, source_target_pairs={{0,2},{1,3},{2,0},{3,1},{4,6},{5,7},{6,4},{7,5},{8,10},{9,11},{10,... | collective-permute-start | bytes 1572872 | tf_op jit(solution)/shard_map/ppermute | solution.py:48
  109.8 10.6 %collective-permute-start.32 = (bf16[1280,128]{1,0:T(8,128)(2,1)S(1)}, bf16[1280,128]{1,0:T(8,128)(2,1)S(1)}, u32[]{:S(2)}, u32[]{:S(2)}) collective-permute-start(bf16[1280,128]{1,0:T(8,128)(2,1)S(1)} %collective-permute-done.28.refs_4_), channel_id=1, source_target_pairs={{4,12},{12,20},{20,28},{28,24},{24,16},{16,8},{8,0},{0,4},{5,13},{... | collective-permute-start | bytes 983048 | tf_op jit(solution)/shard_map/ppermute | solution.py:409
  110.5 10.6 %collective-permute-start.35 = (bf16[1280,128]{1,0:T(8,128)(2,1)S(1)}, bf16[1280,128]{1,0:T(8,128)(2,1)S(1)}, u32[]{:S(2)}, u32[]{:S(2)}) collective-permute-start(bf16[1280,128]{1,0:T(8,128)(2,1)S(1)} %collective-permute-done.31.refs_7_), channel_id=1, source_target_pairs={{12,4},{20,12},{28,20},{24,28},{16,24},{8,16},{0,8},{4,0},{13,5},{... | collective-permute-start | bytes 983048 | tf_op jit(solution)/shard_map/ppermute | solution.py:409
  111.8 29.6 %collective-permute-start.14 = (bf16[256,1280]{1,0:T(8,128)(2,1)S(1)}, bf16[256,1280]{1,0:T(8,128)(2,1)S(1)}, u32[]{:S(2)}, u32[]{:S(2)}) collective-permute-start(bf16[256,1280]{1,0:T(8,128)(2,1)S(1)} %collective-permute-done.12.refs_6_), channel_id=1, source_target_pairs={{4,12},{12,20},{20,28},{28,24},{24,16},{16,8},{8,0},{0,4},{5,13},{... | collective-permute-start | bytes 1966088 | tf_op jit(solution)/shard_map/ppermute | solution.py:409
  112.5 29.6 %collective-permute-start.21 = (bf16[256,1280]{1,0:T(8,128)(2,1)S(1)}, bf16[256,1280]{1,0:T(8,128)(2,1)S(1)}, u32[]{:S(2)}, u32[]{:S(2)}) collective-permute-start(bf16[256,1280]{1,0:T(8,128)(2,1)S(1)} %collective-permute-done.19.refs_14_), channel_id=1, source_target_pairs={{12,4},{20,12},{28,20},{24,28},{16,24},{8,16},{0,8},{4,0},{13,5},{... | collective-permute-start | bytes 1966088 | tf_op jit(solution)/shard_map/ppermute | solution.py:409
  120.4 21.1 %collective-permute-start.33 = (bf16[1280,128]{1,0:T(8,128)(2,1)S(1)}, bf16[1280,128]{1,0:T(8,128)(2,1)S(1)}, u32[]{:S(2)}, u32[]{:S(2)}) collective-permute-start(bf16[1280,128]{1,0:T(8,128)(2,1)S(1)} %collective-permute-done.29.refs_5_), channel_id=1, source_target_pairs={{4,12},{12,20},{20,28},{28,24},{24,16},{16,8},{8,0},{0,4},{5,13},{... | collective-permute-start | bytes 983048 | tf_op jit(solution)/shard_map/ppermute | solution.py:409
  121.0 24.4 %collective-permute-start.15 = (bf16[256,1280]{1,0:T(8,128)(2,1)S(1)}, bf16[256,1280]{1,0:T(8,128)(2,1)S(1)}, u32[]{:S(2)}, u32[]{:S(2)}) collective-permute-start(bf16[256,1280]{1,0:T(8,128)(2,1)S(1)} %collective-permute-done.13.refs_7_), channel_id=1, source_target_pairs={{12,4},{20,12},{28,20},{24,28},{16,24},{8,16},{0,8},{4,0},{13,5},{... | collective-permute-start | bytes 1966088 | tf_op jit(solution)/shard_map/ppermute | solution.py:409
  122.4 33.1 %collective-permute-start.20 = (bf16[256,1280]{1,0:T(8,128)(2,1)S(1)}, bf16[256,1280]{1,0:T(8,128)(2,1)S(1)}, u32[]{:S(2)}, u32[]{:S(2)}) collective-permute-start(bf16[256,1280]{1,0:T(8,128)(2,1)S(1)} %collective-permute-done.18.refs_13_), channel_id=1, source_target_pairs={{4,12},{12,20},{20,28},{28,24},{24,16},{16,8},{8,0},{0,4},{5,13},{... | collective-permute-start | bytes 1966088 | tf_op jit(solution)/shard_map/ppermute | solution.py:409
  141.5 42.8 %collective-permute-start.11 = (bf16[512,1024]{1,0:T(8,128)(2,1)S(1)}, bf16[512,1024]{1,0:T(8,128)(2,1)S(1)}, u32[]{:S(2)}, u32[]{:S(2)}) collective-permute-start(bf16[512,1024]{1,0:T(8,128)(2,1)S(1)} %pad_maximum_fusion), channel_id=1, source_target_pairs={{0,1},{1,0},{2,3},{3,2},{4,5},{5,4},{6,7},{7,6},{8,9},{9,8},{10,11... | collective-permute-start | bytes 3145736 | tf_op jit(solution)/shard_map/ppermute | solution.py:48
  141.5 28.1 %collective-permute-start.16 = (bf16[256,1280]{1,0:T(8,128)(2,1)S(1)}, bf16[256,1280]{1,0:T(8,128)(2,1)S(1)}, u32[]{:S(2)}, u32[]{:S(2)}) collective-permute-start(bf16[256,1280]{1,0:T(8,128)(2,1)S(1)} %collective-permute-done.14.refs_8_), channel_id=1, source_target_pairs={{4,12},{12,20},{20,28},{28,24},{24,16},{16,8},{8,0},{0,4},{5,13},{... | collective-permute-start | bytes 1966088 | tf_op jit(solution)/shard_map/ppermute | solution.py:409
  142.1 28.1 %collective-permute-start.23 = (bf16[256,1280]{1,0:T(8,128)(2,1)S(1)}, bf16[256,1280]{1,0:T(8,128)(2,1)S(1)}, u32[]{:S(2)}, u32[]{:S(2)}) collective-permute-start(bf16[256,1280]{1,0:T(8,128)(2,1)S(1)} %collective-permute-done.21.refs_16_), channel_id=1, source_target_pairs={{12,4},{20,12},{28,20},{24,28},{16,24},{8,16},{0,8},{4,0},{13,5},{... | collective-permute-start | bytes 1966088 | tf_op jit(solution)/shard_map/ppermute | solution.py:409
  145.5 28.3 %collective-permute-start.17 = (bf16[256,1280]{1,0:T(8,128)(2,1)S(1)}, bf16[256,1280]{1,0:T(8,128)(2,1)S(1)}, u32[]{:S(2)}, u32[]{:S(2)}) collective-permute-start(bf16[256,1280]{1,0:T(8,128)(2,1)S(1)} %collective-permute-done.15.refs_9_), channel_id=1, source_target_pairs={{12,4},{20,12},{28,20},{24,28},{16,24},{8,16},{0,8},{4,0},{13,5},{... | collective-permute-start | bytes 1966088 | tf_op jit(solution)/shard_map/ppermute | solution.py:409
  155.5 28.1 %collective-permute-start.22 = (bf16[256,1280]{1,0:T(8,128)(2,1)S(1)}, bf16[256,1280]{1,0:T(8,128)(2,1)S(1)}, u32[]{:S(2)}, u32[]{:S(2)}) collective-permute-start(bf16[256,1280]{1,0:T(8,128)(2,1)S(1)} %collective-permute-done.20.refs_15_), channel_id=1, source_target_pairs={{4,12},{12,20},{20,28},{28,24},{24,16},{16,8},{8,0},{0,4},{5,13},{... | collective-permute-start | bytes 1966088 | tf_op jit(solution)/shard_map/ppermute | solution.py:409
  169.5 33.8 %collective-permute-start.24 = (bf16[256,1280]{1,0:T(8,128)(2,1)S(1)}, bf16[256,1280]{1,0:T(8,128)(2,1)S(1)}, u32[]{:S(2)}, u32[]{:S(2)}) collective-permute-start(bf16[256,1280]{1,0:T(8,128)(2,1)S(1)} %collective-permute-done.16.refs_10_), channel_id=1, source_target_pairs={{4,12},{12,20},{20,28},{28,24},{24,16},{16,8},{8,0},{0,4},{5,13},{... | collective-permute-start | bytes 1966088 | tf_op jit(solution)/shard_map/ppermute | solution.py:409
  170.2 34.4 %collective-permute-start.25 = (bf16[256,1280]{1,0:T(8,128)(2,1)S(1)}, bf16[256,1280]{1,0:T(8,128)(2,1)S(1)}, u32[]{:S(2)}, u32[]{:S(2)}) collective-permute-start(bf16[256,1280]{1,0:T(8,128)(2,1)S(1)} %collective-permute-done.23.refs_18_), channel_id=1, source_target_pairs={{12,4},{20,12},{28,20},{24,28},{16,24},{8,16},{0,8},{4,0},{13,5},{... | collective-permute-start | bytes 1966088 | tf_op jit(solution)/shard_map/ppermute | solution.py:409
  173.8 21.1 %collective-permute-start.34 = (bf16[1280,128]{1,0:T(8,128)(2,1)S(1)}, bf16[1280,128]{1,0:T(8,128)(2,1)S(1)}, u32[]{:S(2)}, u32[]{:S(2)}) collective-permute-start(bf16[1280,128]{1,0:T(8,128)(2,1)S(1)} %collective-permute-done.30.refs_6_), channel_id=1, source_target_pairs={{12,4},{20,12},{28,20},{24,28},{16,24},{8,16},{0,8},{4,0},{13,5},{... | collective-permute-start | bytes 983048 | tf_op jit(solution)/shard_map/ppermute | solution.py:409
  183.6 18.4 %collective-permute-start.36 = (bf16[1280,128]{1,0:T(8,128)(2,1)S(1)}, bf16[1280,128]{1,0:T(8,128)(2,1)S(1)}, u32[]{:S(2)}, u32[]{:S(2)}) collective-permute-start(bf16[1280,128]{1,0:T(8,128)(2,1)S(1)} %collective-permute-done.32.refs_8_), channel_id=1, source_target_pairs={{4,12},{12,20},{20,28},{28,24},{24,16},{16,8},{8,0},{0,4},{5,13},{... | collective-permute-start | bytes 983048 | tf_op jit(solution)/shard_map/ppermute | solution.py:409
  184.2 18.4 %collective-permute-start.41 = (bf16[1280,128]{1,0:T(8,128)(2,1)S(1)}, bf16[1280,128]{1,0:T(8,128)(2,1)S(1)}, u32[]{:S(2)}, u32[]{:S(2)}) collective-permute-start(bf16[1280,128]{1,0:T(8,128)(2,1)S(1)} %collective-permute-done.35.refs_11_), channel_id=1, source_target_pairs={{12,4},{20,12},{28,20},{24,28},{16,24},{8,16},{0,8},{4,0},{13,5},{... | collective-permute-start | bytes 983048 | tf_op jit(solution)/shard_map/ppermute | solution.py:409
  194.8 29.8 %collective-permute-start.37 = (bf16[1280,128]{1,0:T(8,128)(2,1)S(1)}, bf16[1280,128]{1,0:T(8,128)(2,1)S(1)}, u32[]{:S(2)}, u32[]{:S(2)}) collective-permute-start(bf16[1280,128]{1,0:T(8,128)(2,1)S(1)} %collective-permute-done.34.refs_10_), channel_id=1, source_target_pairs={{12,4},{20,12},{28,20},{24,28},{16,24},{8,16},{0,8},{4,0},{13,5},{... | collective-permute-start | bytes 983048 | tf_op jit(solution)/shard_map/ppermute | solution.py:409
  202.0 25.1 %collective-permute-start.40 = (bf16[1280,128]{1,0:T(8,128)(2,1)S(1)}, bf16[1280,128]{1,0:T(8,128)(2,1)S(1)}, u32[]{:S(2)}, u32[]{:S(2)}) collective-permute-start(bf16[1280,128]{1,0:T(8,128)(2,1)S(1)} %collective-permute-done.33.refs_9_), channel_id=1, source_target_pairs={{4,12},{12,20},{20,28},{28,24},{24,16},{16,8},{8,0},{0,4},{5,13},{... | collective-permute-start | bytes 983048 | tf_op jit(solution)/shard_map/ppermute | solution.py:409
  202.6 23.3 %collective-permute-start.44 = (bf16[1280,128]{1,0:T(8,128)(2,1)S(1)}, bf16[1280,128]{1,0:T(8,128)(2,1)S(1)}, u32[]{:S(2)}, u32[]{:S(2)}) collective-permute-start(bf16[1280,128]{1,0:T(8,128)(2,1)S(1)} %collective-permute-done.36.refs_3_), channel_id=1, source_target_pairs={{4,12},{12,20},{20,28},{28,24},{24,16},{16,8},{8,0},{0,4},{5,13},{... | collective-permute-start | bytes 983048 | tf_op jit(solution)/shard_map/ppermute | solution.py:409
  203.3 22.6 %collective-permute-start.45 = (bf16[1280,128]{1,0:T(8,128)(2,1)S(1)}, bf16[1280,128]{1,0:T(8,128)(2,1)S(1)}, u32[]{:S(2)}, u32[]{:S(2)}) collective-permute-start(bf16[1280,128]{1,0:T(8,128)(2,1)S(1)} %collective-permute-done.41.refs_4_), channel_id=1, source_target_pairs={{12,4},{20,12},{28,20},{24,28},{16,24},{8,16},{0,8},{4,0},{13,5},{... | collective-permute-start | bytes 983048 | tf_op jit(solution)/shard_map/ppermute | solution.py:409
  205.6 7.9 %collective-permute-start.26 = (bf16[1,2560]{1,0:T(2,128)(2,1)S(1)}, bf16[1,2560]{1,0:T(2,128)(2,1)S(1)}, u32[]{:S(2)}, u32[]{:S(2)}) collective-permute-start(bf16[1,2560]{1,0:T(2,128)(2,1)S(1)} %pad_maximum_fusion.1), channel_id=1, source_target_pairs={{0,4},{4,8},{8,12},{12,16},{16,20},{20,24},{24,28},{1,5},{5,9},{9,... | collective-permute-start | bytes 15368 | tf_op jit(solution)/shard_map/ppermute | solution.py:369
  213.4 6.0 %collective-permute-start.27 = (bf16[1,2560]{1,0:T(2,128)(2,1)S(1)}, bf16[1,2560]{1,0:T(2,128)(2,1)S(1)}, u32[]{:S(2)}, u32[]{:S(2)}) collective-permute-start(bf16[1,2560]{1,0:T(2,128)(2,1)S(1)} %pad_maximum_fusion.2), channel_id=1, source_target_pairs={{4,0},{8,4},{12,8},{16,12},{20,16},{24,20},{28,24},{5,1},{9,5},{13... | collective-permute-start | bytes 15368 | tf_op jit(solution)/shard_map/ppermute | solution.py:370
  225.9 4.5 %collective-permute-start.38 = (bf16[512,512]{1,0:T(8,128)(2,1)S(1)}, bf16[512,512]{1,0:T(8,128)(2,1)S(1)}, u32[]{:S(2)}, u32[]{:S(2)}) collective-permute-start(bf16[512,512]{1,0:T(8,128)(2,1)S(1)} %get-tuple-element.52), channel_id=1, source_target_pairs={{0,1},{1,0},{2,3},{3,2},{4,5},{5,4},{6,7},{7,6},{8,9},{9,8},{10,11... | collective-permute-start | bytes 1572872 | tf_op jit(solution)/shard_map/ppermute | solution.py:48
  226.5 3.1 %collective-permute-start.46 = (bf16[512,256]{1,0:T(8,128)(2,1)S(1)}, bf16[512,256]{1,0:T(8,128)(2,1)S(1)}, u32[]{:S(2)}, u32[]{:S(2)}) collective-permute-start(bf16[512,256]{1,0:T(8,128)(2,1)S(1)} %shard_map.202), channel_id=1, source_target_pairs={{0,1},{1,0},{2,3},{3,2},{4,5},{5,4},{6,7},{7,6},{8,9},{9,8},{10,11... | collective-permute-start | bytes 786440 | tf_op jit(solution)/shard_map/ppermute | solution.py:48
  228.2 2.7 %collective-permute-start.42 = (bf16[512,512]{1,0:T(8,128)(2,1)S(1)}, bf16[512,512]{1,0:T(8,128)(2,1)S(1)}, u32[]{:S(2)}, u32[]{:S(2)}) collective-permute-start(bf16[512,512]{1,0:T(8,128)(2,1)S(1)} %get-tuple-element.54), channel_id=1, source_target_pairs={{0,1},{1,0},{2,3},{3,2},{4,5},{5,4},{6,7},{7,6},{8,9},{9,8},{10,11... | collective-permute-start | bytes 1572872 | tf_op jit(solution)/shard_map/ppermute | solution.py:48
  229.7 3.3 %collective-permute-start.47 = (bf16[512,256]{1,0:T(8,128)(2,1)S(1)}, bf16[512,256]{1,0:T(8,128)(2,1)S(1)}, u32[]{:S(2)}, u32[]{:S(2)}) collective-permute-start(bf16[512,256]{1,0:T(8,128)(2,1)S(1)} %fusion.28), channel_id=1, source_target_pairs={{1,3},{5,7},{8,10},{12,14},{19,17},{23,21},{26,24},{30,28}} | collective-permute-start | bytes 786440 | tf_op jit(solution)/shard_map/ppermute | solution.py:640
  230.6 8.4 %collective-permute-start.39 = (bf16[512,256]{1,0:T(8,128)(2,1)S(1)}, bf16[512,256]{1,0:T(8,128)(2,1)S(1)}, u32[]{:S(2)}, u32[]{:S(2)}) collective-permute-start(bf16[512,256]{1,0:T(8,128)(2,1)S(1)} %slice.554), channel_id=1, source_target_pairs={{0,2},{1,3},{2,0},{3,1},{4,6},{5,7},{6,4},{7,5},{8,10},{9,11},{10,... | collective-permute-start | bytes 786440 | tf_op jit(solution)/shard_map/ppermute | solution.py:48
  231.2 13.4 %collective-permute-start.43 = (bf16[512,256]{1,0:T(8,128)(2,1)S(1)}, bf16[512,256]{1,0:T(8,128)(2,1)S(1)}, u32[]{:S(2)}, u32[]{:S(2)}) collective-permute-start(bf16[512,256]{1,0:T(8,128)(2,1)S(1)} %slice.553), channel_id=1, source_target_pairs={{0,2},{1,3},{2,0},{3,1},{4,6},{5,7},{6,4},{7,5},{8,10},{9,11},{10,... | collective-permute-start | bytes 786440 | tf_op jit(solution)/shard_map/ppermute | solution.py:48

commit v5 on v4

--- a/solution.py
+++ b/solution.py
@@ -152,24 +152,25 @@
     window_ref = None if final else refs.pop(0)
     for way in range(2):
         got = got_refs[way][:STATE].astype(jnp.float32)
+        before = got
+        if not first:
+            held_decay = before_ref[way, STATE : STATE + 1]
+            before = got * held_decay + before_ref[way, :STATE]
+        if final:
+            refs[0][way] = before.astype(jnp.bfloat16)
+            continue
         got_decay = got_refs[way][STATE : STATE + 1].astype(jnp.float32) + got_refs[way][
             STATE + 1 : STATE + 2
         ].astype(jnp.float32)
-        before, before_decay = got, got_decay
-        if not first:
-            held_decay = before_ref[way, STATE : STATE + 1]
-            before = got * held_decay + before_ref[way, :STATE]
-            before_decay = got_decay * held_decay
-        if final:
-            refs[0][way] = before.astype(jnp.bfloat16)
-            continue
+        before_decay = got_decay if first else got_decay * held_decay
         decay = window_ref[way, STATE : STATE + 1]
         state = got * decay + window_ref[way, :STATE]
         decay = decay * got_decay
         for ref, value, factor in ((refs[0], before, before_decay), (refs[1], state, decay)):
             ref[way, :STATE] = value
             ref[way, STATE:] = jnp.broadcast_to(factor, (8, factor.shape[1]))
-        refs[2 + way][...] = message(state, decay)
+        alone = refs[2 + way].shape[0] == STATE
+        refs[2 + way][...] = state.astype(jnp.bfloat16) if alone else message(state, decay)
 
 
 def within_kernel(values_ref, inputs_ref, readout_ref, rows_ref, cols_ref, out_ref):
@@ -512,7 +513,8 @@
             final = 2 * offset >= sp_count
             outs = [((2, STATE, channels), jnp.bfloat16)]
             if not final:
-                outs = [wide_state, wide_state, sent, sent]
+                next_sent = ((STATE, channels), jnp.bfloat16) if 4 * offset >= sp_count else sent
+                outs = [wide_state, wide_state, next_sent, next_sent]
             result = call(
                 functools.partial(link_kernel, offset == 1, final),
                 outs,

time: 249 us -> 249 us (level)
  no operation moved by 1% of the time
where the time goes in v5:
time: 249 us; the launch traced here: 246 us
  waiting for transfers between devices  147 us (59%)
  starting transfers between devices  59.3 us (24%)
  Pallas kernels  21.2 us (9%)
  other arithmetic  9.46 us (4%)
  local copies, waits for them, and re-layouts  7.46 us (3%)
    ppermute x28, waiting for transfers between devices, send_on(): return lax.ppermute(array, 'sp', pairs)  108 us
    ppermute x28, starting transfers between devices, send_on(): return lax.ppermute(array, 'sp', pairs)  25.8 us
    pallas_call x13, Pallas kernels, call(): pl.pallas_call(kernel, out_shape=[jax.ShapeDtypeStruct(shape, kind) for s...  21.2 us
    ppermute x9, waiting for transfers between devices, swap(): lax.ppermute(array, 'tp', [(i, i ^ 1 << bit) for i in range(self.count)])  14.1 us
    ppermute x3, starting transfers between devices, shards(): got_f = lax.ppermute(send_f, 'sp', forward)  13.3 us
    ppermute x3, waiting for transfers between devices, shards(): got_b = lax.ppermute(send_b, 'sp', [(b, a) for a, b in forward])  12.9 us
    ppermute x2, starting transfers between devices, edges(): low = lax.ppermute(last, 'sp', forward)  7.53 us
    ppermute x9, starting transfers between devices, swap(): lax.ppermute(array, 'tp', [(i, i ^ 1 << bit) for i in range(self.count)])  5.57 us
  transfers between devices with their start and end apart: 48, of which 22 were waited for; matrix products, arithmetic and copies ran while one was open for 3% of the time, Pallas kernels for 7%

profile of v5, /device:TPU:0, one launch (start us, length us, event | category | flops | bytes accessed | tf_op | source)
XLA Modules:
  0.0 245.5 jit_solution(16623404563124158028)
XLA Ops:
  1.5 4.9 %collective-permute-start = (bf16[3,1024]{1,0:T(4,128)(2,1)S(1)}, bf16[3,1024]{1,0:T(4,128)(2,1)S(1)}, u32[]{:S(2)}, u32[]{:S(2)}) collective-permute-start(bf16[3,1024]{1,0:T(4,128)(2,1)S(1)} %pad_maximum_fusion.3), channel_id=1, source_target_pairs={{0,4},{4,8},{8,12},{12,16},{16,20},{20,24},{24,28},{1,5},{5,9},{9,... | collective-permute-start | bytes 18440 | tf_op jit(solution)/shard_map/ppermute | solution.py:370
  6.4 1.3 collective-permute-start.1
  7.7 1.0 fusion.40
  8.7 1.0 fusion.46
  11.9 1.2 shard_map.190
  13.1 1.0 maximum_convert_fusion.3
  14.2 1.2 maximum_convert_fusion.2
  15.9 1.1 multiply_convert_fusion.values_ref
  17.4 4.6 %collective-permute-start.2 = (bf16[136,512]{1,0:T(8,128)(2,1)S(1)}, bf16[136,512]{1,0:T(8,128)(2,1)S(1)}, u32[]{:S(2)}, u32[]{:S(2)}) collective-permute-start(bf16[136,512]{1,0:T(8,128)(2,1)S(1)} %get-tuple-element.34), channel_id=1, source_target_pairs={{0,4},{4,8},{8,12},{12,16},{16,20},{20,24},{24,28},{1,5},{5,9},{9,... | collective-permute-start | bytes 417800 | tf_op jit(solution)/shard_map/ppermute | solution.py:511
  22.0 1.3 collective-permute-start.3
  23.3 1.2 collective-permute-done.2.refs_0_
  24.6 4.8 %collective-permute-done.3.refs_1_ = bf16[136,512]{1,0:T(8,128)(2,1)S(1)} collective-permute-done((bf16[136,512]{1,0:T(8,128)(2,1)S(1)}, bf16[136,512]{1,0:T(8,128)(2,1)S(1)}, u32[]{:S(2)}, u32[]{:S(2)}) %collective-permute-start.3) | collective-permute-done | bytes 139296 | tf_op jit(solution)/shard_map/ppermute | solution.py:512
  29.5 4.4 %collective-permute-start.4 = (bf16[136,512]{1,0:T(8,128)(2,1)S(1)}, bf16[136,512]{1,0:T(8,128)(2,1)S(1)}, u32[]{:S(2)}, u32[]{:S(2)}) collective-permute-start(bf16[136,512]{1,0:T(8,128)(2,1)S(1)} %get-tuple-element.37), channel_id=1, source_target_pairs={{0,8},{4,12},{8,16},{12,20},{16,24},{20,28},{1,9},{5,13},{9,17},{1... | collective-permute-start | bytes 417800 | tf_op jit(solution)/shard_map/ppermute | solution.py:511
  33.9 1.3 collective-permute-start.5
  36.5 4.3 %collective-permute-done.5.refs_1_ = bf16[136,512]{1,0:T(8,128)(2,1)S(1)} collective-permute-done((bf16[136,512]{1,0:T(8,128)(2,1)S(1)}, bf16[136,512]{1,0:T(8,128)(2,1)S(1)}, u32[]{:S(2)}, u32[]{:S(2)}) %collective-permute-start.5) | collective-permute-done | bytes 139296 | tf_op jit(solution)/shard_map/ppermute | solution.py:512
  40.9 0.9 shard_map.194
  41.8 4.3 %collective-permute-start.6 = (bf16[128,512]{1,0:T(8,128)(2,1)S(1)}, bf16[128,512]{1,0:T(8,128)(2,1)S(1)}, u32[]{:S(2)}, u32[]{:S(2)}) collective-permute-start(bf16[128,512]{1,0:T(8,128)(2,1)S(1)} %get-tuple-element.41), channel_id=1, source_target_pairs={{0,16},{4,20},{8,24},{12,28},{1,17},{5,21},{9,25},{13,29},{2,18},{... | collective-permute-start | bytes 393224 | tf_op jit(solution)/shard_map/ppermute | solution.py:511
  46.1 1.3 collective-permute-start.7
  48.0 2.7 %shard_map.191.within_ref = f32[512,512]{1,0:T(8,128)S(1)} custom-call(bf16[512,512]{1,0:T(8,128)(2,1)S(1)} %multiply_convert_fusion.values_ref, bf16[512,256]{1,0:T(8,128)(2,1)S(1)} %multiply_convert_fusion.2.inputs_ref, bf16[512,256]{1,0:T(8,128)(2,1)S(1)} %multiply_convert_fusion.1.readout_ref, f32[3,8,512]{2,1,0:T(8,128)S(1)} %get-tuple-element.30.rows_ref, ...), custom_call_target="tpu_custom_call" | custom-call | tf_op jit(solution)/shard_map/pallas_call | solution.py:377
  50.7 3.8 %collective-permute-done.7.refs_1_ = bf16[128,512]{1,0:T(8,128)(2,1)S(1)} collective-permute-done((bf16[128,512]{1,0:T(8,128)(2,1)S(1)}, bf16[128,512]{1,0:T(8,128)(2,1)S(1)}, u32[]{:S(2)}, u32[]{:S(2)}) %collective-permute-start.7) | collective-permute-done | bytes 131104 | tf_op jit(solution)/shard_map/ppermute | solution.py:512
  54.5 2.8 %shard_map.196 = (bf16[512,1024]{1,0:T(8,128)(2,1)S(1)}, bf16[512,1024]{1,0:T(8,128)(2,1)S(1)}) custom-call(s32[24]{0:T(128)S(1)} %get-tuple-element.80.info_ref.refs_0_, f32[512,512]{1,0:T(8,128)S(1)} %shard_map.191.within_ref, bf16[512,256]{1,0:T(8,128)(2,1)S(1)} %multiply_convert_fusion.1.readout_ref, f32[2,512,8]{2,1,0:T(8,128)S(1)} %get-tuple-element.31.cols_ref, ...), custom_call_target="tpu_custom_call" | custom-call | tf_op jit(solution)/shard_map/pallas_call | solution.py:377
  57.4 2.6 %collective-permute-done.8 = bf16[512,1024]{1,0:T(8,128)(2,1)S(1)} collective-permute-done((bf16[512,1024]{1,0:T(8,128)(2,1)S(1)}, bf16[512,1024]{1,0:T(8,128)(2,1)S(1)}, u32[]{:S(2)}, u32[]{:S(2)}) %collective-permute-start.8) | collective-permute-done | bytes 1048608 | tf_op jit(solution)/shard_map/ppermute | solution.py:48
  60.5 1.5 collective-permute-start.9
  62.1 0.9 collective-permute-start.28
  63.0 1.2 collective-permute-start.31
  65.1 7.7 %collective-permute-done.28.refs_4_ = bf16[1280,128]{1,0:T(8,128)(2,1)S(1)} collective-permute-done((bf16[1280,128]{1,0:T(8,128)(2,1)S(1)}, bf16[1280,128]{1,0:T(8,128)(2,1)S(1)}, u32[]{:S(2)}, u32[]{:S(2)}) %collective-permute-start.28) | collective-permute-done | bytes 327712 | tf_op jit(solution)/shard_map/ppermute | solution.py:410
  73.4 6.4 %collective-permute-done.29.refs_5_ = bf16[1280,128]{1,0:T(8,128)(2,1)S(1)} collective-permute-done((bf16[1280,128]{1,0:T(8,128)(2,1)S(1)}, bf16[1280,128]{1,0:T(8,128)(2,1)S(1)}, u32[]{:S(2)}, u32[]{:S(2)}) %collective-permute-start.29) | collective-permute-done | bytes 327712 | tf_op jit(solution)/shard_map/ppermute | solution.py:410
  80.6 1.2 collective-permute-start.30
  82.0 26.3 %collective-permute-done.30.refs_6_ = bf16[1280,128]{1,0:T(8,128)(2,1)S(1)} collective-permute-done((bf16[1280,128]{1,0:T(8,128)(2,1)S(1)}, bf16[1280,128]{1,0:T(8,128)(2,1)S(1)}, u32[]{:S(2)}, u32[]{:S(2)}) %collective-permute-start.30) | collective-permute-done | bytes 327712 | tf_op jit(solution)/shard_map/ppermute | solution.py:410
  108.4 1.1 collective-permute-start.10
  110.3 1.2 collective-permute-start.35
  112.3 1.2 collective-permute-start.21
  113.5 6.5 %collective-permute-done.32.refs_8_ = bf16[1280,128]{1,0:T(8,128)(2,1)S(1)} collective-permute-done((bf16[1280,128]{1,0:T(8,128)(2,1)S(1)}, bf16[1280,128]{1,0:T(8,128)(2,1)S(1)}, u32[]{:S(2)}, u32[]{:S(2)}) %collective-permute-start.32) | collective-permute-done | bytes 327712 | tf_op jit(solution)/shard_map/ppermute | solution.py:410
  120.8 1.2 collective-permute-start.15
  123.0 18.1 %collective-permute-done.33.refs_9_ = bf16[1280,128]{1,0:T(8,128)(2,1)S(1)} collective-permute-done((bf16[1280,128]{1,0:T(8,128)(2,1)S(1)}, bf16[1280,128]{1,0:T(8,128)(2,1)S(1)}, u32[]{:S(2)}, u32[]{:S(2)}) %collective-permute-start.33) | collective-permute-done | bytes 327712 | tf_op jit(solution)/shard_map/ppermute | solution.py:410
  141.1 0.8 collective-permute-start.16
  141.9 1.2 collective-permute-start.23
  143.1 2.1 collective-permute-done.15.refs_9_
  145.3 1.1 collective-permute-start.17
  146.4 8.7 %collective-permute-done.20.refs_15_ = bf16[256,1280]{1,0:T(8,128)(2,1)S(1)} collective-permute-done((bf16[256,1280]{1,0:T(8,128)(2,1)S(1)}, bf16[256,1280]{1,0:T(8,128)(2,1)S(1)}, u32[]{:S(2)}, u32[]{:S(2)}) %collective-permute-start.20) | collective-permute-done | bytes 655392 | tf_op jit(solution)/shard_map/ppermute | solution.py:410
  156.0 13.2 %collective-permute-done.16.refs_10_ = bf16[256,1280]{1,0:T(8,128)(2,1)S(1)} collective-permute-done((bf16[256,1280]{1,0:T(8,128)(2,1)S(1)}, bf16[256,1280]{1,0:T(8,128)(2,1)S(1)}, u32[]{:S(2)}, u32[]{:S(2)}) %collective-permute-start.16) | collective-permute-done | bytes 655392 | tf_op jit(solution)/shard_map/ppermute | solution.py:410
  170.0 1.2 collective-permute-start.25
  171.2 2.4 collective-permute-done.17.refs_11_
  173.6 1.2 collective-permute-start.34
  174.8 8.4 %collective-permute-done.22.refs_17_ = bf16[256,1280]{1,0:T(8,128)(2,1)S(1)} collective-permute-done((bf16[256,1280]{1,0:T(8,128)(2,1)S(1)}, bf16[256,1280]{1,0:T(8,128)(2,1)S(1)}, u32[]{:S(2)}, u32[]{:S(2)}) %collective-permute-start.22) | collective-permute-done | bytes 655392 | tf_op jit(solution)/shard_map/ppermute | solution.py:410
  184.0 1.2 collective-permute-start.41
  185.4 6.8 %shard_map.197 = (f32[512,1280]{1,0:T(8,128)S(1)}, f32[512,1280]{1,0:T(8,128)S(1)}, bf16[512,256]{1,0:T(8,128)(2,1)S(1)}) custom-call(s32[24]{0:T(128)S(1)} %get-tuple-element.80.info_ref.refs_0_, f32[1,2048]{1,0:T(1,128)S(1)} %bitcast.33, bf16[512,512]{1,0:T(8,128)(2,1)S(1)} %fusion.7.refs_2_, bf16[512,512]{1,0:T(8,128)(2,1)S(1)} %collective-permute-done.10.refs_3_, ...), custom_call_target="tpu_custom_call" | custom-call | tf_op jit(solution)/shard_map/pallas_call | solution.py:377
  192.2 2.4 collective-permute-done.34.refs_10_
  194.6 1.2 collective-permute-start.37
  195.9 5.7 %collective-permute-done.36.refs_3_ = bf16[1280,128]{1,0:T(8,128)(2,1)S(1)} collective-permute-done((bf16[1280,128]{1,0:T(8,128)(2,1)S(1)}, bf16[1280,128]{1,0:T(8,128)(2,1)S(1)}, u32[]{:S(2)}, u32[]{:S(2)}) %collective-permute-start.36) | collective-permute-done | bytes 327712 | tf_op jit(solution)/shard_map/ppermute | solution.py:410
  203.1 1.3 collective-permute-start.45
  204.4 0.8 shard_map.198
  205.4 2.6 %collective-permute-start.26 = (bf16[1,2560]{1,0:T(2,128)(2,1)S(1)}, bf16[1,2560]{1,0:T(2,128)(2,1)S(1)}, u32[]{:S(2)}, u32[]{:S(2)}) collective-permute-start(bf16[1,2560]{1,0:T(2,128)(2,1)S(1)} %pad_maximum_fusion.1), channel_id=1, source_target_pairs={{0,4},{4,8},{8,12},{12,16},{16,20},{20,24},{24,28},{1,5},{5,9},{9,... | collective-permute-start | bytes 15368 | tf_op jit(solution)/shard_map/ppermute | solution.py:370
  208.0 5.2 %collective-permute-done.26 = bf16[1,2560]{1,0:T(2,128)(2,1)S(1)} collective-permute-done((bf16[1,2560]{1,0:T(2,128)(2,1)S(1)}, bf16[1,2560]{1,0:T(2,128)(2,1)S(1)}, u32[]{:S(2)}, u32[]{:S(2)}) %collective-permute-start.26) | collective-permute-done | bytes 5152 | tf_op jit(solution)/shard_map/ppermute | solution.py:370
  213.2 1.3 collective-permute-start.27
  214.6 4.7 %collective-permute-done.27 = bf16[1,2560]{1,0:T(2,128)(2,1)S(1)} collective-permute-done((bf16[1,2560]{1,0:T(2,128)(2,1)S(1)}, bf16[1,2560]{1,0:T(2,128)(2,1)S(1)}, u32[]{:S(2)}, u32[]{:S(2)}) %collective-permute-start.27) | collective-permute-done | bytes 5152 | tf_op jit(solution)/shard_map/ppermute | solution.py:371
  219.8 2.1 fusion.2.refs_1_.hidden_ref
  222.0 2.5 %shard_map.199.refs_2_ = bf16[8,512,256]{2,1,0:T(8,128)(2,1)S(1)} custom-call(s32[24]{0:T(128)S(1)} %get-tuple-element.80.info_ref.refs_0_, bf16[512,1280]{1,0:T(8,128)(2,1)S(1)} %fusion.2.refs_1_.hidden_ref, bf16[1280,128]{1,0:T(8,128)(2,1)S(1)} %get-tuple-element.68.refs_2_, bf16[1280,128]{1,0:T(8,128)(2,1)S(1)} %get-tuple-element.67.refs_3_, ...), custom_call_target="tpu_custom_call" | custom-call | tf_op jit(solution)/shard_map/pallas_call | solution.py:377
  224.5 1.2 shard_map.200
  226.9 1.2 shard_map.201
  231.0 1.8 collective-permute-start.43
  232.9 5.9 %collective-permute-done.39 = bf16[512,256]{1,0:T(8,128)(2,1)S(1)} collective-permute-done((bf16[512,256]{1,0:T(8,128)(2,1)S(1)}, bf16[512,256]{1,0:T(8,128)(2,1)S(1)}, u32[]{:S(2)}, u32[]{:S(2)}) %collective-permute-start.39) | collective-permute-done | bytes 262176 | tf_op jit(solution)/shard_map/ppermute | solution.py:48
  238.9 5.5 %collective-permute-done.43 = bf16[512,256]{1,0:T(8,128)(2,1)S(1)} collective-permute-done((bf16[512,256]{1,0:T(8,128)(2,1)S(1)}, bf16[512,256]{1,0:T(8,128)(2,1)S(1)}, u32[]{:S(2)}, u32[]{:S(2)}) %collective-permute-start.43) | collective-permute-done | bytes 262176 | tf_op jit(solution)/shard_map/ppermute | solution.py:48
  244.5 1.0 fusion.15
  (119 shorter events, 21.8 us)
Async XLA Ops:
  1.5 11.6 %collective-permute-start = (bf16[3,1024]{1,0:T(4,128)(2,1)S(1)}, bf16[3,1024]{1,0:T(4,128)(2,1)S(1)}, u32[]{:S(2)}, u32[]{:S(2)}) collective-permute-start(bf16[3,1024]{1,0:T(4,128)(2,1)S(1)} %pad_maximum_fusion.3), channel_id=1, source_target_pairs={{0,4},{4,8},{8,12},{12,16},{16,20},{20,24},{24,28},{1,5},{5,9},{9,... | collective-permute-start | bytes 18440 | tf_op jit(solution)/shard_map/ppermute | solution.py:370
  6.4 6.7 %collective-permute-start.1 = (bf16[3,1024]{1,0:T(4,128)(2,1)S(1)}, bf16[3,1024]{1,0:T(4,128)(2,1)S(1)}, u32[]{:S(2)}, u32[]{:S(2)}) collective-permute-start(bf16[3,1024]{1,0:T(4,128)(2,1)S(1)} %pad_maximum_fusion.4), channel_id=1, source_target_pairs={{4,0},{8,4},{12,8},{16,12},{20,16},{24,20},{28,24},{5,1},{9,5},{13... | collective-permute-start | bytes 18440 | tf_op jit(solution)/shard_map/ppermute | solution.py:371
  10.4 0.8 copy-start.4
  11.2 0.8 copy-start.5
  17.0 6.3 %copy-start.13 = (f32[7,256]{1,0:T(8,128)S(1)}, f32[7,256]{1,0:T(8,128)}, u32[]{:S(2)}) copy-start(f32[7,256]{1,0:T(8,128)} %param.30) | copy-start | bytes 21508
  17.0 18.9 %copy-start.10 = (bf16[512,256]{1,0:T(8,128)(2,1)S(1)}, bf16[512,256]{1,0:T(8,128)(2,1)}, u32[]{:S(2)}) copy-start(bf16[512,256]{1,0:T(8,128)(2,1)} %param.24) | copy-start | bytes 786436
  17.4 7.1 %collective-permute-start.2 = (bf16[136,512]{1,0:T(8,128)(2,1)S(1)}, bf16[136,512]{1,0:T(8,128)(2,1)S(1)}, u32[]{:S(2)}, u32[]{:S(2)}) collective-permute-start(bf16[136,512]{1,0:T(8,128)(2,1)S(1)} %get-tuple-element.34), channel_id=1, source_target_pairs={{0,4},{4,8},{8,12},{12,16},{16,20},{20,24},{24,28},{1,5},{5,9},{9,... | collective-permute-start | bytes 417800 | tf_op jit(solution)/shard_map/ppermute | solution.py:511
  22.0 7.4 %collective-permute-start.3 = (bf16[136,512]{1,0:T(8,128)(2,1)S(1)}, bf16[136,512]{1,0:T(8,128)(2,1)S(1)}, u32[]{:S(2)}, u32[]{:S(2)}) collective-permute-start(bf16[136,512]{1,0:T(8,128)(2,1)S(1)} %get-tuple-element.35), channel_id=1, source_target_pairs={{4,0},{8,4},{12,8},{16,12},{20,16},{24,20},{28,24},{5,1},{9,5},{13... | collective-permute-start | bytes 417800 | tf_op jit(solution)/shard_map/ppermute | solution.py:512
  29.5 7.1 %collective-permute-start.4 = (bf16[136,512]{1,0:T(8,128)(2,1)S(1)}, bf16[136,512]{1,0:T(8,128)(2,1)S(1)}, u32[]{:S(2)}, u32[]{:S(2)}) collective-permute-start(bf16[136,512]{1,0:T(8,128)(2,1)S(1)} %get-tuple-element.37), channel_id=1, source_target_pairs={{0,8},{4,12},{8,16},{12,20},{16,24},{20,28},{1,9},{5,13},{9,17},{1... | collective-permute-start | bytes 417800 | tf_op jit(solution)/shard_map/ppermute | solution.py:511
  33.9 6.9 %collective-permute-start.5 = (bf16[136,512]{1,0:T(8,128)(2,1)S(1)}, bf16[136,512]{1,0:T(8,128)(2,1)S(1)}, u32[]{:S(2)}, u32[]{:S(2)}) collective-permute-start(bf16[136,512]{1,0:T(8,128)(2,1)S(1)} %get-tuple-element.38), channel_id=1, source_target_pairs={{8,0},{12,4},{16,8},{20,12},{24,16},{28,20},{9,1},{13,5},{17,9},{2... | collective-permute-start | bytes 417800 | tf_op jit(solution)/shard_map/ppermute | solution.py:512
  41.8 8.9 %collective-permute-start.6 = (bf16[128,512]{1,0:T(8,128)(2,1)S(1)}, bf16[128,512]{1,0:T(8,128)(2,1)S(1)}, u32[]{:S(2)}, u32[]{:S(2)}) collective-permute-start(bf16[128,512]{1,0:T(8,128)(2,1)S(1)} %get-tuple-element.41), channel_id=1, source_target_pairs={{0,16},{4,20},{8,24},{12,28},{1,17},{5,21},{9,25},{13,29},{2,18},{... | collective-permute-start | bytes 393224 | tf_op jit(solution)/shard_map/ppermute | solution.py:511
  46.1 8.4 %collective-permute-start.7 = (bf16[128,512]{1,0:T(8,128)(2,1)S(1)}, bf16[128,512]{1,0:T(8,128)(2,1)S(1)}, u32[]{:S(2)}, u32[]{:S(2)}) collective-permute-start(bf16[128,512]{1,0:T(8,128)(2,1)S(1)} %get-tuple-element.42), channel_id=1, source_target_pairs={{16,0},{20,4},{24,8},{28,12},{17,1},{21,5},{25,9},{29,13},{18,2},{... | collective-permute-start | bytes 393224 | tf_op jit(solution)/shard_map/ppermute | solution.py:512
  47.9 6.6 %copy-start = (bf16[512,2048]{1,0:T(8,128)(2,1)S(1)}, bf16[512,2048]{1,0:T(8,128)(2,1)}, u32[]{:S(2)}) copy-start(bf16[512,2048]{1,0:T(8,128)(2,1)} %map_ref.1) | copy-start | bytes 6291460
  47.9 6.6 %copy-start.3 = (bf16[512,512]{1,0:T(8,128)(2,1)S(1)}, bf16[512,512]{1,0:T(8,128)(2,1)}, u32[]{:S(2)}) copy-start(bf16[512,512]{1,0:T(8,128)(2,1)} %valve_ref.1) | copy-start | bytes 1572868
  47.9 6.6 %copy-start.7 = (f32[512]{0:T(512)S(1)}, f32[512]{0:T(512)}, u32[]{:S(2)}) copy-start(f32[512]{0:T(512)} %param.31) | copy-start | bytes 6148
  57.3 2.7 %collective-permute-start.8 = (bf16[512,1024]{1,0:T(8,128)(2,1)S(1)}, bf16[512,1024]{1,0:T(8,128)(2,1)S(1)}, u32[]{:S(2)}, u32[]{:S(2)}) collective-permute-start(bf16[512,1024]{1,0:T(8,128)(2,1)S(1)} %get-tuple-element.45), channel_id=1, source_target_pairs={{0,1},{1,0},{2,3},{3,2},{4,5},{5,4},{6,7},{7,6},{8,9},{9,8},{10,11... | collective-permute-start | bytes 3145736 | tf_op jit(solution)/shard_map/ppermute | solution.py:48
  60.0 2.0 copy-start.8
  60.0 5.0 %copy-start.1 = (bf16[256,1280]{1,0:T(8,128)(2,1)S(1)}, bf16[256,1280]{1,0:T(8,128)(2,1)}, u32[]{:S(2)}) copy-start(bf16[256,1280]{1,0:T(8,128)(2,1)} %refs_5_.1) | copy-start | bytes 1966084
  60.0 12.7 %copy-start.2 = (bf16[256,1280]{1,0:T(8,128)(2,1)S(1)}, bf16[256,1280]{1,0:T(8,128)(2,1)}, u32[]{:S(2)}) copy-start(bf16[256,1280]{1,0:T(8,128)(2,1)} %refs_12_.1) | copy-start | bytes 1966084
  60.0 21.8 %copy-start.9 = (bf16[512,512]{1,0:T(8,128)(2,1)S(1)}, bf16[512,512]{1,0:T(8,128)(2,1)}, u32[]{:S(2)}) copy-start(bf16[512,512]{1,0:T(8,128)(2,1)} %param.20) | copy-start | bytes 1572868
  60.5 20.1 %collective-permute-start.9 = (bf16[512,512]{1,0:T(8,128)(2,1)S(1)}, bf16[512,512]{1,0:T(8,128)(2,1)S(1)}, u32[]{:S(2)}, u32[]{:S(2)}) collective-permute-start(bf16[512,512]{1,0:T(8,128)(2,1)S(1)} %slice.552), channel_id=1, source_target_pairs={{0,2},{1,3},{2,0},{3,1},{4,6},{5,7},{6,4},{7,5},{8,10},{9,11},{10,... | collective-permute-start | bytes 1572872 | tf_op jit(solution)/shard_map/ppermute | solution.py:48
  62.1 123.2 %copy-start.11 = (f32[3,1280]{1,0:T(4,128)S(1)}, f32[3,1280]{1,0:T(4,128)}, u32[]{:S(2)}) copy-start(f32[3,1280]{1,0:T(4,128)} %param.37) | copy-start | bytes 46084
  62.1 123.2 %copy-start.12 = (f32[3,1280]{1,0:T(4,128)S(1)}, f32[3,1280]{1,0:T(4,128)}, u32[]{:S(2)}) copy-start(f32[3,1280]{1,0:T(4,128)} %param.36) | copy-start | bytes 46084
  62.1 123.2 %copy-start.6 = (f32[2048]{0:T(1024)S(1)}, f32[2048]{0:T(1024)}, u32[]{:S(2)}) copy-start(f32[2048]{0:T(1024)} %param.33) | copy-start | bytes 24580
  62.1 10.6 %collective-permute-start.28 = (bf16[1280,128]{1,0:T(8,128)(2,1)S(1)}, bf16[1280,128]{1,0:T(8,128)(2,1)S(1)}, u32[]{:S(2)}, u32[]{:S(2)}) collective-permute-start(bf16[1280,128]{1,0:T(8,128)(2,1)S(1)} %get-tuple-element.68.refs_2_), channel_id=1, source_target_pairs={{4,12},{12,20},{20,28},{28,24},{24,16},{16,8},{8,0},{0,4},{5,13},{... | collective-permute-start | bytes 983048 | tf_op jit(solution)/shard_map/ppermute | solution.py:410
  63.0 9.8 %collective-permute-start.31 = (bf16[1280,128]{1,0:T(8,128)(2,1)S(1)}, bf16[1280,128]{1,0:T(8,128)(2,1)S(1)}, u32[]{:S(2)}, u32[]{:S(2)}) collective-permute-start(bf16[1280,128]{1,0:T(8,128)(2,1)S(1)} %get-tuple-element.67.refs_3_), channel_id=1, source_target_pairs={{12,4},{20,12},{28,20},{24,28},{16,24},{8,16},{0,8},{4,0},{13,5},{... | collective-permute-start | bytes 983048 | tf_op jit(solution)/shard_map/ppermute | solution.py:410
  64.2 15.6 %collective-permute-start.29 = (bf16[1280,128]{1,0:T(8,128)(2,1)S(1)}, bf16[1280,128]{1,0:T(8,128)(2,1)S(1)}, u32[]{:S(2)}, u32[]{:S(2)}) collective-permute-start(bf16[1280,128]{1,0:T(8,128)(2,1)S(1)} %get-tuple-element.67.refs_3_), channel_id=1, source_target_pairs={{4,12},{12,20},{20,28},{28,24},{24,16},{16,8},{8,0},{0,4},{5,13},{... | collective-permute-start | bytes 983048 | tf_op jit(solution)/shard_map/ppermute | solution.py:410
  65.0 44.4 %collective-permute-start.12 = (bf16[256,1280]{1,0:T(8,128)(2,1)S(1)}, bf16[256,1280]{1,0:T(8,128)(2,1)S(1)}, u32[]{:S(2)}, u32[]{:S(2)}) collective-permute-start(bf16[256,1280]{1,0:T(8,128)(2,1)S(1)} %copy-done.1), channel_id=1, source_target_pairs={{4,12},{12,20},{20,28},{28,24},{24,16},{16,8},{8,0},{0,4},{5,13},{... | collective-permute-start | bytes 1966088 | tf_op jit(solution)/shard_map/ppermute | solution.py:410
  72.8 37.5 %collective-permute-start.19 = (bf16[256,1280]{1,0:T(8,128)(2,1)S(1)}, bf16[256,1280]{1,0:T(8,128)(2,1)S(1)}, u32[]{:S(2)}, u32[]{:S(2)}) collective-permute-start(bf16[256,1280]{1,0:T(8,128)(2,1)S(1)} %copy-done.2), channel_id=1, source_target_pairs={{12,4},{20,12},{28,20},{24,28},{16,24},{8,16},{0,8},{4,0},{13,5},{... | collective-permute-start | bytes 1966088 | tf_op jit(solution)/shard_map/ppermute | solution.py:410
  72.8 38.7 %collective-permute-start.13 = (bf16[256,1280]{1,0:T(8,128)(2,1)S(1)}, bf16[256,1280]{1,0:T(8,128)(2,1)S(1)}, u32[]{:S(2)}, u32[]{:S(2)}) collective-permute-start(bf16[256,1280]{1,0:T(8,128)(2,1)S(1)} %copy-done.1), channel_id=1, source_target_pairs={{12,4},{20,12},{28,20},{24,28},{16,24},{8,16},{0,8},{4,0},{13,5},{... | collective-permute-start | bytes 1966088 | tf_op jit(solution)/shard_map/ppermute | solution.py:410
  79.8 32.5 %collective-permute-start.18 = (bf16[256,1280]{1,0:T(8,128)(2,1)S(1)}, bf16[256,1280]{1,0:T(8,128)(2,1)S(1)}, u32[]{:S(2)}, u32[]{:S(2)}) collective-permute-start(bf16[256,1280]{1,0:T(8,128)(2,1)S(1)} %copy-done.2), channel_id=1, source_target_pairs={{4,12},{12,20},{20,28},{28,24},{24,16},{16,8},{8,0},{0,4},{5,13},{... | collective-permute-start | bytes 1966088 | tf_op jit(solution)/shard_map/ppermute | solution.py:410
  80.6 27.8 %collective-permute-start.30 = (bf16[1280,128]{1,0:T(8,128)(2,1)S(1)}, bf16[1280,128]{1,0:T(8,128)(2,1)S(1)}, u32[]{:S(2)}, u32[]{:S(2)}) collective-permute-start(bf16[1280,128]{1,0:T(8,128)(2,1)S(1)} %get-tuple-element.68.refs_2_), channel_id=1, source_target_pairs={{12,4},{20,12},{28,20},{24,28},{16,24},{8,16},{0,8},{4,0},{13,5},{... | collective-permute-start | bytes 983048 | tf_op jit(solution)/shard_map/ppermute | solution.py:410
  108.4 13.7 %collective-permute-start.10 = (bf16[512,512]{1,0:T(8,128)(2,1)S(1)}, bf16[512,512]{1,0:T(8,128)(2,1)S(1)}, u32[]{:S(2)}, u32[]{:S(2)}) collective-permute-start(bf16[512,512]{1,0:T(8,128)(2,1)S(1)} %fusion.7.refs_2_), channel_id=1, source_target_pairs={{0,2},{1,3},{2,0},{3,1},{4,6},{5,7},{6,4},{7,5},{8,10},{9,11},{10,... | collective-permute-start | bytes 1572872 | tf_op jit(solution)/shard_map/ppermute | solution.py:48
  109.4 10.6 %collective-permute-start.32 = (bf16[1280,128]{1,0:T(8,128)(2,1)S(1)}, bf16[1280,128]{1,0:T(8,128)(2,1)S(1)}, u32[]{:S(2)}, u32[]{:S(2)}) collective-permute-start(bf16[1280,128]{1,0:T(8,128)(2,1)S(1)} %collective-permute-done.28.refs_4_), channel_id=1, source_target_pairs={{4,12},{12,20},{20,28},{28,24},{24,16},{16,8},{8,0},{0,4},{5,13},{... | collective-permute-start | bytes 983048 | tf_op jit(solution)/shard_map/ppermute | solution.py:410
  110.3 10.6 %collective-permute-start.35 = (bf16[1280,128]{1,0:T(8,128)(2,1)S(1)}, bf16[1280,128]{1,0:T(8,128)(2,1)S(1)}, u32[]{:S(2)}, u32[]{:S(2)}) collective-permute-start(bf16[1280,128]{1,0:T(8,128)(2,1)S(1)} %collective-permute-done.31.refs_7_), channel_id=1, source_target_pairs={{12,4},{20,12},{28,20},{24,28},{16,24},{8,16},{0,8},{4,0},{13,5},{... | collective-permute-start | bytes 983048 | tf_op jit(solution)/shard_map/ppermute | solution.py:410
  111.5 29.6 %collective-permute-start.14 = (bf16[256,1280]{1,0:T(8,128)(2,1)S(1)}, bf16[256,1280]{1,0:T(8,128)(2,1)S(1)}, u32[]{:S(2)}, u32[]{:S(2)}) collective-permute-start(bf16[256,1280]{1,0:T(8,128)(2,1)S(1)} %collective-permute-done.12.refs_6_), channel_id=1, source_target_pairs={{4,12},{12,20},{20,28},{28,24},{24,16},{16,8},{8,0},{0,4},{5,13},{... | collective-permute-start | bytes 1966088 | tf_op jit(solution)/shard_map/ppermute | solution.py:410
  112.3 29.6 %collective-permute-start.21 = (bf16[256,1280]{1,0:T(8,128)(2,1)S(1)}, bf16[256,1280]{1,0:T(8,128)(2,1)S(1)}, u32[]{:S(2)}, u32[]{:S(2)}) collective-permute-start(bf16[256,1280]{1,0:T(8,128)(2,1)S(1)} %collective-permute-done.19.refs_14_), channel_id=1, source_target_pairs={{12,4},{20,12},{28,20},{24,28},{16,24},{8,16},{0,8},{4,0},{13,5},{... | collective-permute-start | bytes 1966088 | tf_op jit(solution)/shard_map/ppermute | solution.py:410
  120.0 21.1 %collective-permute-start.33 = (bf16[1280,128]{1,0:T(8,128)(2,1)S(1)}, bf16[1280,128]{1,0:T(8,128)(2,1)S(1)}, u32[]{:S(2)}, u32[]{:S(2)}) collective-permute-start(bf16[1280,128]{1,0:T(8,128)(2,1)S(1)} %collective-permute-done.29.refs_5_), channel_id=1, source_target_pairs={{4,12},{12,20},{20,28},{28,24},{24,16},{16,8},{8,0},{0,4},{5,13},{... | collective-permute-start | bytes 983048 | tf_op jit(solution)/shard_map/ppermute | solution.py:410
  120.8 24.4 %collective-permute-start.15 = (bf16[256,1280]{1,0:T(8,128)(2,1)S(1)}, bf16[256,1280]{1,0:T(8,128)(2,1)S(1)}, u32[]{:S(2)}, u32[]{:S(2)}) collective-permute-start(bf16[256,1280]{1,0:T(8,128)(2,1)S(1)} %collective-permute-done.13.refs_7_), channel_id=1, source_target_pairs={{12,4},{20,12},{28,20},{24,28},{16,24},{8,16},{0,8},{4,0},{13,5},{... | collective-permute-start | bytes 1966088 | tf_op jit(solution)/shard_map/ppermute | solution.py:410
  122.1 33.1 %collective-permute-start.20 = (bf16[256,1280]{1,0:T(8,128)(2,1)S(1)}, bf16[256,1280]{1,0:T(8,128)(2,1)S(1)}, u32[]{:S(2)}, u32[]{:S(2)}) collective-permute-start(bf16[256,1280]{1,0:T(8,128)(2,1)S(1)} %collective-permute-done.18.refs_13_), channel_id=1, source_target_pairs={{4,12},{12,20},{20,28},{28,24},{24,16},{16,8},{8,0},{0,4},{5,13},{... | collective-permute-start | bytes 1966088 | tf_op jit(solution)/shard_map/ppermute | solution.py:410
  141.1 43.0 %collective-permute-start.11 = (bf16[512,1024]{1,0:T(8,128)(2,1)S(1)}, bf16[512,1024]{1,0:T(8,128)(2,1)S(1)}, u32[]{:S(2)}, u32[]{:S(2)}) collective-permute-start(bf16[512,1024]{1,0:T(8,128)(2,1)S(1)} %pad_maximum_fusion), channel_id=1, source_target_pairs={{0,1},{1,0},{2,3},{3,2},{4,5},{5,4},{6,7},{7,6},{8,9},{9,8},{10,11... | collective-permute-start | bytes 3145736 | tf_op jit(solution)/shard_map/ppermute | solution.py:48
  141.1 28.1 %collective-permute-start.16 = (bf16[256,1280]{1,0:T(8,128)(2,1)S(1)}, bf16[256,1280]{1,0:T(8,128)(2,1)S(1)}, u32[]{:S(2)}, u32[]{:S(2)}) collective-permute-start(bf16[256,1280]{1,0:T(8,128)(2,1)S(1)} %collective-permute-done.14.refs_8_), channel_id=1, source_target_pairs={{4,12},{12,20},{20,28},{28,24},{24,16},{16,8},{8,0},{0,4},{5,13},{... | collective-permute-start | bytes 1966088 | tf_op jit(solution)/shard_map/ppermute | solution.py:410
  141.9 28.1 %collective-permute-start.23 = (bf16[256,1280]{1,0:T(8,128)(2,1)S(1)}, bf16[256,1280]{1,0:T(8,128)(2,1)S(1)}, u32[]{:S(2)}, u32[]{:S(2)}) collective-permute-start(bf16[256,1280]{1,0:T(8,128)(2,1)S(1)} %collective-permute-done.21.refs_16_), channel_id=1, source_target_pairs={{12,4},{20,12},{28,20},{24,28},{16,24},{8,16},{0,8},{4,0},{13,5},{... | collective-permute-start | bytes 1966088 | tf_op jit(solution)/shard_map/ppermute | solution.py:410
  145.3 28.3 %collective-permute-start.17 = (bf16[256,1280]{1,0:T(8,128)(2,1)S(1)}, bf16[256,1280]{1,0:T(8,128)(2,1)S(1)}, u32[]{:S(2)}, u32[]{:S(2)}) collective-permute-start(bf16[256,1280]{1,0:T(8,128)(2,1)S(1)} %collective-permute-done.15.refs_9_), channel_id=1, source_target_pairs={{12,4},{20,12},{28,20},{24,28},{16,24},{8,16},{0,8},{4,0},{13,5},{... | collective-permute-start | bytes 1966088 | tf_op jit(solution)/shard_map/ppermute | solution.py:410
  155.1 28.1 %collective-permute-start.22 = (bf16[256,1280]{1,0:T(8,128)(2,1)S(1)}, bf16[256,1280]{1,0:T(8,128)(2,1)S(1)}, u32[]{:S(2)}, u32[]{:S(2)}) collective-permute-start(bf16[256,1280]{1,0:T(8,128)(2,1)S(1)} %collective-permute-done.20.refs_15_), channel_id=1, source_target_pairs={{4,12},{12,20},{20,28},{28,24},{24,16},{16,8},{8,0},{0,4},{5,13},{... | collective-permute-start | bytes 1966088 | tf_op jit(solution)/shard_map/ppermute | solution.py:410
  169.2 34.0 %collective-permute-start.24 = (bf16[256,1280]{1,0:T(8,128)(2,1)S(1)}, bf16[256,1280]{1,0:T(8,128)(2,1)S(1)}, u32[]{:S(2)}, u32[]{:S(2)}) collective-permute-start(bf16[256,1280]{1,0:T(8,128)(2,1)S(1)} %collective-permute-done.16.refs_10_), channel_id=1, source_target_pairs={{4,12},{12,20},{20,28},{28,24},{24,16},{16,8},{8,0},{0,4},{5,13},{... | collective-permute-start | bytes 1966088 | tf_op jit(solution)/shard_map/ppermute | solution.py:410
  170.0 34.4 %collective-permute-start.25 = (bf16[256,1280]{1,0:T(8,128)(2,1)S(1)}, bf16[256,1280]{1,0:T(8,128)(2,1)S(1)}, u32[]{:S(2)}, u32[]{:S(2)}) collective-permute-start(bf16[256,1280]{1,0:T(8,128)(2,1)S(1)} %collective-permute-done.23.refs_18_), channel_id=1, source_target_pairs={{12,4},{20,12},{28,20},{24,28},{16,24},{8,16},{0,8},{4,0},{13,5},{... | collective-permute-start | bytes 1966088 | tf_op jit(solution)/shard_map/ppermute | solution.py:410
  173.6 21.1 %collective-permute-start.34 = (bf16[1280,128]{1,0:T(8,128)(2,1)S(1)}, bf16[1280,128]{1,0:T(8,128)(2,1)S(1)}, u32[]{:S(2)}, u32[]{:S(2)}) collective-permute-start(bf16[1280,128]{1,0:T(8,128)(2,1)S(1)} %collective-permute-done.30.refs_6_), channel_id=1, source_target_pairs={{12,4},{20,12},{28,20},{24,28},{16,24},{8,16},{0,8},{4,0},{13,5},{... | collective-permute-start | bytes 983048 | tf_op jit(solution)/shard_map/ppermute | solution.py:410
  183.2 18.4 %collective-permute-start.36 = (bf16[1280,128]{1,0:T(8,128)(2,1)S(1)}, bf16[1280,128]{1,0:T(8,128)(2,1)S(1)}, u32[]{:S(2)}, u32[]{:S(2)}) collective-permute-start(bf16[1280,128]{1,0:T(8,128)(2,1)S(1)} %collective-permute-done.32.refs_8_), channel_id=1, source_target_pairs={{4,12},{12,20},{20,28},{28,24},{24,16},{16,8},{8,0},{0,4},{5,13},{... | collective-permute-start | bytes 983048 | tf_op jit(solution)/shard_map/ppermute | solution.py:410
  184.0 18.4 %collective-permute-start.41 = (bf16[1280,128]{1,0:T(8,128)(2,1)S(1)}, bf16[1280,128]{1,0:T(8,128)(2,1)S(1)}, u32[]{:S(2)}, u32[]{:S(2)}) collective-permute-start(bf16[1280,128]{1,0:T(8,128)(2,1)S(1)} %collective-permute-done.35.refs_11_), channel_id=1, source_target_pairs={{12,4},{20,12},{28,20},{24,28},{16,24},{8,16},{0,8},{4,0},{13,5},{... | collective-permute-start | bytes 983048 | tf_op jit(solution)/shard_map/ppermute | solution.py:410
  194.6 29.8 %collective-permute-start.37 = (bf16[1280,128]{1,0:T(8,128)(2,1)S(1)}, bf16[1280,128]{1,0:T(8,128)(2,1)S(1)}, u32[]{:S(2)}, u32[]{:S(2)}) collective-permute-start(bf16[1280,128]{1,0:T(8,128)(2,1)S(1)} %collective-permute-done.34.refs_10_), channel_id=1, source_target_pairs={{12,4},{20,12},{28,20},{24,28},{16,24},{8,16},{0,8},{4,0},{13,5},{... | collective-permute-start | bytes 983048 | tf_op jit(solution)/shard_map/ppermute | solution.py:410
  201.6 25.3 %collective-permute-start.40 = (bf16[1280,128]{1,0:T(8,128)(2,1)S(1)}, bf16[1280,128]{1,0:T(8,128)(2,1)S(1)}, u32[]{:S(2)}, u32[]{:S(2)}) collective-permute-start(bf16[1280,128]{1,0:T(8,128)(2,1)S(1)} %collective-permute-done.33.refs_9_), channel_id=1, source_target_pairs={{4,12},{12,20},{20,28},{28,24},{24,16},{16,8},{8,0},{0,4},{5,13},{... | collective-permute-start | bytes 983048 | tf_op jit(solution)/shard_map/ppermute | solution.py:410
  202.4 23.4 %collective-permute-start.44 = (bf16[1280,128]{1,0:T(8,128)(2,1)S(1)}, bf16[1280,128]{1,0:T(8,128)(2,1)S(1)}, u32[]{:S(2)}, u32[]{:S(2)}) collective-permute-start(bf16[1280,128]{1,0:T(8,128)(2,1)S(1)} %collective-permute-done.36.refs_3_), channel_id=1, source_target_pairs={{4,12},{12,20},{20,28},{28,24},{24,16},{16,8},{8,0},{0,4},{5,13},{... | collective-permute-start | bytes 983048 | tf_op jit(solution)/shard_map/ppermute | solution.py:410
  203.1 22.6 %collective-permute-start.45 = (bf16[1280,128]{1,0:T(8,128)(2,1)S(1)}, bf16[1280,128]{1,0:T(8,128)(2,1)S(1)}, u32[]{:S(2)}, u32[]{:S(2)}) collective-permute-start(bf16[1280,128]{1,0:T(8,128)(2,1)S(1)} %collective-permute-done.41.refs_4_), channel_id=1, source_target_pairs={{12,4},{20,12},{28,20},{24,28},{16,24},{8,16},{0,8},{4,0},{13,5},{... | collective-permute-start | bytes 983048 | tf_op jit(solution)/shard_map/ppermute | solution.py:410
  205.4 7.9 %collective-permute-start.26 = (bf16[1,2560]{1,0:T(2,128)(2,1)S(1)}, bf16[1,2560]{1,0:T(2,128)(2,1)S(1)}, u32[]{:S(2)}, u32[]{:S(2)}) collective-permute-start(bf16[1,2560]{1,0:T(2,128)(2,1)S(1)} %pad_maximum_fusion.1), channel_id=1, source_target_pairs={{0,4},{4,8},{8,12},{12,16},{16,20},{20,24},{24,28},{1,5},{5,9},{9,... | collective-permute-start | bytes 15368 | tf_op jit(solution)/shard_map/ppermute | solution.py:370
  213.2 6.0 %collective-permute-start.27 = (bf16[1,2560]{1,0:T(2,128)(2,1)S(1)}, bf16[1,2560]{1,0:T(2,128)(2,1)S(1)}, u32[]{:S(2)}, u32[]{:S(2)}) collective-permute-start(bf16[1,2560]{1,0:T(2,128)(2,1)S(1)} %pad_maximum_fusion.2), channel_id=1, source_target_pairs={{4,0},{8,4},{12,8},{16,12},{20,16},{24,20},{28,24},{5,1},{9,5},{13... | collective-permute-start | bytes 15368 | tf_op jit(solution)/shard_map/ppermute | solution.py:371
  225.7 4.5 %collective-permute-start.38 = (bf16[512,512]{1,0:T(8,128)(2,1)S(1)}, bf16[512,512]{1,0:T(8,128)(2,1)S(1)}, u32[]{:S(2)}, u32[]{:S(2)}) collective-permute-start(bf16[512,512]{1,0:T(8,128)(2,1)S(1)} %get-tuple-element.52), channel_id=1, source_target_pairs={{0,1},{1,0},{2,3},{3,2},{4,5},{5,4},{6,7},{7,6},{8,9},{9,8},{10,11... | collective-permute-start | bytes 1572872 | tf_op jit(solution)/shard_map/ppermute | solution.py:48
  226.3 3.1 %collective-permute-start.46 = (bf16[512,256]{1,0:T(8,128)(2,1)S(1)}, bf16[512,256]{1,0:T(8,128)(2,1)S(1)}, u32[]{:S(2)}, u32[]{:S(2)}) collective-permute-start(bf16[512,256]{1,0:T(8,128)(2,1)S(1)} %shard_map.202), channel_id=1, source_target_pairs={{0,1},{1,0},{2,3},{3,2},{4,5},{5,4},{6,7},{7,6},{8,9},{9,8},{10,11... | collective-permute-start | bytes 786440 | tf_op jit(solution)/shard_map/ppermute | solution.py:48
  228.1 2.7 %collective-permute-start.42 = (bf16[512,512]{1,0:T(8,128)(2,1)S(1)}, bf16[512,512]{1,0:T(8,128)(2,1)S(1)}, u32[]{:S(2)}, u32[]{:S(2)}) collective-permute-start(bf16[512,512]{1,0:T(8,128)(2,1)S(1)} %get-tuple-element.54), channel_id=1, source_target_pairs={{0,1},{1,0},{2,3},{3,2},{4,5},{5,4},{6,7},{7,6},{8,9},{9,8},{10,11... | collective-permute-start | bytes 1572872 | tf_op jit(solution)/shard_map/ppermute | solution.py:48
  229.5 3.3 %collective-permute-start.47 = (bf16[512,256]{1,0:T(8,128)(2,1)S(1)}, bf16[512,256]{1,0:T(8,128)(2,1)S(1)}, u32[]{:S(2)}, u32[]{:S(2)}) collective-permute-start(bf16[512,256]{1,0:T(8,128)(2,1)S(1)} %fusion.28), channel_id=1, source_target_pairs={{1,3},{5,7},{8,10},{12,14},{19,17},{23,21},{26,24},{30,28}} | collective-permute-start | bytes 786440 | tf_op jit(solution)/shard_map/ppermute | solution.py:642
  230.4 8.4 %collective-permute-start.39 = (bf16[512,256]{1,0:T(8,128)(2,1)S(1)}, bf16[512,256]{1,0:T(8,128)(2,1)S(1)}, u32[]{:S(2)}, u32[]{:S(2)}) collective-permute-start(bf16[512,256]{1,0:T(8,128)(2,1)S(1)} %slice.554), channel_id=1, source_target_pairs={{0,2},{1,3},{2,0},{3,1},{4,6},{5,7},{6,4},{7,5},{8,10},{9,11},{10,... | collective-permute-start | bytes 786440 | tf_op jit(solution)/shard_map/ppermute | solution.py:48
  231.0 13.4 %collective-permute-start.43 = (bf16[512,256]{1,0:T(8,128)(2,1)S(1)}, bf16[512,256]{1,0:T(8,128)(2,1)S(1)}, u32[]{:S(2)}, u32[]{:S(2)}) collective-permute-start(bf16[512,256]{1,0:T(8,128)(2,1)S(1)} %slice.553), channel_id=1, source_target_pairs={{0,2},{1,3},{2,0},{3,1},{4,6},{5,7},{6,4},{7,5},{8,10},{9,11},{10,... | collective-permute-start | bytes 786440 | tf_op jit(solution)/shard_map/ppermute | solution.py:48
